TPU v7x, 32 devices: a whole 2x2x4 slice. The times are simulated.
32 devices in a mesh: sp: 4 (over y, x), tp: 8 (over z, core).
Axes of the slice: x: 2, y: 2, z: 4, core: 2. Of those that a mesh axis runs over, the one named last changes fastest.
Arguments:
- queries: bfloat16 [3072, 16, 128], P('sp', 'tp'), may hold values from -240 to 240
- key_pairs: bfloat16 [3072, 16, 128], P('sp', 'tp'), may hold values from -11 to 11
- head_values: bfloat16 [3072, 16, 128], P('sp', 'tp'), may hold values from -6 to 6
- lambdas: float32 [16], P('tp'), may hold values from 0.3 to 0.8
- head_gain: float32 [128], replicated, may hold values from 0.1 to 1.9
- out_weight: bfloat16 [2048, 2048], replicated, may hold values from -0.125 to 0.125
- residual: bfloat16 [3072, 2048], P(('sp', 'tp')), may hold values from -6 to 6
- norm_gain: float32 [2048], replicated, may hold values from 0.1 to 1.9
- expert_ids: int32 [3072, 2], P(('sp', 'tp')), may hold values from 0 to 7, all different within a row; in each aligned block of 96 rows (0 to 95, 96 to 191, ...) at most 32 rows name the same one
- route_weights: float32 [3072, 2], P(('sp', 'tp')), may hold values from 0.2 to 1
- gate_weight: bfloat16 [8, 2048, 2048], P('sp', None, 'tp'), may hold values from -0.125 to 0.125
- up_weight: bfloat16 [8, 2048, 2048], P('sp', None, 'tp'), may hold values from -0.125 to 0.125
- down_weight: bfloat16 [8, 2048, 2048], P('sp', 'tp'), may hold values from -0.125 to 0.125
Outputs:
- merged: bfloat16 [3072, 2048], P(('sp', 'tp'))
Inputs may be any that keep to these rules, and one draw needn't show every extreme that they name: `expert_ids`: within the rows of one device each expert is named at most 32 times, and exactly 32 times in some device.
All inputs are finite; a program needn't handle non-finite values.
Results may differ from a plain program's by a relative error of at most 0.019.
Values may be sent and summed in bfloat16 or wider, within the bound.
No kernel may reach another device: no remote copies, remote signals or barrier semaphores. Data moves between devices by JAX's collectives and lax.ppermute only.
A program may use at most 128 MiB of HBM per device.

v0:
```python
import math

import jax
import jax.numpy as jnp
from jax import lax
from jax.sharding import PartitionSpec as P


def shards(
    queries,
    key_pairs,
    head_values,
    lambdas,
    head_gain,
    out_weight,
    residual,
    norm_gain,
    expert_ids,
    route_weights,
    gate_weight,
    up_weight,
    down_weight,
):
    tokens_here, heads_here, pair_width = queries.shape
    half_width = pair_width // 2
    value_width = head_values.shape[2]
    score_scale = half_width ** (-0.5)
    query_pos = lax.axis_index("sp") * tokens_here + jnp.arange(tokens_here, dtype=jnp.int32)
    split_queries = queries.reshape(tokens_here, heads_here, 2, half_width)
    start_state = (
        jnp.full((2, heads_here, tokens_here), -1e30, jnp.float32),
        jnp.zeros((2, heads_here, tokens_here), jnp.float32),
        jnp.zeros((2, heads_here, tokens_here, value_width), jnp.float32),
    )
    key_piece = lax.all_gather(key_pairs, "sp", axis=0, tiled=True)
    value_piece = lax.all_gather(head_values, "sp", axis=0, tiled=True)
    span_rows = key_piece.shape[0]
    width_rows = math.gcd(span_rows, 512)

    def block_step(block_index, state):
        running_max, totals, summed = state
        offset = block_index * width_rows
        key_block = lax.dynamic_slice_in_dim(key_piece, offset, width_rows, 0).reshape(
            width_rows, heads_here, 2, half_width
        )
        value_block = lax.dynamic_slice_in_dim(value_piece, offset, width_rows, 0)
        key_pos = offset + jnp.arange(width_rows, dtype=jnp.int32)
        allowed = key_pos[None, :] <= query_pos[:, None]
        scores = (
            jnp.einsum(
                "qhcd,khcd->chqk", split_queries, key_block, preferred_element_type=jnp.float32
            )
            * score_scale
        )
        scores = jnp.where(allowed[None, None], scores, -jnp.inf)
        fresh_max = jnp.maximum(running_max, jnp.max(scores, axis=3))
        decay = jnp.exp(running_max - fresh_max)
        weights = jnp.exp(scores - fresh_max[..., None])
        totals = totals * decay + jnp.sum(weights, axis=3)
        summed = summed * decay[..., None] + jnp.einsum(
            "chqk,khv->chqv",
            weights.astype(jnp.bfloat16),
            value_block,
            preferred_element_type=jnp.float32,
        )
        return (fresh_max, totals, summed)

    def through(state):
        return lax.fori_loop(0, span_rows // width_rows, block_step, state)

    def untouched(state):
        return state

    running_max, totals, summed = lax.cond(
        jnp.int32(0) <= query_pos[-1], through, untouched, start_state
    )
    mixed = (
        summed[0] / totals[0][..., None] - lambdas[:, None, None] * summed[1] / totals[1][..., None]
    )
    normed_heads = (
        mixed * lax.rsqrt(jnp.mean(mixed * mixed, axis=2, keepdims=True) + 1e-06) * head_gain
    )
    attended = (
        jnp.transpose(normed_heads, (1, 0, 2))
        .reshape(tokens_here, heads_here * value_width)
        .astype(jnp.bfloat16)
    )
    rows_here = residual.shape[0]
    regrouped = lax.all_to_all(attended, "tp", split_axis=0, concat_axis=1, tiled=True)
    projected = jnp.dot(regrouped, out_weight, preferred_element_type=jnp.float32)
    updated = (residual.astype(jnp.float32) + projected).astype(jnp.bfloat16)
    widened = updated.astype(jnp.float32)
    normed = (
        widened * lax.rsqrt(jnp.mean(widened * widened, axis=1, keepdims=True) + 1e-06) * norm_gain
    ).astype(jnp.bfloat16)
    route_count = expert_ids.shape[1]
    local_experts = gate_weight.shape[0]
    sp_count = lax.axis_size("sp")
    expert_count = local_experts * sp_count
    capacity = max(2, 4 * rows_here * route_count // (3 * expert_count))
    model_width = normed.shape[1]
    flat_ids = expert_ids.reshape(-1)
    indicator = (flat_ids[:, None] == jnp.arange(expert_count, dtype=jnp.int32)[None, :]).astype(
        jnp.int32
    )
    ranking = jnp.sum(jnp.cumsum(indicator, axis=0) * indicator, axis=1) - 1
    slots = flat_ids * capacity + ranking
    sources = jnp.arange(rows_here * route_count, dtype=jnp.int32) // route_count
    outgoing = (
        jnp.zeros((expert_count * capacity, model_width), jnp.bfloat16)
        .at[slots]
        .set(normed[sources])
    )
    arrived = lax.all_to_all(
        outgoing.reshape(sp_count, local_experts, capacity, model_width),
        "sp",
        split_axis=0,
        concat_axis=0,
        tiled=True,
    )
    piece_rows = lax.all_gather(arrived[None], "tp", axis=0, tiled=True)
    gate_part = jnp.einsum(
        "tsecd,edf->tsecf", piece_rows, gate_weight, preferred_element_type=jnp.float32
    )
    up_part = jnp.einsum(
        "tsecd,edf->tsecf", piece_rows, up_weight, preferred_element_type=jnp.float32
    )
    inner_rows = (jax.nn.silu(gate_part) * up_part).astype(jnp.bfloat16)
    partial_value = jnp.einsum(
        "tsecf,efd->tsecd", inner_rows, down_weight, preferred_element_type=jnp.float32
    )
    reduced = lax.psum_scatter(
        partial_value.astype(jnp.bfloat16), "tp", scatter_dimension=0, tiled=True
    )
    returned = lax.all_to_all(reduced[0], "sp", split_axis=0, concat_axis=0, tiled=True)
    picked = (
        returned.reshape(expert_count * capacity, model_width)[slots]
        .astype(jnp.float32)
        .reshape(rows_here, route_count, model_width)
    )
    moe_sum = jnp.sum(picked * route_weights[:, :, None], axis=1)
    return (updated.astype(jnp.float32) + moe_sum).astype(jnp.bfloat16)


def solution(mesh):
    placed = (
        P("sp", "tp", None),
        P("sp", "tp", None),
        P("sp", "tp", None),
        P("tp"),
        P(),
        P(),
        P(("sp", "tp"), None),
        P(),
        P(("sp", "tp"), None),
        P(("sp", "tp"), None),
        P("sp", None, "tp"),
        P("sp", None, "tp"),
        P("sp", "tp", None),
    )
    return jax.shard_map(
        shards, mesh=mesh, in_specs=placed, out_specs=P(("sp", "tp"), None), check_vma=False
    )
```

profile of v0, /device:TPU:0, one launch (start us, length us, event | category | flops | bytes accessed | tf_op | source)
XLA Modules:
  0.0 527.9 jit_solution(12281369762968562152)
XLA Ops:
  6.5 2.1 copy.39
  8.7 1.9 copy.40
  10.7 0.6 slice.24
  12.2 0.6 reduce-window.6
  13.1 29.7 %all-gather.5.cloned.1.call-done = bf16[3072,2,128]{0,2,1:T(8,128)(2,1)} async-done(((bf16[768,2,128]{0,2,1:T(8,128)(2,1)}), bf16[3072,2,128]{0,2,1:T(8,128)(2,1)}) %all-gather.5.cloned.1.call-update) | async-done | bytes 1572880 | tf_op jit(solution)/shard_map/all_gather | solution.py:35
  42.8 32.7 %all-gather.7.cloned.1.call-done = bf16[3072,2,128]{0,2,1:T(8,128)(2,1)} async-done(((bf16[768,2,128]{0,2,1:T(8,128)(2,1)}), bf16[3072,2,128]{0,2,1:T(8,128)(2,1)}) %all-gather.7.cloned.1.call-update) | async-done | bytes 1572880 | tf_op jit(solution)/shard_map/all_gather | solution.py:36
  75.5 83.6 %conditional.1 = (f32[2,2,768]{2,1,0:T(2,128)}, f32[2,2,768,128]{2,3,0,1:T(8,128)}) conditional(s32[]{:T(128)} %bitcast.1, () %tuple.27, (bf16[768,2,128]{2,1,0:T(2,128)(2,1)S(1)}, s32[768]{0:T(1024)S(1)}, bf16[3072,2,128]{0,2,1:T(8,128)(2,1)}, bf16[3072,2,128]{0,2,1:T(8,128)(2,1)}) %tuple.70), branch_computations={%region_0.0_spmd, %region_1.6_spmd} | conditional | flops 618151424 | bytes 26430768 | solution.py:74
  75.5 0.4 copy.41
  76.0 83.1 %while.17 = (s32[]{:T(128)}, f32[2,2,768]{2,1,0:T(2,128)S(1)}, f32[2,2,768]{2,1,0:T(2,128)}, f32[2,2,768,128]{2,3,0,1:T(8,128)}, s32[768]{0:T(1024)S(1)}, /*inde...) while((s32[]{:T(128)}, f32[2,2,768]{2,1,0:T(2,128)S(1)}, ...), condition=%wide.region_5.5_spmd.clone, body=%wide.region_2.4_spmd.clone.sunk | while | flops 618151424 | bytes 24857784 | solution.py:69
  76.0 1.0 constant_dynamic-slice_fusion.2
  77.3 3.9 fusion.56
  81.2 4.3 fusion.58
  85.5 0.6 fusion.59
  86.1 2.7 bitcast_add_fusion.2
  88.8 1.0 constant_dynamic-slice_fusion.2
  90.1 3.9 fusion.56
  94.0 4.3 fusion.58
  98.3 1.3 fusion.59
  99.6 3.3 bitcast_add_fusion.2
  102.9 1.0 constant_dynamic-slice_fusion.2
  104.2 3.9 fusion.56
  108.0 4.3 fusion.58
  112.3 1.3 fusion.59
  113.7 3.3 bitcast_add_fusion.2
  117.0 1.0 constant_dynamic-slice_fusion.2
  118.2 3.9 fusion.56
  122.1 4.3 fusion.58
  126.4 1.3 fusion.59
  127.7 3.3 bitcast_add_fusion.2
  131.0 1.0 constant_dynamic-slice_fusion.2
  132.3 3.9 fusion.56
  136.2 4.3 fusion.58
  140.4 1.3 fusion.59
  141.8 3.3 bitcast_add_fusion.2
  145.1 1.0 constant_dynamic-slice_fusion.2
  146.3 3.9 fusion.56
  150.2 4.3 fusion.58
  154.5 1.3 fusion.59
  155.8 3.3 bitcast_add_fusion.2
  159.1 0.7 slice_bitcast_fusion.2
  159.9 1.6 multiply_reduce_fusion.2
  161.6 0.4 copy.43
  162.1 1.0 convert_element_type.62
  163.1 4.6 all-to-all-start
  168.0 12.2 %all-to-all-done = bf16[8,96,256]{2,1,0:T(8,128)(2,1)S(1)} async-done(((bf16[8,96,256]{2,1,0:T(8,128)(2,1)}), bf16[8,96,256]{2,1,0:T(8,128)(2,1)S(1)}, u32[]{:S(2)}, u32[]{:S(2)}) %all-to-all-start) | async-done | bytes 393248 | tf_op jit(solution)/shard_map/all_to_all | solution.py:89
  180.3 5.0 multiply_reduce_fusion.1
  185.3 0.9 copy-done.1
  186.3 4.5 scatter_custom_fusion
  190.9 17.2 %all_to_all.26 = bf16[4,2,32,2048]{3,2,1,0:T(8,128)(2,1)} all-to-all(bf16[4,2,32,2048]{3,2,1,0:T(8,128)(2,1)S(1)} %bitcast.127), channel_id=1, replica_groups=mesh['sp'=4,'tp'=8] {'sp'}, dimensions={0} | all-to-all | bytes 2097152 | tf_op jit(solution)/shard_map/all_to_all | solution.py:114
  208.1 80.3 %all-gather.9.cloned.1.call-done = bf16[32,2,32,2048]{3,2,1,0:T(8,128)(2,1)} async-done(((bf16[4,2,32,2048]{3,2,1,0:T(8,128)(2,1)}), bf16[32,2,32,2048]{3,2,1,0:T(8,128)(2,1)}) %all-gather.9.cloned.1.call-update) | async-done | bytes 8388624 | tf_op jit(solution)/shard_map/all_gather | solution.py:121
  288.4 8.4 %copy.47 = bf16[32,2,32,2048]{3,2,0,1:T(8,128)(2,1)} copy(bf16[32,2,32,2048]{3,2,1,0:T(8,128)(2,1)} %all-gather.9.cloned.1.call-done) | data formatting | bytes 16777216 | tf_op jit(solution)/shard_map/all_gather | solution.py:121
  296.9 7.1 %fusion.17 = f32[2,8,4,32,256]{4,3,2,1,0:T(8,128)} fusion(bf16[8,4,2,32,2048]{4,3,1,0,2:T(8,128)(2,1)} %bitcast.124, bf16[2,2048,256]{2,1,0:T(8,128)(2,1)S(1)} %copy-done.10), kind=kOutput, calls=%fused_computation.30 | convolution fusion | flops 2147483648 | bytes 12582912 | tf_op jit(solution)/shard_map/tsecd,edf->tsecf/dot_general | solution.py:125
  303.9 13.5 %convert_bitcast_fusion = bf16[8,4,2,32,2048]{4,3,1,0,2:T(8,128)(2,1)} fusion(bf16[2,256,2048]{2,1,0:T(8,128)(2,1)S(1)} %copy-done, f32[2,8,4,32,256]{4,3,2,1,0:T(8,128)} %fusion.17, bf16[8,4,2,32,2048]{4,3,1,0,2:T(8,128)(2,1)} %bitcast.125, bf16[2,2048,256]{2,1,0:T(8,128)(2,1)} %param.27), kind=kOutput, calls=%fused_computation.25 | convolution fusion | flops 4302307328 | bytes 23068672 | tf_op jit(solution)/shard_map/tsecf,efd->tsecd/dot_general | solution.py:129
  317.5 0.6 copy-done.11
  318.1 0.6 dynamic-slice
  318.7 173.0 %all-reduce.4.cloned.1.call-done = bf16[8,4,2,32,2048]{4,3,1,0,2:T(8,128)(2,1)} async-done(((bf16[8,4,2,32,2048]{4,3,1,0,2:T(8,128)(2,1)}), bf16[8,4,2,32,2048]{4,3,1,0,2:T(8,128)(2,1)}) %all-reduce.4.cloned.1.call-update) | async-done | bytes 8388624
  491.6 1.9 dynamic-slice_bitcast_fusion
  493.6 1.0 copy.48
  494.6 3.6 all-to-all-start.2
  498.4 13.3 %all-to-all-done.2 = bf16[4,2,32,2048]{3,2,1,0:T(8,128)(2,1)S(1)} async-done(((bf16[4,2,32,2048]{3,2,1,0:T(8,128)(2,1)}), bf16[4,2,32,2048]{3,2,1,0:T(8,128)(2,1)S(1)}, u32[]{:S(2)}, u32[]{:S(2)}) %all-to-all-start.2) | async-done | bytes 1048608 | tf_op jit(solution)/shard_map/all_to_all | solution.py:135
  511.7 2.0 gather_fusion
  513.8 3.0 reshape.182
  516.8 3.7 multiply_reduce_fusion
  520.5 0.8 add_convert_fusion
  (88 shorter events, 3.4 us)
Async XLA Ops:
  6.5 297.4 %copy-start = (bf16[2,256,2048]{2,1,0:T(8,128)(2,1)S(1)}, bf16[2,256,2048]{2,1,0:T(8,128)(2,1)}, u32[]{:S(2)}) copy-start(bf16[2,256,2048]{2,1,0:T(8,128)(2,1)} %param.29) | copy-start | bytes 6291460
  6.5 5.4 %copy-start.6 = (s32[96,2]{0,1:T(2,128)S(1)}, s32[96,2]{0,1:T(2,128)}, u32[]{:S(2)}) copy-start(s32[96,2]{0,1:T(2,128)} %param.25) | copy-start | bytes 2308
  6.5 69.0 %copy-start.3 = (bf16[768,2,128]{2,1,0:T(2,128)(2,1)S(1)}, bf16[768,2,128]{2,1,0:T(2,128)(2,1)}, u32[]{:S(2)}) copy-start(bf16[768,2,128]{2,1,0:T(2,128)(2,1)} %param.17) | copy-start | bytes 1179652
  6.5 36.2 %all-gather.5.cloned.1.call-start = ((), (), s32[]{:S(2)}) async-start(), calls=%async_computation.3 | async-start | bytes 1966080 | tf_op jit(solution)/shard_map/all_gather | solution.py:35
  8.6 66.9 %all-gather.7.cloned.1.call-start = ((), (), s32[]{:S(2)}) async-start(), calls=%async_computation.4 | async-start | bytes 1966080 | tf_op jit(solution)/shard_map/all_gather | solution.py:36
  75.5 84.3 %copy-start.8 = (f32[2]{0:T(128)S(1)}, f32[2]{0:T(128)}, u32[]{:S(2)}) copy-start(f32[2]{0:T(128)} %param.20) | copy-start | bytes 28
  159.1 2.4 copy-start.9
  161.5 18.7 %copy-start.4 = (bf16[96,2048]{1,0:T(8,128)(2,1)S(1)}, bf16[96,2048]{1,0:T(8,128)(2,1)}, u32[]{:S(2)}) copy-start(bf16[96,2048]{1,0:T(8,128)(2,1)} %param.23) | copy-start | bytes 1179652
  163.1 17.1 %all-to-all-start = ((bf16[8,96,256]{2,1,0:T(8,128)(2,1)}), bf16[8,96,256]{2,1,0:T(8,128)(2,1)S(1)}, u32[]{:S(2)}, u32[]{:S(2)}) async-start(bf16[8,96,256]{2,1,0:T(8,128)(2,1)} %convert_element_type.62), calls=%async_computation | async-start | bytes 786432 | tf_op jit(solution)/shard_map/all_to_all | solution.py:89
  167.7 120.8 %all-gather.9.cloned.1.call-start = ((), (), s32[]{:S(2)}) async-start(), calls=%async_computation.5 | async-start | bytes 9437184 | tf_op jit(solution)/shard_map/all_gather | solution.py:121
  180.2 5.9 %copy-start.5 = (f32[2048]{0:T(1024)S(1)}, f32[2048]{0:T(1024)}, u32[]{:S(2)}) copy-start(f32[2048]{0:T(1024)} %param.24) | copy-start | bytes 24580
  185.3 0.9 copy-start.1
  208.1 283.5 %all-reduce.4.cloned.1.call-start = ((), (), s32[]{:S(2)}) async-start(), calls=%async_computation.6 | async-start | bytes 16777216
  288.4 8.4 %copy-start.10 = (bf16[2,2048,256]{2,1,0:T(8,128)(2,1)S(1)}, bf16[2,2048,256]{2,1,0:T(8,128)(2,1)}, u32[]{:S(2)}) copy-start(bf16[2,2048,256]{2,1,0:T(8,128)(2,1)} %param.28) | copy-start | bytes 6291460
  317.4 0.7 copy-start.11
  493.6 4.7 copy-start.7
  494.6 17.1 %all-to-all-start.2 = ((bf16[4,2,32,2048]{3,2,1,0:T(8,128)(2,1)}), bf16[4,2,32,2048]{3,2,1,0:T(8,128)(2,1)S(1)}, u32[]{:S(2)}, u32[]{:S(2)}) async-start(bf16[4,2,32,2048]{3,2,1,0:T(8,128)(2,1)} %copy.48), calls=%async_computation.2 | async-start | bytes 2097152 | tf_op jit(solution)/shard_map/all_to_all | solution.py:135
  513.8 6.8 %copy-start.2 = (f32[96,2048]{1,0:T(8,128)S(1)}, f32[96,2048]{1,0:T(8,128)}, u32[]{:S(2)}) copy-start(f32[96,2048]{1,0:T(8,128)} %copy-done.1) | copy-start | bytes 2359300
Sparse Core Ops, SparseCore 0:
  9.2 33.5 all-gather.4
  44.6 30.8 all-gather.6
  208.2 80.1 all-gather.8
  317.6 174.0 all-reduce.3
where the time goes:
time: 529 us; the launch traced here: 528 us
  waiting for transfers between devices  341 us (64%)
  matrix products  67.9 us (13%)
  other arithmetic  41.9 us (8%)
  local copies, waits for them, and re-layouts  37.1 us (7%)
  blocking collectives  17.2 us (3%)
  between operations  14 us (3%)
  starting transfers between devices  8.38 us (2%)
    unnamed x5, waiting for transfers between devices  173 us
    all_gather x1, waiting for transfers between devices, shards(): piece_rows = lax.all_gather(arrived[None], 'tp', axis=0, tiled=True)  80.3 us
    all_gather x1, waiting for transfers between devices, shards(): value_piece = lax.all_gather(head_values, 'sp', axis=0, tiled=True)  32.7 us
    all_gather x1, waiting for transfers between devices, shards(): key_piece = lax.all_gather(key_pairs, 'sp', axis=0, tiled=True)  29.7 us
    convert_element_type x6, other arithmetic, block_step(): weights.astype(jnp.bfloat16)  25.6 us
    dot_general x6, matrix products, block_step(): jnp.einsum('qhcd,khcd->chqk', split_queries, key_block, preferred_element...  23.2 us
    dot_general x6, matrix products, block_step(): jnp.einsum('chqk,khv->chqv', weights.astype(jnp.bfloat16), value_block, p...  19.2 us
    all_to_all x1, blocking collectives, shards(): lax.all_to_all(outgoing.reshape(sp_count, local_experts, capacity, model_...  17.2 us
  transfers between devices with their start and end apart: 6, of which 6 were waited for; matrix products, arithmetic and copies ran while one was open for 1% of the time, Pallas kernels for 0%

commit v1 on v0

--- a/solution.py
+++ b/solution.py
@@ -1,9 +1,369 @@
+import functools
 import math
 
 import jax
 import jax.numpy as jnp
 from jax import lax
+from jax.experimental import pallas as pl
+from jax.experimental.pallas import tpu as pltpu
 from jax.sharding import PartitionSpec as P
+
+LANES = 128
+OWNERS_PER_TILE = 4
+
+
+def attention_kernel(
+    part_ref, lam_ref, gain_ref, rows_ref, out_ref, stack_ref, acc_ref, top_ref, *, sub, key_rows, parts, scale
+):
+    tile = pl.program_id(0)
+    tile_rows = OWNERS_PER_TILE * sub
+    span = tile_rows * parts
+    width = rows_ref.shape[2]
+    half = width // 2
+    query_rows = key_rows // parts
+    tiles_per_source = key_rows // span
+
+    source = tile // tiles_per_source
+    start = pl.multiple_of((tile % tiles_per_source) * tile_rows, tile_rows)
+    query = rows_ref[source, pl.ds(start, tile_rows), :]
+    low = lax.broadcasted_iota(jnp.int32, (tile_rows, width), 1) < half
+    nothing = jnp.zeros_like(query)
+    stack_ref[0:tile_rows, :] = jnp.where(low, query, nothing)
+    stack_ref[tile_rows:, :] = jnp.where(low, nothing, query)
+    top_ref[...] = jnp.full_like(top_ref, -1e30)
+    acc_ref[...] = jnp.zeros_like(acc_ref)
+    ones = jnp.ones((span, LANES), jnp.bfloat16)
+
+    def one_tile(index, diagonal):
+        owner = index // tiles_per_source
+        offset = pl.multiple_of((index % tiles_per_source) * span, span)
+        keys = rows_ref[owner, pl.ds(query_rows + offset, span), :]
+        values = rows_ref[owner, pl.ds(query_rows + key_rows + offset, span), :]
+        scores = (
+            lax.dot_general(
+                stack_ref[...], keys, (((1,), (1,)), ((), ())), preferred_element_type=jnp.float32
+            )
+            * scale
+        )
+        if diagonal:
+            row = lax.broadcasted_iota(jnp.int32, (tile_rows, LANES), 0)
+            place = row + part_ref[0] * sub
+            for step in range(1, OWNERS_PER_TILE):
+                place = place + jnp.where(row >= step * sub, (parts - 1) * sub, 0)
+            gap = place - lax.broadcasted_iota(jnp.int32, (tile_rows, LANES), 1)
+            gap = jnp.concatenate([gap, gap], axis=0)
+            scores = jnp.concatenate(
+                [
+                    jnp.where(gap >= first, scores[:, first : first + LANES], -jnp.inf)
+                    for first in range(0, span, LANES)
+                ],
+                axis=1,
+            )
+        before = top_ref[...]
+        after = jnp.maximum(before, jnp.max(scores, axis=1, keepdims=True))
+        decay = jnp.exp(before - after)
+        weights = jnp.exp(scores - after[:, :1])
+        top_ref[...] = after
+        acc_ref[...] = acc_ref[...] * decay[:, :1] + jnp.dot(
+            weights.astype(jnp.bfloat16),
+            jnp.concatenate([values, ones], axis=1),
+            preferred_element_type=jnp.float32,
+        )
+
+    one_tile(tile, True)
+
+    @pl.loop(0, tile)
+    def _(index):
+        one_tile(index, False)
+
+    first = acc_ref[0:tile_rows, :]
+    second = acc_ref[tile_rows:, :]
+    mixed = (
+        first[:, :width] / first[:, width : width + 1]
+        - lam_ref[0] * second[:, :width] / second[:, width : width + 1]
+    )
+    scaled = mixed * lax.rsqrt(jnp.mean(mixed * mixed, axis=1, keepdims=True) + 1e-06)
+    out_ref[...] = (scaled * gain_ref[...]).astype(out_ref.dtype)
+
+
+def attention(part, lam, gain, arrived, sub, key_rows, parts, scale):
+    sources, _, width = arrived.shape
+    tile_rows = OWNERS_PER_TILE * sub
+    total_rows = sources * key_rows // parts
+    pairs = total_rows * sources * key_rows
+    return pl.pallas_call(
+        functools.partial(attention_kernel, sub=sub, key_rows=key_rows, parts=parts, scale=scale),
+        grid=(total_rows // tile_rows,),
+        out_shape=jax.ShapeDtypeStruct((total_rows, width), jnp.bfloat16),
+        in_specs=[
+            pl.BlockSpec(memory_space=pltpu.SMEM),
+            pl.BlockSpec(memory_space=pltpu.SMEM),
+            pl.BlockSpec((1, width), lambda i: (0, 0)),
+            pl.BlockSpec(memory_space=pltpu.VMEM),
+        ],
+        out_specs=pl.BlockSpec((tile_rows, width), lambda i: (i, 0)),
+        scratch_shapes=[
+            pltpu.VMEM((2 * tile_rows, width), jnp.bfloat16),
+            pltpu.VMEM((2 * tile_rows, width + LANES), jnp.float32),
+            pltpu.VMEM((2 * tile_rows, LANES), jnp.float32),
+        ],
+        compiler_params=pltpu.CompilerParams(vmem_limit_bytes=32 * 1024 * 1024),
+        cost_estimate=pl.CostEstimate(
+            flops=8 * pairs * width, bytes_accessed=2 * arrived.size, transcendentals=pairs
+        ),
+        name="attention",
+    )(part, lam, gain, arrived)
+
+
+def project_kernel(heads_ref, weight_ref, residual_ref, gain_ref, routes_ref, updated_ref, normed_ref, acc_ref, *, parts):
+    step = pl.program_id(0)
+    sub, width = heads_ref.shape[2:]
+    held = heads_ref.shape[0] // parts
+    left = jnp.concatenate(
+        [
+            jnp.concatenate([heads_ref[part * held + head, 0] for head in range(held)], axis=1)
+            for part in range(parts)
+        ],
+        axis=0,
+    )
+    product = jnp.dot(left, weight_ref[...], preferred_element_type=jnp.float32)
+
+    @pl.when(step == 0)
+    def _():
+        acc_ref[...] = residual_ref[...].astype(jnp.float32) + product
+
+    @pl.when(step > 0)
+    def _():
+        acc_ref[...] += product
+
+    @pl.when(step == pl.num_programs(0) - 1)
+    def _():
+        updated = acc_ref[...].astype(jnp.bfloat16)
+        updated_ref[...] = updated
+        wide = updated.astype(jnp.float32)
+        scaled = wide * lax.rsqrt(jnp.mean(wide * wide, axis=1, keepdims=True) + 1e-06)
+        model = wide.shape[1]
+        normed_ref[:, :model] = (scaled * gain_ref[...]).astype(jnp.bfloat16)
+        normed_ref[:, model:] = routes_ref[...]
+
+
+def project(heads, out_weight, residual, gain, routes, parts):
+    sources, columns, sub, width = heads.shape
+    rows, model = residual.shape
+    depth = sources // parts * width
+    return pl.pallas_call(
+        functools.partial(project_kernel, parts=parts),
+        grid=(columns,),
+        out_shape=(
+            jax.ShapeDtypeStruct((rows, model), jnp.bfloat16),
+            jax.ShapeDtypeStruct((rows, model + LANES), jnp.bfloat16),
+        ),
+        in_specs=[
+            pl.BlockSpec((sources, 1, sub, width), lambda i: (0, i, 0, 0)),
+            pl.BlockSpec((depth, model), lambda i: (i, 0)),
+            pl.BlockSpec((rows, model), lambda i: (0, 0)),
+            pl.BlockSpec((1, model), lambda i: (0, 0)),
+            pl.BlockSpec((rows, LANES), lambda i: (0, 0)),
+        ],
+        out_specs=(
+            pl.BlockSpec((rows, model), lambda i: (0, 0)),
+            pl.BlockSpec((rows, model + LANES), lambda i: (0, 0)),
+        ),
+        scratch_shapes=[pltpu.VMEM((rows, model), jnp.float32)],
+        compiler_params=pltpu.CompilerParams(vmem_limit_bytes=24 * 1024 * 1024),
+        cost_estimate=pl.CostEstimate(
+            flops=2 * rows * model * columns * depth, bytes_accessed=2 * out_weight.size, transcendentals=0
+        ),
+        name="project",
+    )(heads, out_weight, residual, gain, routes)
+
+
+def expert_kernel(*refs, blocks, experts):
+    first_ref = refs[0]
+    block_refs = refs[1 : 1 + blocks]
+    gate_a, up_a, down_a, gate_b, up_b, down_b = refs[1 + blocks : 7 + blocks]
+    out_refs = refs[7 + blocks : 7 + 2 * blocks]
+    rows_ref, acc_ref = refs[7 + 2 * blocks :]
+    expert = pl.program_id(0)
+    model = rows_ref.shape[1] - LANES
+
+    @pl.when(expert == 0)
+    def _():
+        place = 0
+        for ref in block_refs:
+            rows_ref[place : place + ref.shape[0], :] = ref[...]
+            place += ref.shape[0]
+
+    routes = rows_ref[:, model:].astype(jnp.float32)
+    lane = lax.broadcasted_iota(jnp.int32, routes.shape, 1)
+    mine = first_ref[0] + expert
+    share = jnp.sum(
+        jnp.where((lane == mine) | (lane == mine + experts), routes, 0.0), axis=1, keepdims=True
+    )
+    rows = rows_ref[:, :model]
+    product = None
+    for gate_ref, up_ref, down_ref in ((gate_a, up_a, down_a), (gate_b, up_b, down_b)):
+        gate = jnp.dot(rows, gate_ref[0], preferred_element_type=jnp.float32)
+        up = jnp.dot(rows, up_ref[0], preferred_element_type=jnp.float32)
+        inner = (gate / (1.0 + jnp.exp(-gate)) * up * share).astype(jnp.bfloat16)
+        term = jnp.dot(inner, down_ref[0], preferred_element_type=jnp.float32)
+        product = term if product is None else product + term
+
+    @pl.when(expert == 0)
+    def _():
+        acc_ref[...] = product
+
+    @pl.when(expert > 0)
+    def _():
+        acc_ref[...] += product
+
+    @pl.when(expert == pl.num_programs(0) - 1)
+    def _():
+        place = 0
+        for ref in out_refs:
+            ref[...] = acc_ref[place : place + ref.shape[0], :].astype(jnp.bfloat16)
+            place += ref.shape[0]
+
+
+def expert_pass(first, blocks, weights, experts):
+    held, model, hidden = weights[0].shape
+    total = sum(block.shape[0] for block in blocks)
+    whole = [pl.BlockSpec(block.shape, lambda i: (0, 0)) for block in blocks]
+    wide = pl.BlockSpec((1, model, hidden), lambda i: (i, 0, 0))
+    tall = pl.BlockSpec((1, hidden, model), lambda i: (i, 0, 0))
+    return pl.pallas_call(
+        functools.partial(expert_kernel, blocks=len(blocks), experts=experts),
+        grid=(held,),
+        out_shape=tuple(
+            jax.ShapeDtypeStruct((block.shape[0], model), jnp.bfloat16) for block in blocks
+        ),
+        in_specs=[pl.BlockSpec(memory_space=pltpu.SMEM), *whole, wide, wide, tall, wide, wide, tall],
+        out_specs=tuple(
+            pl.BlockSpec((block.shape[0], model), lambda i: (0, 0)) for block in blocks
+        ),
+        scratch_shapes=[
+            pltpu.VMEM((total, model + LANES), jnp.bfloat16),
+            pltpu.VMEM((total, model), jnp.float32),
+        ],
+        compiler_params=pltpu.CompilerParams(vmem_limit_bytes=40 * 1024 * 1024),
+        cost_estimate=pl.CostEstimate(
+            flops=12 * held * total * model * hidden,
+            bytes_accessed=12 * held * model * hidden,
+            transcendentals=2 * held * total * hidden,
+        ),
+        name="experts",
+    )(first, *blocks, *weights)
+
+
+def balanced(
+    queries,
+    key_pairs,
+    head_values,
+    lambdas,
+    head_gain,
+    out_weight,
+    residual,
+    norm_gain,
+    expert_ids,
+    route_weights,
+    gate_weight,
+    up_weight,
+    down_weight,
+):
+    tokens, heads, width = queries.shape
+    rows, model = residual.shape
+    sp_count, tp_count = lax.axis_size("sp"), lax.axis_size("tp")
+    sp_index = lax.axis_index("sp")
+    parts = sp_count // heads
+    sub = rows // parts
+    held = gate_weight.shape[0]
+    experts = held * sp_count
+
+    swap = [(i, i ^ 1) for i in range(tp_count)]
+    mine = (gate_weight, up_weight, down_weight)
+    other = tuple(lax.ppermute(w, "tp", swap) for w in mine)
+
+    split = jnp.transpose(
+        queries.reshape(tp_count, parts, sub, heads, width), (1, 3, 0, 2, 4)
+    ).reshape(sp_count, tokens // parts, width)
+    keys = jnp.tile(jnp.transpose(key_pairs, (1, 0, 2)), (parts, 1, 1))
+    values = jnp.tile(jnp.transpose(head_values, (1, 0, 2)), (parts, 1, 1))
+    arrived = lax.all_to_all(
+        jnp.concatenate([split, keys, values], axis=1), "sp", split_axis=0, concat_axis=0, tiled=True
+    )
+    attended = attention(
+        (sp_index // heads).reshape(1),
+        lax.dynamic_slice_in_dim(lambdas, sp_index % heads, 1),
+        head_gain.reshape(1, -1),
+        arrived,
+        sub,
+        tokens,
+        parts,
+        (width // 2) ** (-0.5),
+    )
+    regrouped = lax.all_to_all(
+        attended.reshape(sp_count * tp_count, sub, width),
+        ("sp", "tp"),
+        split_axis=0,
+        concat_axis=0,
+        tiled=True,
+    ).reshape(sp_count, tp_count, sub, width)
+
+    share = jnp.sum(
+        jnp.where(
+            expert_ids[:, :, None] == jnp.arange(experts, dtype=jnp.int32),
+            route_weights[:, :, None],
+            0.0,
+        ),
+        axis=1,
+    )
+    coarse = lax.reduce_precision(share, 8, 7)
+    routes = jnp.concatenate(
+        [coarse, share - coarse, jnp.zeros((rows, LANES - 2 * experts), jnp.float32)], axis=1
+    ).astype(jnp.bfloat16)
+    updated, normed = project(
+        regrouped, out_weight, residual, norm_gain.reshape(1, -1), routes, parts
+    )
+
+    across_x = [(i, i ^ 1) for i in range(sp_count)]
+    across_y = [(i, i ^ 2) for i in range(sp_count)]
+
+    def turned(array, steps):
+        return lax.ppermute(
+            array, "tp", [(i, (i + 2 * steps) % tp_count) for i in range(tp_count)]
+        )
+
+    layers = tp_count // 2
+    cut = rows // 2
+    sources = [normed] + [turned(normed, -k) for k in range(1, layers)]
+    first = (sp_index * held).reshape(1)
+    weights = (*mine, *other)
+    reduced = []
+    for block in sources:
+        by_x = lax.ppermute(block, "sp", across_x)
+        by_y = lax.ppermute(block, "sp", across_y)
+        far_low = lax.ppermute(by_x[:cut], "sp", across_y)
+        far_high = lax.ppermute(by_y[cut:], "sp", across_x)
+        own, to_x, to_y, to_low, to_high = expert_pass(
+            first, (block, by_x, by_y, far_low, far_high), weights, experts
+        )
+        add_low = lax.ppermute(to_low, "sp", across_y)
+        add_high = lax.ppermute(to_high, "sp", across_x)
+        to_x = jnp.concatenate(
+            [(to_x[:cut].astype(jnp.float32) + add_low.astype(jnp.float32)).astype(jnp.bfloat16), to_x[cut:]]
+        )
+        to_y = jnp.concatenate(
+            [to_y[:cut], (to_y[cut:].astype(jnp.float32) + add_high.astype(jnp.float32)).astype(jnp.bfloat16)]
+        )
+        from_x = lax.ppermute(to_x, "sp", across_x)
+        from_y = lax.ppermute(to_y, "sp", across_y)
+        reduced.append(
+            own.astype(jnp.float32) + from_x.astype(jnp.float32) + from_y.astype(jnp.float32)
+        )
+    total = updated.astype(jnp.float32) + reduced[0]
+    for k in range(1, layers):
+        total = total + turned(reduced[k].astype(jnp.bfloat16), k).astype(jnp.float32)
+    return total.astype(jnp.bfloat16)
 
 
 def shards(
@@ -142,6 +502,33 @@
     return (updated.astype(jnp.float32) + moe_sum).astype(jnp.bfloat16)
 
 
+def fits_balanced(queries, residual, expert_ids, gate_weight, sp_count, tp_count):
+    tokens, heads, width = queries.shape
+    rows = residual.shape[0]
+    held = gate_weight.shape[0]
+    if sp_count != 4 or tp_count % 2 or sp_count % heads or width != LANES:
+        return False
+    sub = rows // (sp_count // heads)
+    span = OWNERS_PER_TILE * rows
+    capacity = 4 * rows * expert_ids.shape[1] // (3 * held * sp_count)
+    return (
+        sub % 16 == 0
+        and rows % 32 == 0
+        and tokens % span == 0
+        and span % LANES == 0
+        and 2 * held * sp_count <= LANES
+        and 2 * held * capacity >= rows
+    )
+
+
+def layer(*args):
+    queries, residual, expert_ids, gate_weight = args[0], args[6], args[8], args[10]
+    chosen = fits_balanced(
+        queries, residual, expert_ids, gate_weight, lax.axis_size("sp"), lax.axis_size("tp")
+    )
+    return (balanced if chosen else shards)(*args)
+
+
 def solution(mesh):
     placed = (
         P("sp", "tp", None),
@@ -159,5 +546,5 @@
         P("sp", "tp", None),
     )
     return jax.shard_map(
-        shards, mesh=mesh, in_specs=placed, out_specs=P(("sp", "tp"), None), check_vma=False
-    )
+        layer, mesh=mesh, in_specs=placed, out_specs=P(("sp", "tp"), None), check_vma=False
+    )

time: 529 us -> 263 us (0.50)
  waiting for transfers between devices: 341 us -> 127 us
  matrix products: 67.9 us -> 0 us
  Pallas kernels: 0 us -> 66.1 us
  starting transfers between devices: 8.38 us -> 51.8 us
  other arithmetic: 41.9 us -> 3.84 us
  local copies, waits for them, and re-layouts: 37.1 us -> 12.8 us
  blocking collectives: 17.2 us -> 0 us
  between operations: 14 us -> 0.44 us
    unnamed x5 -> x0, waiting for transfers between devices: 173 us -> none
    all_gather x3 -> x0, waiting for transfers between devices: 143 us -> none  [the longest x1 80.3 us: shards(): piece_rows = lax.all_gather(arrived[None], 'tp', axis=0, tiled=True)]
    ppermute x0 -> x41, waiting for transfers between devices: none -> 91.9 us  [the longest x6 34.5 us: turned(): lax.ppermute(array, 'tp', [(i, (i + 2 * steps) % tp_count) for i in range...]
    dot_general x15 -> x0, matrix products: 67.9 us -> none  [the longest x6 23.2 us: block_step(): jnp.einsum('qhcd,khcd->chqk', split_queries, key_block, preferred_element...]
    pallas_call x0 -> x6, Pallas kernels: none -> 66.1 us  [the longest x4 32.4 us: expert_pass(): pl.pallas_call(functools.partial(expert_kernel, blocks=len(blocks), exper...]
    ppermute x0 -> x41, starting transfers between devices: none -> 41.5 us  [the longest x6 10.2 us: turned(): lax.ppermute(array, 'tp', [(i, (i + 2 * steps) % tp_count) for i in range...]
    convert_element_type x9 -> x12, other arithmetic: 26.7 us -> 2.03 us  [the longest x1 1.2 us: balanced(): return total.astype(jnp.bfloat16)]
    all_to_all x1 -> x0, blocking collectives: 17.2 us -> none  [shards(): lax.all_to_all(outgoing.reshape(sp_count, local_experts, capacity, model_...]
  transfers between devices with their start and end apart: 6 -> 43, of which waited for: 6 -> 21; matrix products, arithmetic and copies ran while one was open for 1% -> 1% of each run, Pallas kernels for 0% -> 25%
where the time goes in v1:
time: 263 us; the launch traced here: 262 us
  waiting for transfers between devices  127 us (48%)
  Pallas kernels  66.1 us (25%)
  starting transfers between devices  51.8 us (20%)
  local copies, waits for them, and re-layouts  12.8 us (5%)
  other arithmetic  3.84 us (1%)
    ppermute x6, waiting for transfers between devices, turned(): lax.ppermute(array, 'tp', [(i, (i + 2 * steps) % tp_count) for i in range...  34.5 us
    pallas_call x4, Pallas kernels, expert_pass(): pl.pallas_call(functools.partial(expert_kernel, blocks=len(blocks), exper...  32.4 us
    pallas_call x1, Pallas kernels, attention(): pl.pallas_call(functools.partial(attention_kernel, sub=sub, key_rows=key_...  30.3 us
    all_to_all x1, waiting for transfers between devices, balanced(): lax.all_to_all(jnp.concatenate([split, keys, values], axis=1), 'sp', spli...  22.3 us
    ppermute x4, waiting for transfers between devices, balanced(): by_x = lax.ppermute(block, 'sp', across_x)  13.8 us
    ppermute x4, waiting for transfers between devices, balanced(): from_y = lax.ppermute(to_y, 'sp', across_y)  13.5 us
    all_to_all x1, waiting for transfers between devices, balanced(): lax.all_to_all(attended.reshape(sp_count * tp_count, sub, width), ('sp',...  12.9 us
    ppermute x4, waiting for transfers between devices, balanced(): by_y = lax.ppermute(block, 'sp', across_y)  10.9 us
  transfers between devices with their start and end apart: 43, of which 21 were waited for; matrix products, arithmetic and copies ran while one was open for 1% of the time, Pallas kernels for 25%

profile of v1, /device:TPU:0, one launch (start us, length us, event | category | flops | bytes accessed | tf_op | source)
XLA Modules:
  0.0 262.1 jit_solution(9970099618193405793)
XLA Ops:
  0.0 1.0 copy.26
  1.1 1.1 copy.25
  2.1 1.1 copy.24
  3.4 1.5 pad_maximum_fusion
  4.9 5.3 %all-to-all-start = ((bf16[4,1920,128]{2,1,0:T(8,128)(2,1)}), bf16[4,1920,128]{2,1,0:T(8,128)(2,1)S(1)}, u32[]{:S(2)}, u32[]{:S(2)}) async-start(bf16[4,1920,128]{2,1,0:T(8,128)(2,1)} %pad_maximum_fusion), calls=%async_computation | async-start | bytes 3932160 | tf_op jit(solution)/shard_map/all_to_all | solution.py:291
  11.3 22.3 %all-to-all-done.rows_ref = bf16[4,1920,128]{2,1,0:T(8,128)(2,1)S(1)} async-done(((bf16[4,1920,128]{2,1,0:T(8,128)(2,1)}), bf16[4,1920,128]{2,1,0:T(8,128)(2,1)S(1)}, u32[]{:S(2)}, u32[]{:S(2)}) %all-to-all-start) | async-done | bytes 1966112 | tf_op jit(solution)/shard_map/all_to_all | solution.py:291
  33.7 30.3 %attention.1 = bf16[1536,128]{1,0:T(8,128)(2,1)} custom-call(s32[1]{0:T(128)} %bitcast.part_ref, f32[1]{0:T(128)} %dynamic_slice.3.lam_ref, f32[1,128]{1,0:T(1,128)S(1)} %bitcast.16, bf16[4,1920,128]{2,1,0:T(8,128)(2,1)S(1)} %all-to-all-done.rows_ref), custom_call_target="tpu_custom_call" | custom-call | flops 4831838208 | bytes 1966080 | tf_op jit(solution)/shard_map/attention/pallas_call | solution.py:94
  63.9 5.0 %all-to-all-start.1 = ((bf16[32,48,128]{2,1,0:T(8,128)(2,1)}), bf16[32,48,128]{2,1,0:T(8,128)(2,1)S(1)}, u32[]{:S(2)}, u32[]{:S(2)}) async-start(bf16[32,48,128]{2,1,0:T(8,128)(2,1)} %bitcast.9), calls=%async_computation.1 | async-start | bytes 786432 | tf_op jit(solution)/shard_map/all_to_all | solution.py:304
  69.5 12.9 %all-to-all-done.1 = bf16[32,48,128]{2,1,0:T(8,128)(2,1)S(1)} async-done(((bf16[32,48,128]{2,1,0:T(8,128)(2,1)}), bf16[32,48,128]{2,1,0:T(8,128)(2,1)S(1)}, u32[]{:S(2)}, u32[]{:S(2)}) %all-to-all-start.1) | async-done | bytes 393248 | tf_op jit(solution)/shard_map/all_to_all | solution.py:304
  82.4 3.4 %copy-done = bf16[2048,2048]{1,0:T(8,128)(2,1)S(1)} copy-done((bf16[2048,2048]{1,0:T(8,128)(2,1)S(1)}, bf16[2048,2048]{1,0:T(8,128)(2,1)}, u32[]{:S(2)}) %copy-start) | copy-done | bytes 8388632
  85.8 3.5 %project.1 = (bf16[96,2048]{1,0:T(8,128)(2,1)S(1)}, bf16[96,2176]{1,0:T(8,128)(2,1)S(1)}) custom-call(bf16[4,8,48,128]{3,2,1,0:T(8,128)(2,1)S(1)} %bitcast.14, bf16[2048,2048]{1,0:T(8,128)(2,1)S(1)} %copy-done, bf16[96,2048]{1,0:T(8,128)(2,1)S(1)} %copy-done.1, f32[1,2048]{1,0:T(1,128)S(1)} %bitcast.15, bf16[96,128]{1,0:T(8,128)(2,1)S(1)} %maximum_maximum_fusion.routes_ref), custom_call_target="tpu_custom_call" | custom-call | flops 805306368 | bytes 8388608 | tf_op jit(solution)/shard_map/project/pallas_call | solution.py:154
  89.3 1.1 collective-permute-start.1
  90.4 10.6 %collective-permute-done.refs_2_ = bf16[96,2176]{1,0:T(8,128)(2,1)S(1)} collective-permute-done((bf16[96,2176]{1,0:T(8,128)(2,1)S(1)}, bf16[96,2176]{1,0:T(8,128)(2,1)S(1)}, u32[]{:S(2)}, u32[]{:S(2)}) %collective-permute-start) | collective-permute-done | bytes 417824 | tf_op jit(solution)/shard_map/ppermute | solution.py:343
  101.0 0.9 collective-permute-start.2
  101.9 0.9 collective-permute-start.3
  102.9 1.5 collective-permute-start.21
  104.3 3.1 %collective-permute-done.2.refs_4_ = bf16[48,2176]{1,0:T(8,128)(2,1)S(1)} collective-permute-done((bf16[48,2176]{1,0:T(8,128)(2,1)S(1)}, bf16[48,2176]{1,0:T(8,128)(2,1)S(1)}, u32[]{:S(2)}, u32[]{:S(2)}) %collective-permute-start.2) | collective-permute-done | bytes 208928 | tf_op jit(solution)/shard_map/ppermute | solution.py:345
  107.4 1.0 collective-permute-done.3.refs_5_
  108.4 1.6 copy-done.3
  110.0 1.6 copy-done.5
  111.6 1.6 copy-done.7
  113.2 8.2 %experts.4 = (bf16[96,2048]{1,0:T(8,128)(2,1)S(1)}, bf16[96,2048]{1,0:T(8,128)(2,1)S(1)}, bf16[96,2048]{1,0:T(8,128)(2,1)S(1)}, bf16[48,2048]{1,0:T(8,128)(2,1)S(1)}, bf16[48,2048]{1,0:T(8,128)(2,1)S(1)}) custom-call(s32[1]{0:T(128)} %bitcast.12.refs_0_, bf16[96,2176]{1,0:T(8,128)(2,1)S(1)} %get-tuple-element.28.refs_1_, ...), custom_call_target="tpu_custom_call" | custom-call | flops 4831838208 | bytes 12582912 | tf_op jit(solution)/shard_map/experts/pallas_call | solution.py:234
  121.4 0.8 collective-permute-start.9
  122.2 1.7 collective-permute-start.11
  124.4 1.5 collective-permute-start.33
  125.9 7.3 %collective-permute-done.21.refs_1_ = bf16[96,2176]{1,0:T(8,128)(2,1)S(1)} collective-permute-done((bf16[96,2176]{1,0:T(8,128)(2,1)S(1)}, bf16[96,2176]{1,0:T(8,128)(2,1)S(1)}, u32[]{:S(2)}, u32[]{:S(2)}) %collective-permute-start.21) | collective-permute-done | bytes 417824 | tf_op jit(solution)/shard_map/ppermute | solution.py:332
  133.2 1.3 collective-permute-start.22
  134.5 0.9 collective-permute-start.7
  135.5 5.2 %collective-permute-done.11.refs_1_ = bf16[96,2176]{1,0:T(8,128)(2,1)S(1)} collective-permute-done((bf16[96,2176]{1,0:T(8,128)(2,1)S(1)}, bf16[96,2176]{1,0:T(8,128)(2,1)S(1)}, u32[]{:S(2)}, u32[]{:S(2)}) %collective-permute-start.11) | collective-permute-done | bytes 417824 | tf_op jit(solution)/shard_map/ppermute | solution.py:332
  140.6 1.3 collective-permute-start.23
  141.9 0.8 collective-permute-start.12
  143.5 1.5 collective-permute-start.34
  145.0 1.8 collective-permute-done.22.refs_2_
  147.7 5.5 %collective-permute-done.23.refs_3_ = bf16[96,2176]{1,0:T(8,128)(2,1)S(1)} collective-permute-done((bf16[96,2176]{1,0:T(8,128)(2,1)S(1)}, bf16[96,2176]{1,0:T(8,128)(2,1)S(1)}, u32[]{:S(2)}, u32[]{:S(2)}) %collective-permute-start.23) | collective-permute-done | bytes 417824 | tf_op jit(solution)/shard_map/ppermute | solution.py:344
  153.1 1.3 collective-permute-start.10
  154.4 1.4 collective-permute-done.12.refs_2_
  156.6 5.5 %collective-permute-done.13.refs_3_ = bf16[96,2176]{1,0:T(8,128)(2,1)S(1)} collective-permute-done((bf16[96,2176]{1,0:T(8,128)(2,1)S(1)}, bf16[96,2176]{1,0:T(8,128)(2,1)S(1)}, u32[]{:S(2)}, u32[]{:S(2)}) %collective-permute-start.13) | collective-permute-done | bytes 417824 | tf_op jit(solution)/shard_map/ppermute | solution.py:344
  162.1 1.3 collective-permute-start.24
  163.4 3.2 %collective-permute-done.34.refs_4_ = bf16[48,2176]{1,0:T(8,128)(2,1)S(1)} collective-permute-done((bf16[48,2176]{1,0:T(8,128)(2,1)S(1)}, bf16[48,2176]{1,0:T(8,128)(2,1)S(1)}, u32[]{:S(2)}, u32[]{:S(2)}) %collective-permute-start.34) | collective-permute-done | bytes 208928 | tf_op jit(solution)/shard_map/ppermute | solution.py:345
  167.2 1.5 collective-permute-start.14
  168.7 8.1 %experts.7 = (bf16[96,2048]{1,0:T(8,128)(2,1)S(1)}, bf16[96,2048]{1,0:T(8,128)(2,1)S(1)}, bf16[96,2048]{1,0:T(8,128)(2,1)S(1)}, bf16[48,2048]{1,0:T(8,128)(2,1)S(1)}, bf16[48,2048]{1,0:T(8,128)(2,1)S(1)}) custom-call(s32[1]{0:T(128)} %bitcast.12.refs_0_, bf16[96,2176]{1,0:T(8,128)(2,1)S(1)} %collective-permute-done.31.refs_1_, ...), custom_call_target="tpu_custom_call" | custom-call | flops 4831838208 | bytes 12582912 | tf_op jit(solution)/shard_map/experts/pallas_call | solution.py:234
  176.7 2.7 %collective-permute-done.24.refs_4_ = bf16[48,2176]{1,0:T(8,128)(2,1)S(1)} collective-permute-done((bf16[48,2176]{1,0:T(8,128)(2,1)S(1)}, bf16[48,2176]{1,0:T(8,128)(2,1)S(1)}, u32[]{:S(2)}, u32[]{:S(2)}) %collective-permute-start.24) | collective-permute-done | bytes 208928 | tf_op jit(solution)/shard_map/ppermute | solution.py:345
  180.1 1.4 collective-permute-start.38
  181.5 8.1 %experts.6 = (bf16[96,2048]{1,0:T(8,128)(2,1)S(1)}, bf16[96,2048]{1,0:T(8,128)(2,1)S(1)}, bf16[96,2048]{1,0:T(8,128)(2,1)S(1)}, bf16[48,2048]{1,0:T(8,128)(2,1)S(1)}, bf16[48,2048]{1,0:T(8,128)(2,1)S(1)}) custom-call(s32[1]{0:T(128)} %bitcast.12.refs_0_, bf16[96,2176]{1,0:T(8,128)(2,1)S(1)} %collective-permute-done.21.refs_1_, ...), custom_call_target="tpu_custom_call" | custom-call | flops 4831838208 | bytes 12582912 | tf_op jit(solution)/shard_map/experts/pallas_call | solution.py:234
  189.6 1.3 collective-permute-start.36
  190.9 0.8 collective-permute-start.28
  191.7 8.1 %experts.5 = (bf16[96,2048]{1,0:T(8,128)(2,1)S(1)}, bf16[96,2048]{1,0:T(8,128)(2,1)S(1)}, bf16[96,2048]{1,0:T(8,128)(2,1)S(1)}, bf16[48,2048]{1,0:T(8,128)(2,1)S(1)}, bf16[48,2048]{1,0:T(8,128)(2,1)S(1)}) custom-call(s32[1]{0:T(128)} %bitcast.12.refs_0_, bf16[96,2176]{1,0:T(8,128)(2,1)S(1)} %collective-permute-done.11.refs_1_, ...), custom_call_target="tpu_custom_call" | custom-call | flops 4831838208 | bytes 12582912 | tf_op jit(solution)/shard_map/experts/pallas_call | solution.py:234
  200.6 1.5 collective-permute-start.18
  202.2 1.3 collective-permute-start.16
  203.6 4.2 %collective-permute-done.26 = bf16[48,2048]{1,0:T(8,128)(2,1)S(1)} collective-permute-done((bf16[48,2048]{1,0:T(8,128)(2,1)S(1)}, bf16[48,2048]{1,0:T(8,128)(2,1)S(1)}, u32[]{:S(2)}, u32[]{:S(2)}) %collective-permute-start.26) | collective-permute-done | bytes 196640 | tf_op jit(solution)/shard_map/ppermute | solution.py:350
  208.4 1.4 collective-permute-start.37
  210.0 2.0 collective-permute-done.16
  212.7 7.8 %collective-permute-done.39 = bf16[96,2048]{1,0:T(8,128)(2,1)S(1)} collective-permute-done((bf16[96,2048]{1,0:T(8,128)(2,1)S(1)}, bf16[96,2048]{1,0:T(8,128)(2,1)S(1)}, u32[]{:S(2)}, u32[]{:S(2)}) %collective-permute-start.39) | collective-permute-done | bytes 393248 | tf_op jit(solution)/shard_map/ppermute | solution.py:359
  220.4 1.2 collective-permute-start.27
  221.6 0.8 collective-permute-start.19
  222.5 5.8 %collective-permute-done.29 = bf16[96,2048]{1,0:T(8,128)(2,1)S(1)} collective-permute-done((bf16[96,2048]{1,0:T(8,128)(2,1)S(1)}, bf16[96,2048]{1,0:T(8,128)(2,1)S(1)}, u32[]{:S(2)}, u32[]{:S(2)}) %collective-permute-start.29) | collective-permute-done | bytes 393248 | tf_op jit(solution)/shard_map/ppermute | solution.py:359
  228.6 1.9 collective-permute-done.27
  230.5 2.6 collective-permute-start.40
  233.2 1.9 collective-permute-start.30
  235.1 1.0 collective-permute-done.17
  236.2 2.6 collective-permute-start.20
  238.8 3.8 %collective-permute-done.40 = bf16[96,2048]{1,0:T(8,128)(2,1)S(1)} collective-permute-done((bf16[96,2048]{1,0:T(8,128)(2,1)S(1)}, bf16[96,2048]{1,0:T(8,128)(2,1)S(1)}, u32[]{:S(2)}, u32[]{:S(2)}) %collective-permute-start.40) | collective-permute-done | bytes 393248 | tf_op jit(solution)/shard_map/ppermute | solution.py:332
  242.6 18.3 %collective-permute-done.30 = bf16[96,2048]{1,0:T(8,128)(2,1)S(1)} collective-permute-done((bf16[96,2048]{1,0:T(8,128)(2,1)S(1)}, bf16[96,2048]{1,0:T(8,128)(2,1)S(1)}, u32[]{:S(2)}, u32[]{:S(2)}) %collective-permute-start.30) | collective-permute-done | bytes 393248 | tf_op jit(solution)/shard_map/ppermute | solution.py:332
  260.9 1.2 add_convert_fusion
  (106 shorter events, 9.3 us)
Async XLA Ops:
  4.9 5.8 %copy-start.12 = (f32[2]{0:T(128)S(1)}, f32[2]{0:T(128)}, u32[]{:S(2)}) copy-start(f32[2]{0:T(128)} %param.16) | copy-start | bytes 28
  4.9 28.8 %copy-start.9 = (f32[128]{0:T(128)S(1)}, f32[128]{0:T(128)}, u32[]{:S(2)}) copy-start(f32[128]{0:T(128)} %param.17) | copy-start | bytes 1540
  4.9 28.8 %all-to-all-start = ((bf16[4,1920,128]{2,1,0:T(8,128)(2,1)}), bf16[4,1920,128]{2,1,0:T(8,128)(2,1)S(1)}, u32[]{:S(2)}, u32[]{:S(2)}) async-start(bf16[4,1920,128]{2,1,0:T(8,128)(2,1)} %pad_maximum_fusion), calls=%async_computation | async-start | bytes 3932160 | tf_op jit(solution)/shard_map/all_to_all | solution.py:291
  10.2 92.6 %collective-permute-start.4 = (bf16[2,2048,256]{2,1,0:T(8,128)(2,1)}, bf16[2,2048,256]{2,1,0:T(8,128)(2,1)}, u32[]{:S(2)}, u32[]{:S(2)}) collective-permute-start(bf16[2,2048,256]{2,1,0:T(8,128)(2,1)} %refs_6_.7), channel_id=1, source_target_pairs={{0,1},{1,0},{2,3},{3,2},{4,5},{5,4},{6,7},{7,6},{8,9},{9,8},{10,11... | collective-permute-start | bytes 6291464 | tf_op jit(solution)/shard_map/ppermute | solution.py:284
  10.2 92.7 %collective-permute-start.5 = (bf16[2,2048,256]{2,1,0:T(8,128)(2,1)}, bf16[2,2048,256]{2,1,0:T(8,128)(2,1)}, u32[]{:S(2)}, u32[]{:S(2)}) collective-permute-start(bf16[2,2048,256]{2,1,0:T(8,128)(2,1)} %refs_7_.7), channel_id=1, source_target_pairs={{0,1},{1,0},{2,3},{3,2},{4,5},{5,4},{6,7},{7,6},{8,9},{9,8},{10,11... | collective-permute-start | bytes 6291464 | tf_op jit(solution)/shard_map/ppermute | solution.py:284
  10.7 93.6 %collective-permute-start.6 = (bf16[2,256,2048]{2,1,0:T(8,128)(2,1)}, bf16[2,256,2048]{2,1,0:T(8,128)(2,1)}, u32[]{:S(2)}, u32[]{:S(2)}) collective-permute-start(bf16[2,256,2048]{2,1,0:T(8,128)(2,1)} %refs_8_.7), channel_id=1, source_target_pairs={{0,1},{1,0},{2,3},{3,2},{4,5},{5,4},{6,7},{7,6},{8,9},{9,8},{10,11... | collective-permute-start | bytes 6291464 | tf_op jit(solution)/shard_map/ppermute | solution.py:284
  33.7 35.3 %copy-start.10 = (f32[96,2]{0,1:T(2,128)S(1)}, f32[96,2]{0,1:T(2,128)}, u32[]{:S(2)}) copy-start(f32[96,2]{0,1:T(2,128)} %param.22) | copy-start | bytes 2308
  33.7 35.3 %copy-start.11 = (s32[96,2]{0,1:T(2,128)S(1)}, s32[96,2]{0,1:T(2,128)}, u32[]{:S(2)}) copy-start(s32[96,2]{0,1:T(2,128)} %param.21) | copy-start | bytes 2308
  33.7 48.7 %copy-start.1 = (bf16[96,2048]{1,0:T(8,128)(2,1)S(1)}, bf16[96,2048]{1,0:T(8,128)(2,1)}, u32[]{:S(2)}) copy-start(bf16[96,2048]{1,0:T(8,128)(2,1)} %residual_ref.1) | copy-start | bytes 1179652
  33.7 48.7 %copy-start.2 = (f32[2048]{0:T(1024)S(1)}, f32[2048]{0:T(1024)}, u32[]{:S(2)}) copy-start(f32[2048]{0:T(1024)} %param.20) | copy-start | bytes 24580
  63.9 18.4 %all-to-all-start.1 = ((bf16[32,48,128]{2,1,0:T(8,128)(2,1)}), bf16[32,48,128]{2,1,0:T(8,128)(2,1)S(1)}, u32[]{:S(2)}, u32[]{:S(2)}) async-start(bf16[32,48,128]{2,1,0:T(8,128)(2,1)} %bitcast.9), calls=%async_computation.1 | async-start | bytes 786432 | tf_op jit(solution)/shard_map/all_to_all | solution.py:304
  82.4 3.4 %copy-start = (bf16[2048,2048]{1,0:T(8,128)(2,1)S(1)}, bf16[2048,2048]{1,0:T(8,128)(2,1)}, u32[]{:S(2)}) copy-start(bf16[2048,2048]{1,0:T(8,128)(2,1)} %weight_ref.1) | copy-start | bytes 25165828
  89.2 11.7 %collective-permute-start = (bf16[96,2176]{1,0:T(8,128)(2,1)S(1)}, bf16[96,2176]{1,0:T(8,128)(2,1)S(1)}, u32[]{:S(2)}, u32[]{:S(2)}) collective-permute-start(bf16[96,2176]{1,0:T(8,128)(2,1)S(1)} %get-tuple-element.28.refs_1_), channel_id=1, source_target_pairs={{0,8},{8,0},{16,24},{24,16},{1,9},{9,1},{17,25},{25,17},{2,10},{10... | collective-permute-start | bytes 1253384 | tf_op jit(solution)/shard_map/ppermute | solution.py:343
  89.3 12.6 %collective-permute-start.1 = (bf16[96,2176]{1,0:T(8,128)(2,1)S(1)}, bf16[96,2176]{1,0:T(8,128)(2,1)S(1)}, u32[]{:S(2)}, u32[]{:S(2)}) collective-permute-start(bf16[96,2176]{1,0:T(8,128)(2,1)S(1)} %get-tuple-element.28.refs_1_), channel_id=1, source_target_pairs={{0,16},{8,24},{16,0},{24,8},{1,17},{9,25},{17,1},{25,9},{2,18},{10... | collective-permute-start | bytes 1253384 | tf_op jit(solution)/shard_map/ppermute | solution.py:344
  101.0 6.4 %collective-permute-start.2 = (bf16[48,2176]{1,0:T(8,128)(2,1)S(1)}, bf16[48,2176]{1,0:T(8,128)(2,1)S(1)}, u32[]{:S(2)}, u32[]{:S(2)}) collective-permute-start(bf16[48,2176]{1,0:T(8,128)(2,1)S(1)} %slice.96), channel_id=1, source_target_pairs={{0,16},{8,24},{16,0},{24,8},{1,17},{9,25},{17,1},{25,9},{2,18},{10... | collective-permute-start | bytes 626696 | tf_op jit(solution)/shard_map/ppermute | solution.py:345
  101.9 6.5 %collective-permute-start.3 = (bf16[48,2176]{1,0:T(8,128)(2,1)S(1)}, bf16[48,2176]{1,0:T(8,128)(2,1)S(1)}, u32[]{:S(2)}, u32[]{:S(2)}) collective-permute-start(bf16[48,2176]{1,0:T(8,128)(2,1)S(1)} %slice.97), channel_id=1, source_target_pairs={{0,8},{8,0},{16,24},{24,16},{1,9},{9,1},{17,25},{25,17},{2,10},{10... | collective-permute-start | bytes 626696 | tf_op jit(solution)/shard_map/ppermute | solution.py:346
  102.8 21.1 %collective-permute-start.31 = (bf16[96,2176]{1,0:T(8,128)(2,1)S(1)}, bf16[96,2176]{1,0:T(8,128)(2,1)S(1)}, u32[]{:S(2)}, u32[]{:S(2)}) collective-permute-start(bf16[96,2176]{1,0:T(8,128)(2,1)S(1)} %get-tuple-element.28.refs_1_), channel_id=1, source_target_pairs={{0,2},{1,3},{2,4},{3,5},{4,6},{5,7},{6,0},{7,1},{8,10},{9,11},{10,... | collective-permute-start | bytes 1253384 | tf_op jit(solution)/shard_map/ppermute | solution.py:332
  102.9 30.4 %collective-permute-start.21 = (bf16[96,2176]{1,0:T(8,128)(2,1)S(1)}, bf16[96,2176]{1,0:T(8,128)(2,1)S(1)}, u32[]{:S(2)}, u32[]{:S(2)}) collective-permute-start(bf16[96,2176]{1,0:T(8,128)(2,1)S(1)} %get-tuple-element.28.refs_1_), channel_id=1, source_target_pairs={{0,4},{1,5},{2,6},{3,7},{4,0},{5,1},{6,2},{7,3},{8,12},{9,13},{10,... | collective-permute-start | bytes 1253384 | tf_op jit(solution)/shard_map/ppermute | solution.py:332
  108.4 1.6 copy-start.3
  110.0 1.6 copy-start.5
  111.6 1.6 copy-start.7
  113.2 55.5 %copy-start.8 = (bf16[2,256,2048]{2,1,0:T(8,128)(2,1)S(1)}, bf16[2,256,2048]{2,1,0:T(8,128)(2,1)}, u32[]{:S(2)}) copy-start(bf16[2,256,2048]{2,1,0:T(8,128)(2,1)} %refs_8_.7) | copy-start | bytes 6291460
  121.4 13.2 %collective-permute-start.9 = (bf16[48,2048]{1,0:T(8,128)(2,1)S(1)}, bf16[48,2048]{1,0:T(8,128)(2,1)S(1)}, u32[]{:S(2)}, u32[]{:S(2)}) collective-permute-start(bf16[48,2048]{1,0:T(8,128)(2,1)S(1)} %get-tuple-element.33), channel_id=1, source_target_pairs={{0,8},{8,0},{16,24},{24,16},{1,9},{9,1},{17,25},{25,17},{2,10},{10... | collective-permute-start | bytes 589832 | tf_op jit(solution)/shard_map/ppermute | solution.py:351
  122.2 18.4 %collective-permute-start.11 = (bf16[96,2176]{1,0:T(8,128)(2,1)S(1)}, bf16[96,2176]{1,0:T(8,128)(2,1)S(1)}, u32[]{:S(2)}, u32[]{:S(2)}) collective-permute-start(bf16[96,2176]{1,0:T(8,128)(2,1)S(1)} %get-tuple-element.28.refs_1_), channel_id=1, source_target_pairs={{0,6},{1,7},{2,0},{3,1},{4,2},{5,3},{6,4},{7,5},{8,14},{9,15},{10,... | collective-permute-start | bytes 1253384 | tf_op jit(solution)/shard_map/ppermute | solution.py:332
  123.9 18.9 %collective-permute-start.32 = (bf16[96,2176]{1,0:T(8,128)(2,1)S(1)}, bf16[96,2176]{1,0:T(8,128)(2,1)S(1)}, u32[]{:S(2)}, u32[]{:S(2)}) collective-permute-start(bf16[96,2176]{1,0:T(8,128)(2,1)S(1)} %collective-permute-done.31.refs_1_), channel_id=1, source_target_pairs={{0,8},{8,0},{16,24},{24,16},{1,9},{9,1},{17,25},{25,17},{2,10},{10... | collective-permute-start | bytes 1253384 | tf_op jit(solution)/shard_map/ppermute | solution.py:343
  124.4 19.1 %collective-permute-start.33 = (bf16[96,2176]{1,0:T(8,128)(2,1)S(1)}, bf16[96,2176]{1,0:T(8,128)(2,1)S(1)}, u32[]{:S(2)}, u32[]{:S(2)}) collective-permute-start(bf16[96,2176]{1,0:T(8,128)(2,1)S(1)} %collective-permute-done.31.refs_1_), channel_id=1, source_target_pairs={{0,16},{8,24},{16,0},{24,8},{1,17},{9,25},{17,1},{25,9},{2,18},{10... | collective-permute-start | bytes 1253384 | tf_op jit(solution)/shard_map/ppermute | solution.py:344
  133.2 13.7 %collective-permute-start.22 = (bf16[96,2176]{1,0:T(8,128)(2,1)S(1)}, bf16[96,2176]{1,0:T(8,128)(2,1)S(1)}, u32[]{:S(2)}, u32[]{:S(2)}) collective-permute-start(bf16[96,2176]{1,0:T(8,128)(2,1)S(1)} %collective-permute-done.21.refs_1_), channel_id=1, source_target_pairs={{0,8},{8,0},{16,24},{24,16},{1,9},{9,1},{17,25},{25,17},{2,10},{10... | collective-permute-start | bytes 1253384 | tf_op jit(solution)/shard_map/ppermute | solution.py:343
  134.5 7.3 %collective-permute-start.7 = (bf16[48,2048]{1,0:T(8,128)(2,1)S(1)}, bf16[48,2048]{1,0:T(8,128)(2,1)S(1)}, u32[]{:S(2)}, u32[]{:S(2)}) collective-permute-start(bf16[48,2048]{1,0:T(8,128)(2,1)S(1)} %get-tuple-element.31), channel_id=1, source_target_pairs={{0,16},{8,24},{16,0},{24,8},{1,17},{9,25},{17,1},{25,9},{2,18},{10... | collective-permute-start | bytes 589832 | tf_op jit(solution)/shard_map/ppermute | solution.py:350
  140.6 12.5 %collective-permute-start.23 = (bf16[96,2176]{1,0:T(8,128)(2,1)S(1)}, bf16[96,2176]{1,0:T(8,128)(2,1)S(1)}, u32[]{:S(2)}, u32[]{:S(2)}) collective-permute-start(bf16[96,2176]{1,0:T(8,128)(2,1)S(1)} %collective-permute-done.21.refs_1_), channel_id=1, source_target_pairs={{0,16},{8,24},{16,0},{24,8},{1,17},{9,25},{17,1},{25,9},{2,18},{10... | collective-permute-start | bytes 1253384 | tf_op jit(solution)/shard_map/ppermute | solution.py:344
  141.9 13.9 %collective-permute-start.12 = (bf16[96,2176]{1,0:T(8,128)(2,1)S(1)}, bf16[96,2176]{1,0:T(8,128)(2,1)S(1)}, u32[]{:S(2)}, u32[]{:S(2)}) collective-permute-start(bf16[96,2176]{1,0:T(8,128)(2,1)S(1)} %collective-permute-done.11.refs_1_), channel_id=1, source_target_pairs={{0,8},{8,0},{16,24},{24,16},{1,9},{9,1},{17,25},{25,17},{2,10},{10... | collective-permute-start | bytes 1253384 | tf_op jit(solution)/shard_map/ppermute | solution.py:343
  142.7 25.9 %copy-start.6 = (bf16[2,2048,256]{2,1,0:T(8,128)(2,1)S(1)}, bf16[2,2048,256]{2,1,0:T(8,128)(2,1)}, u32[]{:S(2)}) copy-start(bf16[2,2048,256]{2,1,0:T(8,128)(2,1)} %refs_7_.7) | copy-start | bytes 6291460
  142.8 25.9 %copy-start.4 = (bf16[2,2048,256]{2,1,0:T(8,128)(2,1)S(1)}, bf16[2,2048,256]{2,1,0:T(8,128)(2,1)}, u32[]{:S(2)}) copy-start(bf16[2,2048,256]{2,1,0:T(8,128)(2,1)} %refs_6_.7) | copy-start | bytes 6291460
  142.8 19.3 %collective-permute-start.13 = (bf16[96,2176]{1,0:T(8,128)(2,1)S(1)}, bf16[96,2176]{1,0:T(8,128)(2,1)S(1)}, u32[]{:S(2)}, u32[]{:S(2)}) collective-permute-start(bf16[96,2176]{1,0:T(8,128)(2,1)S(1)} %collective-permute-done.11.refs_1_), channel_id=1, source_target_pairs={{0,16},{8,24},{16,0},{24,8},{1,17},{9,25},{17,1},{25,9},{2,18},{10... | collective-permute-start | bytes 1253384 | tf_op jit(solution)/shard_map/ppermute | solution.py:344
  143.5 23.1 %collective-permute-start.34 = (bf16[48,2176]{1,0:T(8,128)(2,1)S(1)}, bf16[48,2176]{1,0:T(8,128)(2,1)S(1)}, u32[]{:S(2)}, u32[]{:S(2)}) collective-permute-start(bf16[48,2176]{1,0:T(8,128)(2,1)S(1)} %slice.102), channel_id=1, source_target_pairs={{0,16},{8,24},{16,0},{24,8},{1,17},{9,25},{17,1},{25,9},{2,18},{10... | collective-permute-start | bytes 626696 | tf_op jit(solution)/shard_map/ppermute | solution.py:345
  146.9 20.3 %collective-permute-start.35 = (bf16[48,2176]{1,0:T(8,128)(2,1)S(1)}, bf16[48,2176]{1,0:T(8,128)(2,1)S(1)}, u32[]{:S(2)}, u32[]{:S(2)}) collective-permute-start(bf16[48,2176]{1,0:T(8,128)(2,1)S(1)} %slice.103), channel_id=1, source_target_pairs={{0,8},{8,0},{16,24},{24,16},{1,9},{9,1},{17,25},{25,17},{2,10},{10... | collective-permute-start | bytes 626696 | tf_op jit(solution)/shard_map/ppermute | solution.py:346
  153.1 85.7 %collective-permute-start.10 = (bf16[96,2048]{1,0:T(8,128)(2,1)S(1)}, bf16[96,2048]{1,0:T(8,128)(2,1)S(1)}, u32[]{:S(2)}, u32[]{:S(2)}) collective-permute-start(bf16[96,2048]{1,0:T(8,128)(2,1)S(1)} %pad_maximum_fusion.2), channel_id=1, source_target_pairs={{0,16},{8,24},{16,0},{24,8},{1,17},{9,25},{17,1},{25,9},{2,18},{10... | collective-permute-start | bytes 1179656 | tf_op jit(solution)/shard_map/ppermute | solution.py:359
  155.8 83.0 %collective-permute-start.8 = (bf16[96,2048]{1,0:T(8,128)(2,1)S(1)}, bf16[96,2048]{1,0:T(8,128)(2,1)S(1)}, u32[]{:S(2)}, u32[]{:S(2)}) collective-permute-start(bf16[96,2048]{1,0:T(8,128)(2,1)S(1)} %pad_maximum_fusion.1), channel_id=1, source_target_pairs={{0,8},{8,0},{16,24},{24,16},{1,9},{9,1},{17,25},{25,17},{2,10},{10... | collective-permute-start | bytes 1179656 | tf_op jit(solution)/shard_map/ppermute | solution.py:358
  162.1 17.4 %collective-permute-start.24 = (bf16[48,2176]{1,0:T(8,128)(2,1)S(1)}, bf16[48,2176]{1,0:T(8,128)(2,1)S(1)}, u32[]{:S(2)}, u32[]{:S(2)}) collective-permute-start(bf16[48,2176]{1,0:T(8,128)(2,1)S(1)} %slice.100), channel_id=1, source_target_pairs={{0,16},{8,24},{16,0},{24,8},{1,17},{9,25},{17,1},{25,9},{2,18},{10... | collective-permute-start | bytes 626696 | tf_op jit(solution)/shard_map/ppermute | solution.py:345
  166.6 13.5 %collective-permute-start.25 = (bf16[48,2176]{1,0:T(8,128)(2,1)S(1)}, bf16[48,2176]{1,0:T(8,128)(2,1)S(1)}, u32[]{:S(2)}, u32[]{:S(2)}) collective-permute-start(bf16[48,2176]{1,0:T(8,128)(2,1)S(1)} %slice.101), channel_id=1, source_target_pairs={{0,8},{8,0},{16,24},{24,16},{1,9},{9,1},{17,25},{25,17},{2,10},{10... | collective-permute-start | bytes 626696 | tf_op jit(solution)/shard_map/ppermute | solution.py:346
  167.2 22.4 %collective-permute-start.14 = (bf16[48,2176]{1,0:T(8,128)(2,1)S(1)}, bf16[48,2176]{1,0:T(8,128)(2,1)S(1)}, u32[]{:S(2)}, u32[]{:S(2)}) collective-permute-start(bf16[48,2176]{1,0:T(8,128)(2,1)S(1)} %slice.98), channel_id=1, source_target_pairs={{0,16},{8,24},{16,0},{24,8},{1,17},{9,25},{17,1},{25,9},{2,18},{10... | collective-permute-start | bytes 626696 | tf_op jit(solution)/shard_map/ppermute | solution.py:345
  179.5 11.4 %collective-permute-start.15 = (bf16[48,2176]{1,0:T(8,128)(2,1)S(1)}, bf16[48,2176]{1,0:T(8,128)(2,1)S(1)}, u32[]{:S(2)}, u32[]{:S(2)}) collective-permute-start(bf16[48,2176]{1,0:T(8,128)(2,1)S(1)} %slice.99), channel_id=1, source_target_pairs={{0,8},{8,0},{16,24},{24,16},{1,9},{9,1},{17,25},{25,17},{2,10},{10... | collective-permute-start | bytes 626696 | tf_op jit(solution)/shard_map/ppermute | solution.py:346
  180.1 19.8 %collective-permute-start.38 = (bf16[48,2048]{1,0:T(8,128)(2,1)S(1)}, bf16[48,2048]{1,0:T(8,128)(2,1)S(1)}, u32[]{:S(2)}, u32[]{:S(2)}) collective-permute-start(bf16[48,2048]{1,0:T(8,128)(2,1)S(1)} %get-tuple-element.48), channel_id=1, source_target_pairs={{0,8},{8,0},{16,24},{24,16},{1,9},{9,1},{17,25},{25,17},{2,10},{10... | collective-permute-start | bytes 589832 | tf_op jit(solution)/shard_map/ppermute | solution.py:351
  189.6 11.0 %collective-permute-start.36 = (bf16[48,2048]{1,0:T(8,128)(2,1)S(1)}, bf16[48,2048]{1,0:T(8,128)(2,1)S(1)}, u32[]{:S(2)}, u32[]{:S(2)}) collective-permute-start(bf16[48,2048]{1,0:T(8,128)(2,1)S(1)} %get-tuple-element.46), channel_id=1, source_target_pairs={{0,16},{8,24},{16,0},{24,8},{1,17},{9,25},{17,1},{25,9},{2,18},{10... | collective-permute-start | bytes 589832 | tf_op jit(solution)/shard_map/ppermute | solution.py:350
  190.9 11.3 %collective-permute-start.28 = (bf16[48,2048]{1,0:T(8,128)(2,1)S(1)}, bf16[48,2048]{1,0:T(8,128)(2,1)S(1)}, u32[]{:S(2)}, u32[]{:S(2)}) collective-permute-start(bf16[48,2048]{1,0:T(8,128)(2,1)S(1)} %get-tuple-element.43), channel_id=1, source_target_pairs={{0,8},{8,0},{16,24},{24,16},{1,9},{9,1},{17,25},{25,17},{2,10},{10... | collective-permute-start | bytes 589832 | tf_op jit(solution)/shard_map/ppermute | solution.py:351
  199.9 7.8 %collective-permute-start.26 = (bf16[48,2048]{1,0:T(8,128)(2,1)S(1)}, bf16[48,2048]{1,0:T(8,128)(2,1)S(1)}, u32[]{:S(2)}, u32[]{:S(2)}) collective-permute-start(bf16[48,2048]{1,0:T(8,128)(2,1)S(1)} %get-tuple-element.41), channel_id=1, source_target_pairs={{0,16},{8,24},{16,0},{24,8},{1,17},{9,25},{17,1},{25,9},{2,18},{10... | collective-permute-start | bytes 589832 | tf_op jit(solution)/shard_map/ppermute | solution.py:350
  200.6 7.8 %collective-permute-start.18 = (bf16[48,2048]{1,0:T(8,128)(2,1)S(1)}, bf16[48,2048]{1,0:T(8,128)(2,1)S(1)}, u32[]{:S(2)}, u32[]{:S(2)}) collective-permute-start(bf16[48,2048]{1,0:T(8,128)(2,1)S(1)} %get-tuple-element.38), channel_id=1, source_target_pairs={{0,8},{8,0},{16,24},{24,16},{1,9},{9,1},{17,25},{25,17},{2,10},{10... | collective-permute-start | bytes 589832 | tf_op jit(solution)/shard_map/ppermute | solution.py:351
  202.2 9.8 %collective-permute-start.16 = (bf16[48,2048]{1,0:T(8,128)(2,1)S(1)}, bf16[48,2048]{1,0:T(8,128)(2,1)S(1)}, u32[]{:S(2)}, u32[]{:S(2)}) collective-permute-start(bf16[48,2048]{1,0:T(8,128)(2,1)S(1)} %get-tuple-element.36), channel_id=1, source_target_pairs={{0,16},{8,24},{16,0},{24,8},{1,17},{9,25},{17,1},{25,9},{2,18},{10... | collective-permute-start | bytes 589832 | tf_op jit(solution)/shard_map/ppermute | solution.py:350
  207.8 12.6 %collective-permute-start.39 = (bf16[96,2048]{1,0:T(8,128)(2,1)S(1)}, bf16[96,2048]{1,0:T(8,128)(2,1)S(1)}, u32[]{:S(2)}, u32[]{:S(2)}) collective-permute-start(bf16[96,2048]{1,0:T(8,128)(2,1)S(1)} %pad_maximum_fusion.8), channel_id=1, source_target_pairs={{0,16},{8,24},{16,0},{24,8},{1,17},{9,25},{17,1},{25,9},{2,18},{10... | collective-permute-start | bytes 1179656 | tf_op jit(solution)/shard_map/ppermute | solution.py:359
  208.4 13.2 %collective-permute-start.37 = (bf16[96,2048]{1,0:T(8,128)(2,1)S(1)}, bf16[96,2048]{1,0:T(8,128)(2,1)S(1)}, u32[]{:S(2)}, u32[]{:S(2)}) collective-permute-start(bf16[96,2048]{1,0:T(8,128)(2,1)S(1)} %pad_maximum_fusion.7), channel_id=1, source_target_pairs={{0,8},{8,0},{16,24},{24,16},{1,9},{9,1},{17,25},{25,17},{2,10},{10... | collective-permute-start | bytes 1179656 | tf_op jit(solution)/shard_map/ppermute | solution.py:358
  212.0 16.3 %collective-permute-start.29 = (bf16[96,2048]{1,0:T(8,128)(2,1)S(1)}, bf16[96,2048]{1,0:T(8,128)(2,1)S(1)}, u32[]{:S(2)}, u32[]{:S(2)}) collective-permute-start(bf16[96,2048]{1,0:T(8,128)(2,1)S(1)} %pad_maximum_fusion.6), channel_id=1, source_target_pairs={{0,16},{8,24},{16,0},{24,8},{1,17},{9,25},{17,1},{25,9},{2,18},{10... | collective-permute-start | bytes 1179656 | tf_op jit(solution)/shard_map/ppermute | solution.py:359
  220.4 10.1 %collective-permute-start.27 = (bf16[96,2048]{1,0:T(8,128)(2,1)S(1)}, bf16[96,2048]{1,0:T(8,128)(2,1)S(1)}, u32[]{:S(2)}, u32[]{:S(2)}) collective-permute-start(bf16[96,2048]{1,0:T(8,128)(2,1)S(1)} %pad_maximum_fusion.5), channel_id=1, source_target_pairs={{0,8},{8,0},{16,24},{24,16},{1,9},{9,1},{17,25},{25,17},{2,10},{10... | collective-permute-start | bytes 1179656 | tf_op jit(solution)/shard_map/ppermute | solution.py:358
  221.6 11.6 %collective-permute-start.19 = (bf16[96,2048]{1,0:T(8,128)(2,1)S(1)}, bf16[96,2048]{1,0:T(8,128)(2,1)S(1)}, u32[]{:S(2)}, u32[]{:S(2)}) collective-permute-start(bf16[96,2048]{1,0:T(8,128)(2,1)S(1)} %pad_maximum_fusion.4), channel_id=1, source_target_pairs={{0,16},{8,24},{16,0},{24,8},{1,17},{9,25},{17,1},{25,9},{2,18},{10... | collective-permute-start | bytes 1179656 | tf_op jit(solution)/shard_map/ppermute | solution.py:359
  228.3 7.8 %collective-permute-start.17 = (bf16[96,2048]{1,0:T(8,128)(2,1)S(1)}, bf16[96,2048]{1,0:T(8,128)(2,1)S(1)}, u32[]{:S(2)}, u32[]{:S(2)}) collective-permute-start(bf16[96,2048]{1,0:T(8,128)(2,1)S(1)} %pad_maximum_fusion.3), channel_id=1, source_target_pairs={{0,8},{8,0},{16,24},{24,16},{1,9},{9,1},{17,25},{25,17},{2,10},{10... | collective-permute-start | bytes 1179656 | tf_op jit(solution)/shard_map/ppermute | solution.py:358
  230.5 12.1 %collective-permute-start.40 = (bf16[96,2048]{1,0:T(8,128)(2,1)S(1)}, bf16[96,2048]{1,0:T(8,128)(2,1)S(1)}, u32[]{:S(2)}, u32[]{:S(2)}) collective-permute-start(bf16[96,2048]{1,0:T(8,128)(2,1)S(1)} %add_convert_fusion.1), channel_id=1, source_target_pairs={{0,6},{1,7},{2,0},{3,1},{4,2},{5,3},{6,4},{7,5},{8,14},{9,15},{10,... | collective-permute-start | bytes 1179656 | tf_op jit(solution)/shard_map/ppermute | solution.py:332
  233.2 27.7 %collective-permute-start.30 = (bf16[96,2048]{1,0:T(8,128)(2,1)S(1)}, bf16[96,2048]{1,0:T(8,128)(2,1)S(1)}, u32[]{:S(2)}, u32[]{:S(2)}) collective-permute-start(bf16[96,2048]{1,0:T(8,128)(2,1)S(1)} %add_convert_fusion.2), channel_id=1, source_target_pairs={{0,4},{1,5},{2,6},{3,7},{4,0},{5,1},{6,2},{7,3},{8,12},{9,13},{10,... | collective-permute-start | bytes 1179656 | tf_op jit(solution)/shard_map/ppermute | solution.py:332
  236.2 24.6 %collective-permute-start.20 = (bf16[96,2048]{1,0:T(8,128)(2,1)S(1)}, bf16[96,2048]{1,0:T(8,128)(2,1)S(1)}, u32[]{:S(2)}, u32[]{:S(2)}) collective-permute-start(bf16[96,2048]{1,0:T(8,128)(2,1)S(1)} %add_convert_fusion.3), channel_id=1, source_target_pairs={{0,2},{1,3},{2,4},{3,5},{4,6},{5,7},{6,0},{7,1},{8,10},{9,11},{10,... | collective-permute-start | bytes 1179656 | tf_op jit(solution)/shard_map/ppermute | solution.py:332

commit v2 on v1

--- a/solution.py
+++ b/solution.py
@@ -13,9 +13,23 @@
 
 
 def attention_kernel(
-    part_ref, lam_ref, gain_ref, rows_ref, out_ref, stack_ref, acc_ref, top_ref, *, sub, key_rows, parts, scale
+    part_ref,
+    lam_ref,
+    gain_ref,
+    rows_ref,
+    out_ref,
+    stack_ref,
+    score_ref,
+    acc_ref,
+    top_ref,
+    *,
+    sub,
+    key_rows,
+    parts,
+    scale,
 ):
     tile = pl.program_id(0)
+    exact = math.frexp(scale)[0] == 0.5
     tile_rows = OWNERS_PER_TILE * sub
     span = tile_rows * parts
     width = rows_ref.shape[2]
@@ -26,6 +40,8 @@
     source = tile // tiles_per_source
     start = pl.multiple_of((tile % tiles_per_source) * tile_rows, tile_rows)
     query = rows_ref[source, pl.ds(start, tile_rows), :]
+    if exact:
+        query = (query.astype(jnp.float32) * scale).astype(jnp.bfloat16)
     low = lax.broadcasted_iota(jnp.int32, (tile_rows, width), 1) < half
     nothing = jnp.zeros_like(query)
     stack_ref[0:tile_rows, :] = jnp.where(low, query, nothing)
@@ -34,54 +50,63 @@
     acc_ref[...] = jnp.zeros_like(acc_ref)
     ones = jnp.ones((span, LANES), jnp.bfloat16)
 
-    def one_tile(index, diagonal):
-        owner = index // tiles_per_source
+    def place_of(index, base):
         offset = pl.multiple_of((index % tiles_per_source) * span, span)
-        keys = rows_ref[owner, pl.ds(query_rows + offset, span), :]
-        values = rows_ref[owner, pl.ds(query_rows + key_rows + offset, span), :]
-        scores = (
-            lax.dot_general(
-                stack_ref[...], keys, (((1,), (1,)), ((), ())), preferred_element_type=jnp.float32
-            )
-            * scale
+        return index // tiles_per_source, pl.ds(base + offset, span)
+
+    def score(index):
+        owner, place = place_of(index, query_rows)
+        scores = lax.dot_general(
+            stack_ref[...],
+            rows_ref[owner, place, :],
+            (((1,), (1,)), ((), ())),
+            preferred_element_type=jnp.float32,
         )
-        if diagonal:
-            row = lax.broadcasted_iota(jnp.int32, (tile_rows, LANES), 0)
-            place = row + part_ref[0] * sub
-            for step in range(1, OWNERS_PER_TILE):
-                place = place + jnp.where(row >= step * sub, (parts - 1) * sub, 0)
-            gap = place - lax.broadcasted_iota(jnp.int32, (tile_rows, LANES), 1)
-            gap = jnp.concatenate([gap, gap], axis=0)
-            scores = jnp.concatenate(
-                [
-                    jnp.where(gap >= first, scores[:, first : first + LANES], -jnp.inf)
-                    for first in range(0, span, LANES)
-                ],
-                axis=1,
-            )
+        return scores if exact else scores * scale
+
+    def absorb(index, scores):
+        owner, place = place_of(index, query_rows + key_rows)
         before = top_ref[...]
         after = jnp.maximum(before, jnp.max(scores, axis=1, keepdims=True))
         decay = jnp.exp(before - after)
-        weights = jnp.exp(scores - after[:, :1])
+        weights = jnp.exp(scores - jnp.concatenate([after] * (span // LANES), axis=1))
         top_ref[...] = after
-        acc_ref[...] = acc_ref[...] * decay[:, :1] + jnp.dot(
+        acc_ref[...] = acc_ref[...] * jnp.concatenate(
+            [decay] * (1 + width // LANES), axis=1
+        ) + jnp.dot(
             weights.astype(jnp.bfloat16),
-            jnp.concatenate([values, ones], axis=1),
+            jnp.concatenate([rows_ref[owner, place, :], ones], axis=1),
             preferred_element_type=jnp.float32,
         )
 
-    one_tile(tile, True)
+    score_ref[0] = score(0)
 
     @pl.loop(0, tile)
     def _(index):
-        one_tile(index, False)
+        score_ref[(index + 1) % 2] = score(index + 1)
+        absorb(index, score_ref[index % 2])
+
+    scores = score_ref[tile % 2]
+    row = lax.broadcasted_iota(jnp.int32, (tile_rows, LANES), 0)
+    place = row + part_ref[0] * sub
+    for step in range(1, OWNERS_PER_TILE):
+        place = place + jnp.where(row >= step * sub, (parts - 1) * sub, 0)
+    gap = place - lax.broadcasted_iota(jnp.int32, (tile_rows, LANES), 1)
+    gap = jnp.concatenate([gap, gap], axis=0)
+    absorb(
+        tile,
+        jnp.concatenate(
+            [
+                jnp.where(gap >= first, scores[:, first : first + LANES], -jnp.inf)
+                for first in range(0, span, LANES)
+            ],
+            axis=1,
+        ),
+    )
 
     first = acc_ref[0:tile_rows, :]
     second = acc_ref[tile_rows:, :]
-    mixed = (
-        first[:, :width] / first[:, width : width + 1]
-        - lam_ref[0] * second[:, :width] / second[:, width : width + 1]
-    )
+    mixed = first[:, :width] / first[:, width:] - lam_ref[0] * second[:, :width] / second[:, width:]
     scaled = mixed * lax.rsqrt(jnp.mean(mixed * mixed, axis=1, keepdims=True) + 1e-06)
     out_ref[...] = (scaled * gain_ref[...]).astype(out_ref.dtype)
 
@@ -92,7 +117,9 @@
     total_rows = sources * key_rows // parts
     pairs = total_rows * sources * key_rows
     return pl.pallas_call(
-        functools.partial(attention_kernel, sub=sub, key_rows=key_rows, parts=parts, scale=scale),
+        functools.partial(
+            attention_kernel, sub=sub, key_rows=key_rows, parts=parts, scale=scale
+        ),
         grid=(total_rows // tile_rows,),
         out_shape=jax.ShapeDtypeStruct((total_rows, width), jnp.bfloat16),
         in_specs=[
@@ -104,10 +131,11 @@
         out_specs=pl.BlockSpec((tile_rows, width), lambda i: (i, 0)),
         scratch_shapes=[
             pltpu.VMEM((2 * tile_rows, width), jnp.bfloat16),
+            pltpu.VMEM((2, 2 * tile_rows, tile_rows * parts), jnp.float32),
             pltpu.VMEM((2 * tile_rows, width + LANES), jnp.float32),
             pltpu.VMEM((2 * tile_rows, LANES), jnp.float32),
         ],
-        compiler_params=pltpu.CompilerParams(vmem_limit_bytes=32 * 1024 * 1024),
+        compiler_params=pltpu.CompilerParams(vmem_limit_bytes=12 * 1024 * 1024),
         cost_estimate=pl.CostEstimate(
             flops=8 * pairs * width, bytes_accessed=2 * arrived.size, transcendentals=pairs
         ),
@@ -117,7 +145,6 @@
 
 def project_kernel(heads_ref, weight_ref, residual_ref, gain_ref, routes_ref, updated_ref, normed_ref, acc_ref, *, parts):
     step = pl.program_id(0)
-    sub, width = heads_ref.shape[2:]
     held = heads_ref.shape[0] // parts
     left = jnp.concatenate(
         [
@@ -170,86 +197,164 @@
             pl.BlockSpec((rows, model + LANES), lambda i: (0, 0)),
         ),
         scratch_shapes=[pltpu.VMEM((rows, model), jnp.float32)],
-        compiler_params=pltpu.CompilerParams(vmem_limit_bytes=24 * 1024 * 1024),
+        compiler_params=pltpu.CompilerParams(vmem_limit_bytes=48 * 1024 * 1024),
         cost_estimate=pl.CostEstimate(
             flops=2 * rows * model * columns * depth, bytes_accessed=2 * out_weight.size, transcendentals=0
         ),
         name="project",
     )(heads, out_weight, residual, gain, routes)
+
+
+def choose_kernel(place_ref, block_ref, chosen_ref, *out_refs, held, experts, capacity):
+    model = block_ref.shape[1] - LANES
+    slots = len(out_refs) * held * capacity
+    source = lax.broadcasted_iota(jnp.int32, (LANES, slots), 0)
+    slot = lax.broadcasted_iota(jnp.int32, (LANES, slots), 1)
+    wanted = 0 * slot
+    for column in range(len(out_refs)):
+        for expert in range(held):
+            first = (column * held + expert) * capacity
+            name = jnp.bitwise_xor(place_ref[0], column) * held + expert
+            inside = (slot >= first) & (slot < first + capacity)
+            wanted = jnp.where(inside, 2 * experts + name, wanted)
+    table = jnp.where(source == wanted, 1.0, 0.0).astype(jnp.bfloat16)
+    ranks = jnp.dot(block_ref[:, model:], table, preferred_element_type=jnp.float32)
+    lane = lax.broadcasted_iota(jnp.int32, ranks.shape, 1)
+    order = lax.rem(lane, capacity).astype(jnp.float32)
+    chosen = jnp.where(ranks == order, 1.0, 0.0).astype(jnp.bfloat16)
+    chosen_ref[...] = chosen
+    rows = lax.dot_general(
+        chosen, block_ref[...], (((0,), (0,)), ((), ())), preferred_element_type=jnp.float32
+    ).astype(jnp.bfloat16)
+    for column, out_ref in enumerate(out_refs):
+        out_ref[...] = rows[column * held * capacity : (column + 1) * held * capacity]
+
+
+def choose(place, block, columns, held, experts, capacity):
+    rows, width = block.shape
+    slots = held * capacity
+    whole = pl.BlockSpec(memory_space=pltpu.VMEM)
+    return pl.pallas_call(
+        functools.partial(choose_kernel, held=held, experts=experts, capacity=capacity),
+        out_shape=(
+            jax.ShapeDtypeStruct((rows, columns * slots), jnp.bfloat16),
+            *(jax.ShapeDtypeStruct((slots, width), jnp.bfloat16) for _ in range(columns)),
+        ),
+        in_specs=[pl.BlockSpec(memory_space=pltpu.SMEM), whole],
+        out_specs=(whole,) * (columns + 1),
+        compiler_params=pltpu.CompilerParams(vmem_limit_bytes=16 * 1024 * 1024),
+        cost_estimate=pl.CostEstimate(
+            flops=2 * rows * width * columns * slots, bytes_accessed=4 * rows * width, transcendentals=0
+        ),
+        name="choose",
+    )(place, block)
+
+
+def merge_kernel(chosen_ref, *refs):
+    out_ref, kept_ref = refs[-2:]
+    slots = refs[0].shape[0]
+    for column, ref in enumerate(refs[:-2]):
+        kept_ref[column * slots : (column + 1) * slots, :] = ref[...]
+    total = jnp.dot(chosen_ref[...], kept_ref[...], preferred_element_type=jnp.float32)
+    out_ref[...] = total.astype(out_ref.dtype)
+
+
+def merge(chosen, parts):
+    rows = chosen.shape[0]
+    model = parts[0].shape[1]
+    whole = pl.BlockSpec(memory_space=pltpu.VMEM)
+    return pl.pallas_call(
+        merge_kernel,
+        out_shape=jax.ShapeDtypeStruct((rows, model), jnp.bfloat16),
+        in_specs=[whole] * (1 + len(parts)),
+        out_specs=whole,
+        scratch_shapes=[pltpu.VMEM((chosen.shape[1], model), jnp.bfloat16)],
+        compiler_params=pltpu.CompilerParams(vmem_limit_bytes=16 * 1024 * 1024),
+        cost_estimate=pl.CostEstimate(
+            flops=2 * rows * chosen.shape[1] * model, bytes_accessed=4 * rows * model, transcendentals=0
+        ),
+        name="merge",
+    )(chosen, *parts)
 
 
 def expert_kernel(*refs, blocks, experts):
     first_ref = refs[0]
     block_refs = refs[1 : 1 + blocks]
-    gate_a, up_a, down_a, gate_b, up_b, down_b = refs[1 + blocks : 7 + blocks]
+    weight_refs = refs[1 + blocks : 7 + blocks]
     out_refs = refs[7 + blocks : 7 + 2 * blocks]
-    rows_ref, acc_ref = refs[7 + 2 * blocks :]
-    expert = pl.program_id(0)
-    model = rows_ref.shape[1] - LANES
-
-    @pl.when(expert == 0)
-    def _():
-        place = 0
-        for ref in block_refs:
-            rows_ref[place : place + ref.shape[0], :] = ref[...]
-            place += ref.shape[0]
-
-    routes = rows_ref[:, model:].astype(jnp.float32)
-    lane = lax.broadcasted_iota(jnp.int32, routes.shape, 1)
-    mine = first_ref[0] + expert
-    share = jnp.sum(
-        jnp.where((lane == mine) | (lane == mine + experts), routes, 0.0), axis=1, keepdims=True
-    )
-    rows = rows_ref[:, :model]
-    product = None
-    for gate_ref, up_ref, down_ref in ((gate_a, up_a, down_a), (gate_b, up_b, down_b)):
-        gate = jnp.dot(rows, gate_ref[0], preferred_element_type=jnp.float32)
-        up = jnp.dot(rows, up_ref[0], preferred_element_type=jnp.float32)
-        inner = (gate / (1.0 + jnp.exp(-gate)) * up * share).astype(jnp.bfloat16)
-        term = jnp.dot(inner, down_ref[0], preferred_element_type=jnp.float32)
-        product = term if product is None else product + term
-
-    @pl.when(expert == 0)
-    def _():
-        acc_ref[...] = product
-
-    @pl.when(expert > 0)
-    def _():
-        acc_ref[...] += product
-
-    @pl.when(expert == pl.num_programs(0) - 1)
-    def _():
-        place = 0
-        for ref in out_refs:
-            ref[...] = acc_ref[place : place + ref.shape[0], :].astype(jnp.bfloat16)
-            place += ref.shape[0]
+    kept_refs = refs[7 + 2 * blocks : 13 + 2 * blocks]
+    rows_ref, sems = refs[13 + 2 * blocks :]
+    model = rows_ref.shape[2] - LANES
+    held = kept_refs[0].shape[0]
+    capacity = block_refs[0].shape[0] // held
+    sets = ((0, 1, 2), (3, 4, 5))
+
+    def copy(index, expert):
+        return pltpu.make_async_copy(
+            weight_refs[index].at[expert], kept_refs[index].at[expert], sems.at[index, expert]
+        )
+
+    for expert in range(held):
+        for indices in sets:
+            for index in indices:
+                copy(index, expert).start()
+
+    for expert in range(held):
+        for number, ref in enumerate(block_refs):
+            rows_ref[expert, number * capacity : (number + 1) * capacity, :] = ref[
+                expert * capacity : (expert + 1) * capacity, :
+            ]
+
+    for expert in range(held):
+        routes = rows_ref[expert, :, model:].astype(jnp.float32)
+        lane = lax.broadcasted_iota(jnp.int32, routes.shape, 1)
+        mine = first_ref[0] + expert
+        share = jnp.sum(
+            jnp.where((lane == mine) | (lane == mine + experts), routes, 0.0), axis=1, keepdims=True
+        )
+        rows = rows_ref[expert, :, :model]
+        total = None
+        for indices in sets:
+            parts = []
+            for index in indices[:2]:
+                copy(index, expert).wait()
+                parts.append(
+                    jnp.dot(rows, kept_refs[index][expert], preferred_element_type=jnp.float32)
+                )
+            gate, up = parts
+            inner = (gate / (1.0 + jnp.exp(-gate)) * up * share).astype(jnp.bfloat16)
+            copy(indices[2], expert).wait()
+            term = jnp.dot(inner, kept_refs[indices[2]][expert], preferred_element_type=jnp.float32)
+            total = term if total is None else total + term
+        total = total.astype(jnp.bfloat16)
+        for number, ref in enumerate(out_refs):
+            ref[expert * capacity : (expert + 1) * capacity, :] = total[
+                number * capacity : (number + 1) * capacity
+            ]
 
 
 def expert_pass(first, blocks, weights, experts):
     held, model, hidden = weights[0].shape
-    total = sum(block.shape[0] for block in blocks)
-    whole = [pl.BlockSpec(block.shape, lambda i: (0, 0)) for block in blocks]
-    wide = pl.BlockSpec((1, model, hidden), lambda i: (i, 0, 0))
-    tall = pl.BlockSpec((1, hidden, model), lambda i: (i, 0, 0))
+    slots = blocks[0].shape[0]
+    total = len(blocks) * slots
+    whole = pl.BlockSpec(memory_space=pltpu.VMEM)
     return pl.pallas_call(
         functools.partial(expert_kernel, blocks=len(blocks), experts=experts),
-        grid=(held,),
-        out_shape=tuple(
-            jax.ShapeDtypeStruct((block.shape[0], model), jnp.bfloat16) for block in blocks
-        ),
-        in_specs=[pl.BlockSpec(memory_space=pltpu.SMEM), *whole, wide, wide, tall, wide, wide, tall],
-        out_specs=tuple(
-            pl.BlockSpec((block.shape[0], model), lambda i: (0, 0)) for block in blocks
-        ),
-        scratch_shapes=[
-            pltpu.VMEM((total, model + LANES), jnp.bfloat16),
-            pltpu.VMEM((total, model), jnp.float32),
+        out_shape=tuple(jax.ShapeDtypeStruct((slots, model), jnp.bfloat16) for _ in blocks),
+        in_specs=[pl.BlockSpec(memory_space=pltpu.SMEM)]
+        + [whole] * len(blocks)
+        + [pl.BlockSpec(memory_space=pl.ANY)] * len(weights),
+        out_specs=(whole,) * len(blocks),
+        scratch_shapes=[pltpu.VMEM(w.shape, w.dtype) for w in weights]
+        + [
+            pltpu.VMEM((held, total // held, model + LANES), jnp.bfloat16),
+            pltpu.SemaphoreType.DMA((len(weights), held)),
         ],
-        compiler_params=pltpu.CompilerParams(vmem_limit_bytes=40 * 1024 * 1024),
+        compiler_params=pltpu.CompilerParams(vmem_limit_bytes=46 * 1024 * 1024),
         cost_estimate=pl.CostEstimate(
-            flops=12 * held * total * model * hidden,
+            flops=12 * total * model * hidden,
             bytes_accessed=12 * held * model * hidden,
-            transcendentals=2 * held * total * hidden,
+            transcendentals=2 * total * hidden,
         ),
         name="experts",
     )(first, *blocks, *weights)
@@ -271,7 +376,7 @@
     down_weight,
 ):
     tokens, heads, width = queries.shape
-    rows, model = residual.shape
+    rows, _ = residual.shape
     sp_count, tp_count = lax.axis_size("sp"), lax.axis_size("tp")
     sp_index = lax.axis_index("sp")
     parts = sp_count // heads
@@ -318,52 +423,53 @@
         axis=1,
     )
     coarse = lax.reduce_precision(share, 8, 7)
+    named = jnp.any(
+        expert_ids[:, :, None] == jnp.arange(experts, dtype=jnp.int32), axis=1
+    ).astype(jnp.float32)
+    earlier = jnp.tril(jnp.ones((rows, rows), jnp.float32), -1)
+    ranks = jnp.where(named > 0, jnp.dot(earlier, named), -1.0)
     routes = jnp.concatenate(
-        [coarse, share - coarse, jnp.zeros((rows, LANES - 2 * experts), jnp.float32)], axis=1
+        [coarse, share - coarse, ranks, jnp.zeros((rows, LANES - 3 * experts), jnp.float32)], axis=1
     ).astype(jnp.bfloat16)
     updated, normed = project(
         regrouped, out_weight, residual, norm_gain.reshape(1, -1), routes, parts
     )
 
-    across_x = [(i, i ^ 1) for i in range(sp_count)]
-    across_y = [(i, i ^ 2) for i in range(sp_count)]
-
-    def turned(array, steps):
-        return lax.ppermute(
-            array, "tp", [(i, (i + 2 * steps) % tp_count) for i in range(tp_count)]
-        )
+    def turn(k):
+        return [(i, (i + 2 * k) % tp_count) for i in range(tp_count)]
+
+    def across(array, column):
+        return lax.ppermute(array, "sp", [(i, i ^ column) for i in range(sp_count)])
 
     layers = tp_count // 2
-    cut = rows // 2
-    sources = [normed] + [turned(normed, -k) for k in range(1, layers)]
+    capacity = row_capacity(rows, expert_ids.shape[1], experts)
+    place = sp_index.reshape(1)
     first = (sp_index * held).reshape(1)
     weights = (*mine, *other)
+    blocks = [normed] + [lax.ppermute(normed, "tp", turn(-k)) for k in range(1, layers)]
+    chosen, arrivals = [], []
+    for block in blocks:
+        table, *sent = choose(place, block, sp_count, held, experts, capacity)
+        chosen.append(table)
+        arrivals.append([sent[0]] + [across(sent[c], c) for c in range(1, sp_count)])
+    results = {}
+    near = near_first(layers)
+    for group in ((0, near[0]), near[1:]):
+        rows_in = [block for k in group for block in arrivals[k]]
+        done = expert_pass(first, rows_in, weights, experts)
+        for i, k in enumerate(group):
+            results[k] = done[i * sp_count : (i + 1) * sp_count]
     reduced = []
-    for block in sources:
-        by_x = lax.ppermute(block, "sp", across_x)
-        by_y = lax.ppermute(block, "sp", across_y)
-        far_low = lax.ppermute(by_x[:cut], "sp", across_y)
-        far_high = lax.ppermute(by_y[cut:], "sp", across_x)
-        own, to_x, to_y, to_low, to_high = expert_pass(
-            first, (block, by_x, by_y, far_low, far_high), weights, experts
-        )
-        add_low = lax.ppermute(to_low, "sp", across_y)
-        add_high = lax.ppermute(to_high, "sp", across_x)
-        to_x = jnp.concatenate(
-            [(to_x[:cut].astype(jnp.float32) + add_low.astype(jnp.float32)).astype(jnp.bfloat16), to_x[cut:]]
-        )
-        to_y = jnp.concatenate(
-            [to_y[:cut], (to_y[cut:].astype(jnp.float32) + add_high.astype(jnp.float32)).astype(jnp.bfloat16)]
-        )
-        from_x = lax.ppermute(to_x, "sp", across_x)
-        from_y = lax.ppermute(to_y, "sp", across_y)
-        reduced.append(
-            own.astype(jnp.float32) + from_x.astype(jnp.float32) + from_y.astype(jnp.float32)
-        )
-    total = updated.astype(jnp.float32) + reduced[0]
-    for k in range(1, layers):
-        total = total + turned(reduced[k].astype(jnp.bfloat16), k).astype(jnp.float32)
-    return total.astype(jnp.bfloat16)
+    for k in range(layers):
+        result = results[k]
+        back = [result[0]] + [across(result[c], c) for c in range(1, sp_count)]
+        reduced.append(merge(chosen[k], back))
+    returned = [lax.ppermute(reduced[k], "tp", turn(k)) for k in range(1, layers)]
+    return summed_rows(updated, reduced[0], *returned)
+
+
+def row_capacity(rows, routes, experts):
+    return max(2, 4 * rows * routes // (3 * experts))
 
 
 def shards(
@@ -431,9 +537,7 @@
     def untouched(state):
         return state
 
-    running_max, totals, summed = lax.cond(
-        jnp.int32(0) <= query_pos[-1], through, untouched, start_state
-    )
+    _, totals, summed = lax.cond(jnp.int32(0) <= query_pos[-1], through, untouched, start_state)
     mixed = (
         summed[0] / totals[0][..., None] - lambdas[:, None, None] * summed[1] / totals[1][..., None]
     )
@@ -502,22 +606,29 @@
     return (updated.astype(jnp.float32) + moe_sum).astype(jnp.bfloat16)
 
 
+def summed_rows(*terms):
+    return sum(term.astype(jnp.float32) for term in terms).astype(jnp.bfloat16)
+
+
+def near_first(layers):
+    return sorted(range(1, layers), key=lambda k: (min(k, layers - k), k))
+
+
 def fits_balanced(queries, residual, expert_ids, gate_weight, sp_count, tp_count):
     tokens, heads, width = queries.shape
     rows = residual.shape[0]
     held = gate_weight.shape[0]
-    if sp_count != 4 or tp_count % 2 or sp_count % heads or width != LANES:
+    if sp_count != 4 or tp_count % 2 or tp_count < 6 or sp_count % heads or width != LANES:
         return False
     sub = rows // (sp_count // heads)
     span = OWNERS_PER_TILE * rows
-    capacity = 4 * rows * expert_ids.shape[1] // (3 * held * sp_count)
+    capacity = row_capacity(rows, expert_ids.shape[1], held * sp_count)
     return (
         sub % 16 == 0
-        and rows % 32 == 0
         and tokens % span == 0
         and span % LANES == 0
-        and 2 * held * sp_count <= LANES
-        and 2 * held * capacity >= rows
+        and capacity % 16 == 0
+        and 3 * held * sp_count <= LANES
     )
 
 

time: 263 us -> 234 us (0.89)
  waiting for transfers between devices: 127 us -> 106 us
  Pallas kernels: 66.1 us -> 56.4 us
  starting transfers between devices: 51.8 us -> 55.3 us
    ppermute x38 -> x30, waiting for transfers between devices: 91.9 us -> 70.7 us  [the longest x24 37 us: across(): return lax.ppermute(array, 'sp', [(i, i ^ column) for i in range(sp_count)])]
    pallas_call x4 -> x2, Pallas kernels: 32.4 us -> 17 us  [expert_pass(): pl.pallas_call(functools.partial(expert_kernel, blocks=len(blocks), exper...]
    pallas_call x0 -> x8, Pallas kernels: none -> 5.47 us  [the longest x4 4.26 us: choose(): pl.pallas_call(functools.partial(choose_kernel, held=held, experts=expert...]
    pallas_call x1, Pallas kernels: 3.47 us -> 7.37 us  [project(): pl.pallas_call(functools.partial(project_kernel, parts=parts), grid=(colu...]
    pallas_call x1, Pallas kernels: 30.3 us -> 26.5 us  [attention(): pl.pallas_call(functools.partial(attention_kernel, sub=sub, key_rows=key_...]
    ppermute x38 -> x30, starting transfers between devices: 41 us -> 44.3 us  [the longest x24 29 us: across(): return lax.ppermute(array, 'sp', [(i, i ^ column) for i in range(sp_count)])]
    unnamed x26 -> x38, local copies, waits for them, and re-layouts: 8.19 us -> 7.67 us
  transfers between devices with their start and end apart: 43 -> 35, of which waited for: 21 -> 12; matrix products, arithmetic and copies ran while one was open for 1% -> 1% of each run, Pallas kernels for 25% -> 24%
where the time goes in v2:
time: 234 us; the launch traced here: 233 us
  waiting for transfers between devices  106 us (45%)
  Pallas kernels  56.4 us (24%)
  starting transfers between devices  55.3 us (24%)
  local copies, waits for them, and re-layouts  12.1 us (5%)
  other arithmetic  2.6 us (1%)
    ppermute x24, waiting for transfers between devices, across(): return lax.ppermute(array, 'sp', [(i, i ^ column) for i in range(sp_count)])  37 us
    ppermute x24, starting transfers between devices, across(): return lax.ppermute(array, 'sp', [(i, i ^ column) for i in range(sp_count)])  29 us
    pallas_call x1, Pallas kernels, attention(): pl.pallas_call(functools.partial(attention_kernel, sub=sub, key_rows=key_...  26.5 us
    ppermute x3, waiting for transfers between devices, balanced(): lax.ppermute(normed, 'tp', turn(-k))  22.8 us
    all_to_all x1, waiting for transfers between devices, balanced(): lax.all_to_all(jnp.concatenate([split, keys, values], axis=1), 'sp', spli...  22.6 us
    pallas_call x2, Pallas kernels, expert_pass(): pl.pallas_call(functools.partial(expert_kernel, blocks=len(blocks), exper...  17 us
    all_to_all x1, waiting for transfers between devices, balanced(): lax.all_to_all(attended.reshape(sp_count * tp_count, sub, width), ('sp',...  13.1 us
    ppermute x3, starting transfers between devices, balanced(): lax.ppermute(reduced[k], 'tp', turn(k))  11.5 us
  transfers between devices with their start and end apart: 35, of which 12 were waited for; matrix products, arithmetic and copies ran while one was open for 1% of the time, Pallas kernels for 24%

profile of v2, /device:TPU:0, one launch (start us, length us, event | category | flops | bytes accessed | tf_op | source)
XLA Modules:
  0.0 233.3 jit_solution(7101267194978970392)
XLA Ops:
  0.0 1.0 copy.30
  1.1 1.1 copy.29
  2.1 1.1 copy.28
  3.4 1.4 pad_maximum_fusion
  4.8 5.3 %all-to-all-start = ((bf16[4,1920,128]{2,1,0:T(8,128)(2,1)}), bf16[4,1920,128]{2,1,0:T(8,128)(2,1)}, u32[]{:S(2)}, u32[]{:S(2)}) async-start(bf16[4,1920,128]{2,1,0:T(8,128)(2,1)} %pad_maximum_fusion), calls=%async_computation | async-start | bytes 3932160 | tf_op jit(solution)/shard_map/all_to_all | solution.py:396
  10.2 0.5 collective-permute-start.8
  11.2 0.6 dynamic_slice.3.lam_ref
  11.9 22.6 %all-to-all-done.rows_ref = bf16[4,1920,128]{2,1,0:T(8,128)(2,1)} async-done(((bf16[4,1920,128]{2,1,0:T(8,128)(2,1)}), bf16[4,1920,128]{2,1,0:T(8,128)(2,1)}, u32[]{:S(2)}, u32[]{:S(2)}) %all-to-all-start) | async-done | bytes 1966112 | tf_op jit(solution)/shard_map/all_to_all | solution.py:396
  34.5 26.5 %attention.1 = bf16[1536,128]{1,0:T(8,128)(2,1)} custom-call(s32[1]{0:T(128)} %bitcast.part_ref, f32[1]{0:T(128)} %dynamic_slice.3.lam_ref, f32[1,128]{1,0:T(1,128)S(1)} %bitcast.18, bf16[4,1920,128]{2,1,0:T(8,128)(2,1)} %all-to-all-done.rows_ref), custom_call_target="tpu_custom_call" | custom-call | flops 4831838208 | bytes 1966080 | tf_op jit(solution)/shard_map/attention/pallas_call | solution.py:119
  61.0 5.1 %all-to-all-start.1 = ((bf16[32,48,128]{2,1,0:T(8,128)(2,1)}), bf16[32,48,128]{2,1,0:T(8,128)(2,1)S(1)}, u32[]{:S(2)}, u32[]{:S(2)}) async-start(bf16[32,48,128]{2,1,0:T(8,128)(2,1)} %bitcast.9), calls=%async_computation.1 | async-start | bytes 786432 | tf_op jit(solution)/shard_map/all_to_all | solution.py:409
  66.4 13.1 %all-to-all-done.1 = bf16[32,48,128]{2,1,0:T(8,128)(2,1)S(1)} async-done(((bf16[32,48,128]{2,1,0:T(8,128)(2,1)}), bf16[32,48,128]{2,1,0:T(8,128)(2,1)S(1)}, u32[]{:S(2)}, u32[]{:S(2)}) %all-to-all-start.1) | async-done | bytes 393248 | tf_op jit(solution)/shard_map/all_to_all | solution.py:409
  79.5 7.4 %project.1 = (bf16[96,2048]{1,0:T(8,128)(2,1)S(1)}, bf16[96,2176]{1,0:T(8,128)(2,1)S(1)}) custom-call(bf16[4,8,48,128]{3,2,1,0:T(8,128)(2,1)S(1)} %bitcast.16, bf16[2048,2048]{1,0:T(8,128)(2,1)} %weight_ref.1, bf16[96,2048]{1,0:T(8,128)(2,1)S(1)} %copy-done.1, f32[1,2048]{1,0:T(1,128)S(1)} %bitcast.17, bf16[96,128]{1,0:T(8,128)(2,1)S(1)} %maximum_maximum_fusion.routes_ref), custom_call_target="tpu_custom_call" | custom-call | flops 805306368 | bytes 8388608 | tf_op jit(solution)/shard_map/project/pallas_call | solution.py:181
  86.9 0.5 collective-permute-start.17
  87.4 3.3 %collective-permute-start.3 = (bf16[96,2176]{1,0:T(8,128)(2,1)S(1)}, bf16[96,2176]{1,0:T(8,128)(2,1)S(1)}, u32[]{:S(2)}, u32[]{:S(2)}) collective-permute-start(bf16[96,2176]{1,0:T(8,128)(2,1)S(1)} %get-tuple-element.44.block_ref), channel_id=1, source_target_pairs={{0,6},{1,7},{2,0},{3,1},{4,2},{5,3},{6,4},{7,5},{8,14},{9,15},{10,... | collective-permute-start | bytes 1253384 | tf_op jit(solution)/shard_map/ppermute | solution.py:449
  90.7 0.6 choose.4
  91.4 0.7 copy-done.13
  92.1 0.7 copy-done.14
  92.8 8.6 %collective-permute-done.18.block_ref = bf16[96,2176]{1,0:T(8,128)(2,1)S(1)} collective-permute-done((bf16[96,2176]{1,0:T(8,128)(2,1)S(1)}, bf16[96,2176]{1,0:T(8,128)(2,1)S(1)}, u32[]{:S(2)}, u32[]{:S(2)}) %collective-permute-start.18) | collective-permute-done | bytes 417824 | tf_op jit(solution)/shard_map/ppermute | solution.py:449
  101.4 1.5 choose.7
  102.8 0.7 copy-done.2
  103.5 0.6 copy-done.10
  104.2 14.2 %collective-permute-done.17.block_ref = bf16[96,2176]{1,0:T(8,128)(2,1)S(1)} collective-permute-done((bf16[96,2176]{1,0:T(8,128)(2,1)S(1)}, bf16[96,2176]{1,0:T(8,128)(2,1)S(1)}, u32[]{:S(2)}, u32[]{:S(2)}) %collective-permute-start.17) | collective-permute-done | bytes 417824 | tf_op jit(solution)/shard_map/ppermute | solution.py:449
  118.3 0.6 collective-permute-start.19
  118.9 1.5 choose.6
  120.4 0.7 copy-done.6
  121.2 0.6 copy-done.8
  121.8 0.8 collective-permute-start.20
  122.5 2.2 collective-permute-start.21
  124.7 0.6 collective-permute-start.22
  125.3 0.8 collective-permute-start.23
  126.2 0.7 copy-done.4
  126.9 2.0 collective-permute-start.24
  128.9 0.6 choose.5
  129.6 8.2 %collective-permute-done.20.refs_3_ = bf16[64,2176]{1,0:T(8,128)(2,1)} collective-permute-done((bf16[64,2176]{1,0:T(8,128)(2,1)}, bf16[64,2176]{1,0:T(8,128)(2,1)}, u32[]{:S(2)}, u32[]{:S(2)}) %collective-permute-start.20) | collective-permute-done | bytes 278560 | tf_op jit(solution)/shard_map/ppermute | solution.py:442
  137.7 1.4 collective-permute-start.1
  139.1 3.1 %collective-permute-start.2 = (bf16[64,2176]{1,0:T(8,128)(2,1)}, bf16[64,2176]{1,0:T(8,128)(2,1)S(1)}, u32[]{:S(2)}, u32[]{:S(2)}) collective-permute-start(bf16[64,2176]{1,0:T(8,128)(2,1)} %copy-done.13), channel_id=1, source_target_pairs={{0,24},{8,16},{16,8},{24,0},{1,25},{9,17},{17,9},{25,1},{2,26},{10... | collective-permute-start | bytes 835592 | tf_op jit(solution)/shard_map/ppermute | solution.py:442
  142.3 12.6 %collective-permute-done.23.refs_7_ = bf16[64,2176]{1,0:T(8,128)(2,1)} collective-permute-done((bf16[64,2176]{1,0:T(8,128)(2,1)}, bf16[64,2176]{1,0:T(8,128)(2,1)}, u32[]{:S(2)}, u32[]{:S(2)}) %collective-permute-start.23) | collective-permute-done | bytes 278560 | tf_op jit(solution)/shard_map/ppermute | solution.py:442
  154.9 1.2 collective-permute-start.5
  156.1 1.9 collective-permute-start.6
  158.0 1.0 copy-done.3
  159.0 1.0 copy-done.5
  159.9 1.0 copy-done.7
  160.9 9.2 %experts.3 = (bf16[64,2048]{1,0:T(8,128)(2,1)S(1)}, bf16[64,2048]{1,0:T(8,128)(2,1)S(1)}, bf16[64,2048]{1,0:T(8,128)(2,1)S(1)}, bf16[64,2048]{1,0:T(8,128)(2,1)S...) custom-call(s32[1]{0:T(128)} %bitcast.13.refs_0_, ...), custom_call_target="tpu_custom_call" | custom-call | flops 3221225472 | bytes 12582912 | tf_op jit(solution)/shard_map/experts/pallas_call | solution.py:341
  170.1 0.4 collective-permute-start.29
  170.5 1.2 collective-permute-start.30
  171.7 1.9 collective-permute-start.31
  173.6 1.8 collective-permute-done.5.refs_7_
  175.5 1.4 collective-permute-start.25
  176.8 1.0 collective-permute-start.26
  177.9 1.4 collective-permute-done.29.refs_1_
  179.3 1.0 collective-permute-start.27
  180.3 7.9 %experts.2 = (bf16[64,2048]{1,0:T(8,128)(2,1)S(1)}, bf16[64,2048]{1,0:T(8,128)(2,1)S(1)}, bf16[64,2048]{1,0:T(8,128)(2,1)S(1)}, bf16[64,2048]{1,0:T(8,128)(2,1)S...) custom-call(s32[1]{0:T(128)} %bitcast.13.refs_0_, ...), custom_call_target="tpu_custom_call" | custom-call | flops 3221225472 | bytes 12582912 | tf_op jit(solution)/shard_map/experts/pallas_call | solution.py:341
  188.2 1.7 collective-permute-start.13
  189.9 0.9 collective-permute-start.14
  190.8 1.0 collective-permute-start.15
  191.8 6.2 %collective-permute-done.26.refs_2_ = bf16[64,2048]{1,0:T(8,128)(2,1)S(1)} collective-permute-done((bf16[64,2048]{1,0:T(8,128)(2,1)S(1)}, bf16[64,2048]{1,0:T(8,128)(2,1)S(1)}, u32[]{:S(2)}, u32[]{:S(2)}) %collective-permute-start.26) | collective-permute-done | bytes 262176 | tf_op jit(solution)/shard_map/ppermute | solution.py:442
  197.9 1.4 collective-permute-start.10
  199.6 8.7 %collective-permute-start.32 = (bf16[96,2048]{1,0:T(8,128)(2,1)S(1)}, bf16[96,2048]{1,0:T(8,128)(2,1)S(1)}, u32[]{:S(2)}, u32[]{:S(2)}) collective-permute-start(bf16[96,2048]{1,0:T(8,128)(2,1)S(1)} %merge.7), channel_id=1, source_target_pairs={{0,6},{1,7},{2,0},{3,1},{4,2},{5,3},{6,4},{7,5},{8,14},{9,15},{10,... | collective-permute-start | bytes 1179656 | tf_op jit(solution)/shard_map/ppermute | solution.py:467
  209.0 2.8 %collective-permute-start.16 = (bf16[96,2048]{1,0:T(8,128)(2,1)S(1)}, bf16[96,2048]{1,0:T(8,128)(2,1)S(1)}, u32[]{:S(2)}, u32[]{:S(2)}) collective-permute-start(bf16[96,2048]{1,0:T(8,128)(2,1)S(1)} %merge.5), channel_id=1, source_target_pairs={{0,2},{1,3},{2,4},{3,5},{4,6},{5,7},{6,0},{7,1},{8,10},{9,11},{10,... | collective-permute-start | bytes 1179656 | tf_op jit(solution)/shard_map/ppermute | solution.py:467
  211.8 1.2 collective-permute-start.11
  212.9 1.4 collective-permute-start.12
  214.3 6.6 %collective-permute-done.11.refs_2_ = bf16[64,2048]{1,0:T(8,128)(2,1)S(1)} collective-permute-done((bf16[64,2048]{1,0:T(8,128)(2,1)S(1)}, bf16[64,2048]{1,0:T(8,128)(2,1)S(1)}, u32[]{:S(2)}, u32[]{:S(2)}) %collective-permute-start.11) | collective-permute-done | bytes 262176 | tf_op jit(solution)/shard_map/ppermute | solution.py:442
  221.3 10.9 %collective-permute-done.28 = bf16[96,2048]{1,0:T(8,128)(2,1)S(1)} collective-permute-done((bf16[96,2048]{1,0:T(8,128)(2,1)S(1)}, bf16[96,2048]{1,0:T(8,128)(2,1)S(1)}, u32[]{:S(2)}, u32[]{:S(2)}) %collective-permute-start.28) | collective-permute-done | bytes 393248 | tf_op jit(solution)/shard_map/ppermute | solution.py:467
  232.2 1.1 add_convert_fusion
  (78 shorter events, 2.7 us)
Async XLA Ops:
  4.8 5.4 %copy-start = (bf16[2,2048,256]{2,1,0:T(8,128)(2,1)S(1)}, bf16[2,2048,256]{2,1,0:T(8,128)(2,1)}, u32[]{:S(2)}) copy-start(bf16[2,2048,256]{2,1,0:T(8,128)(2,1)} %refs_9_.3) | copy-start | bytes 6291460
  4.8 5.9 %copy-start.16 = (s32[96,2]{0,1:T(2,128)S(1)}, s32[96,2]{0,1:T(2,128)}, u32[]{:S(2)}) copy-start(s32[96,2]{0,1:T(2,128)} %param.21) | copy-start | bytes 2308
  4.8 5.9 %copy-start.17 = (f32[96,2]{0,1:T(2,128)S(1)}, f32[96,2]{0,1:T(2,128)}, u32[]{:S(2)}) copy-start(f32[96,2]{0,1:T(2,128)} %param.22) | copy-start | bytes 2308
  4.8 6.4 %copy-start.18 = (f32[2]{0:T(128)S(1)}, f32[2]{0:T(128)}, u32[]{:S(2)}) copy-start(f32[2]{0:T(128)} %param.16) | copy-start | bytes 28
  4.8 29.7 %copy-start.15 = (f32[128]{0:T(128)S(1)}, f32[128]{0:T(128)}, u32[]{:S(2)}) copy-start(f32[128]{0:T(128)} %param.17) | copy-start | bytes 1540
  4.8 29.7 %all-to-all-start = ((bf16[4,1920,128]{2,1,0:T(8,128)(2,1)}), bf16[4,1920,128]{2,1,0:T(8,128)(2,1)}, u32[]{:S(2)}, u32[]{:S(2)}) async-start(bf16[4,1920,128]{2,1,0:T(8,128)(2,1)} %pad_maximum_fusion), calls=%async_computation | async-start | bytes 3932160 | tf_op jit(solution)/shard_map/all_to_all | solution.py:396
  10.2 77.3 %collective-permute-start.7 = (bf16[2,2048,256]{2,1,0:T(8,128)(2,1)S(1)}, bf16[2,2048,256]{2,1,0:T(8,128)(2,1)}, u32[]{:S(2)}, u32[]{:S(2)}) collective-permute-start(bf16[2,2048,256]{2,1,0:T(8,128)(2,1)S(1)} %copy-done), channel_id=1, source_target_pairs={{0,1},{1,0},{2,3},{3,2},{4,5},{5,4},{6,7},{7,6},{8,9},{9,8},{10,11... | collective-permute-start | bytes 6291464 | tf_op jit(solution)/shard_map/ppermute | solution.py:389
  10.2 111.6 %collective-permute-start.8 = (bf16[2,2048,256]{2,1,0:T(8,128)(2,1)}, bf16[2,2048,256]{2,1,0:T(8,128)(2,1)}, u32[]{:S(2)}, u32[]{:S(2)}) collective-permute-start(bf16[2,2048,256]{2,1,0:T(8,128)(2,1)} %refs_10_.3), channel_id=1, source_target_pairs={{0,1},{1,0},{2,3},{3,2},{4,5},{5,4},{6,7},{7,6},{8,9},{9,8},{10,11... | collective-permute-start | bytes 6291464 | tf_op jit(solution)/shard_map/ppermute | solution.py:389
  10.7 111.9 %collective-permute-start.9 = (bf16[2,256,2048]{2,1,0:T(8,128)(2,1)}, bf16[2,256,2048]{2,1,0:T(8,128)(2,1)}, u32[]{:S(2)}, u32[]{:S(2)}) collective-permute-start(bf16[2,256,2048]{2,1,0:T(8,128)(2,1)} %refs_11_.3), channel_id=1, source_target_pairs={{0,1},{1,0},{2,3},{3,2},{4,5},{5,4},{6,7},{7,6},{8,9},{9,8},{10,11... | collective-permute-start | bytes 6291464 | tf_op jit(solution)/shard_map/ppermute | solution.py:389
  34.5 45.0 %copy-start.1 = (bf16[96,2048]{1,0:T(8,128)(2,1)S(1)}, bf16[96,2048]{1,0:T(8,128)(2,1)}, u32[]{:S(2)}) copy-start(bf16[96,2048]{1,0:T(8,128)(2,1)} %residual_ref.1) | copy-start | bytes 1179652
  34.5 45.0 %copy-start.12 = (f32[2048]{0:T(1024)S(1)}, f32[2048]{0:T(1024)}, u32[]{:S(2)}) copy-start(f32[2048]{0:T(1024)} %param.20) | copy-start | bytes 24580
  61.0 18.5 %all-to-all-start.1 = ((bf16[32,48,128]{2,1,0:T(8,128)(2,1)}), bf16[32,48,128]{2,1,0:T(8,128)(2,1)S(1)}, u32[]{:S(2)}, u32[]{:S(2)}) async-start(bf16[32,48,128]{2,1,0:T(8,128)(2,1)} %bitcast.9), calls=%async_computation.1 | async-start | bytes 786432 | tf_op jit(solution)/shard_map/all_to_all | solution.py:409
  86.9 14.5 %collective-permute-start.18 = (bf16[96,2176]{1,0:T(8,128)(2,1)S(1)}, bf16[96,2176]{1,0:T(8,128)(2,1)S(1)}, u32[]{:S(2)}, u32[]{:S(2)}) collective-permute-start(bf16[96,2176]{1,0:T(8,128)(2,1)S(1)} %get-tuple-element.44.block_ref), channel_id=1, source_target_pairs={{0,2},{1,3},{2,4},{3,5},{4,6},{5,7},{6,0},{7,1},{8,10},{9,11},{10,... | collective-permute-start | bytes 1253384 | tf_op jit(solution)/shard_map/ppermute | solution.py:449
  86.9 31.4 %collective-permute-start.17 = (bf16[96,2176]{1,0:T(8,128)(2,1)S(1)}, bf16[96,2176]{1,0:T(8,128)(2,1)S(1)}, u32[]{:S(2)}, u32[]{:S(2)}) collective-permute-start(bf16[96,2176]{1,0:T(8,128)(2,1)S(1)} %get-tuple-element.44.block_ref), channel_id=1, source_target_pairs={{0,4},{1,5},{2,6},{3,7},{4,0},{5,1},{6,2},{7,3},{8,12},{9,13},{10,... | collective-permute-start | bytes 1253384 | tf_op jit(solution)/shard_map/ppermute | solution.py:449
  87.4 37.9 %collective-permute-start.3 = (bf16[96,2176]{1,0:T(8,128)(2,1)S(1)}, bf16[96,2176]{1,0:T(8,128)(2,1)S(1)}, u32[]{:S(2)}, u32[]{:S(2)}) collective-permute-start(bf16[96,2176]{1,0:T(8,128)(2,1)S(1)} %get-tuple-element.44.block_ref), channel_id=1, source_target_pairs={{0,6},{1,7},{2,0},{3,1},{4,2},{5,3},{6,4},{7,5},{8,14},{9,15},{10,... | collective-permute-start | bytes 1253384 | tf_op jit(solution)/shard_map/ppermute | solution.py:449
  91.4 0.7 copy-start.13
  92.1 0.7 copy-start.14
  101.4 23.3 %collective-permute-start = (bf16[64,2176]{1,0:T(8,128)(2,1)S(1)}, bf16[64,2176]{1,0:T(8,128)(2,1)S(1)}, u32[]{:S(2)}, u32[]{:S(2)}) collective-permute-start(bf16[64,2176]{1,0:T(8,128)(2,1)S(1)} %get-tuple-element.47), channel_id=1, source_target_pairs={{0,8},{8,0},{16,24},{24,16},{1,9},{9,1},{17,25},{25,17},{2,10},{10... | collective-permute-start | bytes 835592 | tf_op jit(solution)/shard_map/ppermute | solution.py:442
  102.8 0.7 copy-start.2
  103.5 0.6 copy-start.10
  118.3 7.8 %collective-permute-start.19 = (bf16[64,2176]{1,0:T(8,128)(2,1)S(1)}, bf16[64,2176]{1,0:T(8,128)(2,1)S(1)}, u32[]{:S(2)}, u32[]{:S(2)}) collective-permute-start(bf16[64,2176]{1,0:T(8,128)(2,1)S(1)} %get-tuple-element.65), channel_id=1, source_target_pairs={{0,8},{8,0},{16,24},{24,16},{1,9},{9,1},{17,25},{25,17},{2,10},{10... | collective-permute-start | bytes 835592 | tf_op jit(solution)/shard_map/ppermute | solution.py:442
  120.4 0.7 copy-start.6
  121.2 0.6 copy-start.8
  121.8 16.0 %collective-permute-start.20 = (bf16[64,2176]{1,0:T(8,128)(2,1)}, bf16[64,2176]{1,0:T(8,128)(2,1)}, u32[]{:S(2)}, u32[]{:S(2)}) collective-permute-start(bf16[64,2176]{1,0:T(8,128)(2,1)} %get-tuple-element.66), channel_id=1, source_target_pairs={{0,16},{8,24},{16,0},{24,8},{1,17},{9,25},{17,1},{25,9},{2,18},{10... | collective-permute-start | bytes 835592 | tf_op jit(solution)/shard_map/ppermute | solution.py:442
  122.5 16.6 %collective-permute-start.21 = (bf16[64,2176]{1,0:T(8,128)(2,1)}, bf16[64,2176]{1,0:T(8,128)(2,1)}, u32[]{:S(2)}, u32[]{:S(2)}) collective-permute-start(bf16[64,2176]{1,0:T(8,128)(2,1)} %get-tuple-element.67), channel_id=1, source_target_pairs={{0,24},{8,16},{16,8},{24,0},{1,25},{9,17},{17,9},{25,1},{2,26},{10... | collective-permute-start | bytes 835592 | tf_op jit(solution)/shard_map/ppermute | solution.py:442
  124.7 17.6 %collective-permute-start.22 = (bf16[64,2176]{1,0:T(8,128)(2,1)}, bf16[64,2176]{1,0:T(8,128)(2,1)}, u32[]{:S(2)}, u32[]{:S(2)}) collective-permute-start(bf16[64,2176]{1,0:T(8,128)(2,1)} %get-tuple-element.69), channel_id=1, source_target_pairs={{0,8},{8,0},{16,24},{24,16},{1,9},{9,1},{17,25},{25,17},{2,10},{10... | collective-permute-start | bytes 835592 | tf_op jit(solution)/shard_map/ppermute | solution.py:442
  125.3 29.6 %collective-permute-start.23 = (bf16[64,2176]{1,0:T(8,128)(2,1)}, bf16[64,2176]{1,0:T(8,128)(2,1)}, u32[]{:S(2)}, u32[]{:S(2)}) collective-permute-start(bf16[64,2176]{1,0:T(8,128)(2,1)} %get-tuple-element.70), channel_id=1, source_target_pairs={{0,16},{8,24},{16,0},{24,8},{1,17},{9,25},{17,1},{25,9},{2,18},{10... | collective-permute-start | bytes 835592 | tf_op jit(solution)/shard_map/ppermute | solution.py:442
  126.2 0.7 copy-start.4
  126.9 29.2 %collective-permute-start.24 = (bf16[64,2176]{1,0:T(8,128)(2,1)}, bf16[64,2176]{1,0:T(8,128)(2,1)}, u32[]{:S(2)}, u32[]{:S(2)}) collective-permute-start(bf16[64,2176]{1,0:T(8,128)(2,1)} %get-tuple-element.71), channel_id=1, source_target_pairs={{0,24},{8,16},{16,8},{24,0},{1,25},{9,17},{17,9},{25,1},{2,26},{10... | collective-permute-start | bytes 835592 | tf_op jit(solution)/shard_map/ppermute | solution.py:442
  137.7 32.3 %collective-permute-start.1 = (bf16[64,2176]{1,0:T(8,128)(2,1)}, bf16[64,2176]{1,0:T(8,128)(2,1)S(1)}, u32[]{:S(2)}, u32[]{:S(2)}) collective-permute-start(bf16[64,2176]{1,0:T(8,128)(2,1)} %copy-done.14), channel_id=1, source_target_pairs={{0,16},{8,24},{16,0},{24,8},{1,17},{9,25},{17,1},{25,9},{2,18},{10... | collective-permute-start | bytes 835592 | tf_op jit(solution)/shard_map/ppermute | solution.py:442
  139.1 31.3 %collective-permute-start.2 = (bf16[64,2176]{1,0:T(8,128)(2,1)}, bf16[64,2176]{1,0:T(8,128)(2,1)S(1)}, u32[]{:S(2)}, u32[]{:S(2)}) collective-permute-start(bf16[64,2176]{1,0:T(8,128)(2,1)} %copy-done.13), channel_id=1, source_target_pairs={{0,24},{8,16},{16,8},{24,0},{1,25},{9,17},{17,9},{25,1},{2,26},{10... | collective-permute-start | bytes 835592 | tf_op jit(solution)/shard_map/ppermute | solution.py:442
  142.3 29.4 %collective-permute-start.4 = (bf16[64,2176]{1,0:T(8,128)(2,1)S(1)}, bf16[64,2176]{1,0:T(8,128)(2,1)S(1)}, u32[]{:S(2)}, u32[]{:S(2)}) collective-permute-start(bf16[64,2176]{1,0:T(8,128)(2,1)S(1)} %get-tuple-element.51), channel_id=1, source_target_pairs={{0,8},{8,0},{16,24},{24,16},{1,9},{9,1},{17,25},{25,17},{2,10},{10... | collective-permute-start | bytes 835592 | tf_op jit(solution)/shard_map/ppermute | solution.py:442
  154.9 20.6 %collective-permute-start.5 = (bf16[64,2176]{1,0:T(8,128)(2,1)S(1)}, bf16[64,2176]{1,0:T(8,128)(2,1)S(1)}, u32[]{:S(2)}, u32[]{:S(2)}) collective-permute-start(bf16[64,2176]{1,0:T(8,128)(2,1)S(1)} %get-tuple-element.52), channel_id=1, source_target_pairs={{0,16},{8,24},{16,0},{24,8},{1,17},{9,25},{17,1},{25,9},{2,18},{10... | collective-permute-start | bytes 835592 | tf_op jit(solution)/shard_map/ppermute | solution.py:442
  156.1 20.8 %collective-permute-start.6 = (bf16[64,2176]{1,0:T(8,128)(2,1)S(1)}, bf16[64,2176]{1,0:T(8,128)(2,1)S(1)}, u32[]{:S(2)}, u32[]{:S(2)}) collective-permute-start(bf16[64,2176]{1,0:T(8,128)(2,1)S(1)} %get-tuple-element.53), channel_id=1, source_target_pairs={{0,24},{8,16},{16,8},{24,0},{1,25},{9,17},{17,9},{25,1},{2,26},{10... | collective-permute-start | bytes 835592 | tf_op jit(solution)/shard_map/ppermute | solution.py:442
  158.0 1.0 copy-start.3
  159.0 1.0 copy-start.5
  159.9 1.0 copy-start.7
  170.1 9.2 %collective-permute-start.29 = (bf16[64,2048]{1,0:T(8,128)(2,1)S(1)}, bf16[64,2048]{1,0:T(8,128)(2,1)S(1)}, u32[]{:S(2)}, u32[]{:S(2)}) collective-permute-start(bf16[64,2048]{1,0:T(8,128)(2,1)S(1)} %get-tuple-element.78), channel_id=1, source_target_pairs={{0,8},{8,0},{16,24},{24,16},{1,9},{9,1},{17,25},{25,17},{2,10},{10... | collective-permute-start | bytes 786440 | tf_op jit(solution)/shard_map/ppermute | solution.py:442
  170.5 17.7 %collective-permute-start.30 = (bf16[64,2048]{1,0:T(8,128)(2,1)S(1)}, bf16[64,2048]{1,0:T(8,128)(2,1)S(1)}, u32[]{:S(2)}, u32[]{:S(2)}) collective-permute-start(bf16[64,2048]{1,0:T(8,128)(2,1)S(1)} %get-tuple-element.79), channel_id=1, source_target_pairs={{0,16},{8,24},{16,0},{24,8},{1,17},{9,25},{17,1},{25,9},{2,18},{10... | collective-permute-start | bytes 786440 | tf_op jit(solution)/shard_map/ppermute | solution.py:442
  171.7 18.2 %collective-permute-start.31 = (bf16[64,2048]{1,0:T(8,128)(2,1)S(1)}, bf16[64,2048]{1,0:T(8,128)(2,1)S(1)}, u32[]{:S(2)}, u32[]{:S(2)}) collective-permute-start(bf16[64,2048]{1,0:T(8,128)(2,1)S(1)} %get-tuple-element.80), channel_id=1, source_target_pairs={{0,24},{8,16},{16,8},{24,0},{1,25},{9,17},{17,9},{25,1},{2,26},{10... | collective-permute-start | bytes 786440 | tf_op jit(solution)/shard_map/ppermute | solution.py:442
  175.5 15.3 %collective-permute-start.25 = (bf16[64,2048]{1,0:T(8,128)(2,1)S(1)}, bf16[64,2048]{1,0:T(8,128)(2,1)S(1)}, u32[]{:S(2)}, u32[]{:S(2)}) collective-permute-start(bf16[64,2048]{1,0:T(8,128)(2,1)S(1)} %get-tuple-element.73), channel_id=1, source_target_pairs={{0,8},{8,0},{16,24},{24,16},{1,9},{9,1},{17,25},{25,17},{2,10},{10... | collective-permute-start | bytes 786440 | tf_op jit(solution)/shard_map/ppermute | solution.py:442
  176.8 21.1 %collective-permute-start.26 = (bf16[64,2048]{1,0:T(8,128)(2,1)S(1)}, bf16[64,2048]{1,0:T(8,128)(2,1)S(1)}, u32[]{:S(2)}, u32[]{:S(2)}) collective-permute-start(bf16[64,2048]{1,0:T(8,128)(2,1)S(1)} %get-tuple-element.74), channel_id=1, source_target_pairs={{0,16},{8,24},{16,0},{24,8},{1,17},{9,25},{17,1},{25,9},{2,18},{10... | collective-permute-start | bytes 786440 | tf_op jit(solution)/shard_map/ppermute | solution.py:442
  179.3 20.3 %collective-permute-start.27 = (bf16[64,2048]{1,0:T(8,128)(2,1)S(1)}, bf16[64,2048]{1,0:T(8,128)(2,1)S(1)}, u32[]{:S(2)}, u32[]{:S(2)}) collective-permute-start(bf16[64,2048]{1,0:T(8,128)(2,1)S(1)} %get-tuple-element.75), channel_id=1, source_target_pairs={{0,24},{8,16},{16,8},{24,0},{1,25},{9,17},{17,9},{25,1},{2,26},{10... | collective-permute-start | bytes 786440 | tf_op jit(solution)/shard_map/ppermute | solution.py:442
  180.3 19.0 %copy-start.11 = (bf16[96,256]{1,0:T(8,128)(2,1)S(1)}, bf16[96,256]{1,0:T(8,128)(2,1)}, u32[]{:S(2)}) copy-start(bf16[96,256]{1,0:T(8,128)(2,1)} %copy-done.10) | copy-start | bytes 147460
  180.3 28.0 %copy-start.9 = (bf16[96,256]{1,0:T(8,128)(2,1)S(1)}, bf16[96,256]{1,0:T(8,128)(2,1)}, u32[]{:S(2)}) copy-start(bf16[96,256]{1,0:T(8,128)(2,1)} %copy-done.8) | copy-start | bytes 147460
  188.2 20.4 %collective-permute-start.13 = (bf16[64,2048]{1,0:T(8,128)(2,1)S(1)}, bf16[64,2048]{1,0:T(8,128)(2,1)S(1)}, u32[]{:S(2)}, u32[]{:S(2)}) collective-permute-start(bf16[64,2048]{1,0:T(8,128)(2,1)S(1)} %get-tuple-element.60), channel_id=1, source_target_pairs={{0,8},{8,0},{16,24},{24,16},{1,9},{9,1},{17,25},{25,17},{2,10},{10... | collective-permute-start | bytes 786440 | tf_op jit(solution)/shard_map/ppermute | solution.py:442
  189.9 18.8 %collective-permute-start.14 = (bf16[64,2048]{1,0:T(8,128)(2,1)S(1)}, bf16[64,2048]{1,0:T(8,128)(2,1)S(1)}, u32[]{:S(2)}, u32[]{:S(2)}) collective-permute-start(bf16[64,2048]{1,0:T(8,128)(2,1)S(1)} %get-tuple-element.61), channel_id=1, source_target_pairs={{0,16},{8,24},{16,0},{24,8},{1,17},{9,25},{17,1},{25,9},{2,18},{10... | collective-permute-start | bytes 786440 | tf_op jit(solution)/shard_map/ppermute | solution.py:442
  190.8 17.9 %collective-permute-start.15 = (bf16[64,2048]{1,0:T(8,128)(2,1)S(1)}, bf16[64,2048]{1,0:T(8,128)(2,1)S(1)}, u32[]{:S(2)}, u32[]{:S(2)}) collective-permute-start(bf16[64,2048]{1,0:T(8,128)(2,1)S(1)} %get-tuple-element.62), channel_id=1, source_target_pairs={{0,24},{8,16},{16,8},{24,0},{1,25},{9,17},{17,9},{25,1},{2,26},{10... | collective-permute-start | bytes 786440 | tf_op jit(solution)/shard_map/ppermute | solution.py:442
  197.9 15.0 %collective-permute-start.10 = (bf16[64,2048]{1,0:T(8,128)(2,1)S(1)}, bf16[64,2048]{1,0:T(8,128)(2,1)S(1)}, u32[]{:S(2)}, u32[]{:S(2)}) collective-permute-start(bf16[64,2048]{1,0:T(8,128)(2,1)S(1)} %get-tuple-element.55), channel_id=1, source_target_pairs={{0,8},{8,0},{16,24},{24,16},{1,9},{9,1},{17,25},{25,17},{2,10},{10... | collective-permute-start | bytes 786440 | tf_op jit(solution)/shard_map/ppermute | solution.py:442
  199.6 21.6 %collective-permute-start.32 = (bf16[96,2048]{1,0:T(8,128)(2,1)S(1)}, bf16[96,2048]{1,0:T(8,128)(2,1)S(1)}, u32[]{:S(2)}, u32[]{:S(2)}) collective-permute-start(bf16[96,2048]{1,0:T(8,128)(2,1)S(1)} %merge.7), channel_id=1, source_target_pairs={{0,6},{1,7},{2,0},{3,1},{4,2},{5,3},{6,4},{7,5},{8,14},{9,15},{10,... | collective-permute-start | bytes 1179656 | tf_op jit(solution)/shard_map/ppermute | solution.py:467
  208.6 23.6 %collective-permute-start.28 = (bf16[96,2048]{1,0:T(8,128)(2,1)S(1)}, bf16[96,2048]{1,0:T(8,128)(2,1)S(1)}, u32[]{:S(2)}, u32[]{:S(2)}) collective-permute-start(bf16[96,2048]{1,0:T(8,128)(2,1)S(1)} %merge.6), channel_id=1, source_target_pairs={{0,4},{1,5},{2,6},{3,7},{4,0},{5,1},{6,2},{7,3},{8,12},{9,13},{10,... | collective-permute-start | bytes 1179656 | tf_op jit(solution)/shard_map/ppermute | solution.py:467
  209.0 23.2 %collective-permute-start.16 = (bf16[96,2048]{1,0:T(8,128)(2,1)S(1)}, bf16[96,2048]{1,0:T(8,128)(2,1)S(1)}, u32[]{:S(2)}, u32[]{:S(2)}) collective-permute-start(bf16[96,2048]{1,0:T(8,128)(2,1)S(1)} %merge.5), channel_id=1, source_target_pairs={{0,2},{1,3},{2,4},{3,5},{4,6},{5,7},{6,0},{7,1},{8,10},{9,11},{10,... | collective-permute-start | bytes 1179656 | tf_op jit(solution)/shard_map/ppermute | solution.py:467
  211.8 9.2 %collective-permute-start.11 = (bf16[64,2048]{1,0:T(8,128)(2,1)S(1)}, bf16[64,2048]{1,0:T(8,128)(2,1)S(1)}, u32[]{:S(2)}, u32[]{:S(2)}) collective-permute-start(bf16[64,2048]{1,0:T(8,128)(2,1)S(1)} %get-tuple-element.56), channel_id=1, source_target_pairs={{0,16},{8,24},{16,0},{24,8},{1,17},{9,25},{17,1},{25,9},{2,18},{10... | collective-permute-start | bytes 786440 | tf_op jit(solution)/shard_map/ppermute | solution.py:442
  212.9 8.0 %collective-permute-start.12 = (bf16[64,2048]{1,0:T(8,128)(2,1)S(1)}, bf16[64,2048]{1,0:T(8,128)(2,1)S(1)}, u32[]{:S(2)}, u32[]{:S(2)}) collective-permute-start(bf16[64,2048]{1,0:T(8,128)(2,1)S(1)} %get-tuple-element.57), channel_id=1, source_target_pairs={{0,24},{8,16},{16,8},{24,0},{1,25},{9,17},{17,9},{25,1},{2,26},{10... | collective-permute-start | bytes 786440 | tf_op jit(solution)/shard_map/ppermute | solution.py:442

commit v3 on v2

--- a/solution.py
+++ b/solution.py
@@ -9,37 +9,19 @@
 from jax.sharding import PartitionSpec as P
 
 LANES = 128
-OWNERS_PER_TILE = 4
+KEY_TILE = 256
 
 
 def attention_kernel(
-    part_ref,
-    lam_ref,
-    gain_ref,
-    rows_ref,
-    out_ref,
-    stack_ref,
-    score_ref,
-    acc_ref,
-    top_ref,
-    *,
-    sub,
-    key_rows,
-    parts,
-    scale,
+    part_ref, lam_ref, gain_ref, rows_ref, out_ref, stack_ref, acc_ref, top_ref, *, sub, parts, scale
 ):
+    exact = math.frexp(scale)[0] == 0.5
     tile = pl.program_id(0)
-    exact = math.frexp(scale)[0] == 0.5
-    tile_rows = OWNERS_PER_TILE * sub
-    span = tile_rows * parts
-    width = rows_ref.shape[2]
+    tile_rows, width = out_ref.shape
+    key_rows = tile_rows * parts
     half = width // 2
-    query_rows = key_rows // parts
-    tiles_per_source = key_rows // span
-
-    source = tile // tiles_per_source
-    start = pl.multiple_of((tile % tiles_per_source) * tile_rows, tile_rows)
-    query = rows_ref[source, pl.ds(start, tile_rows), :]
+
+    query = rows_ref[tile, 0:tile_rows, :]
     if exact:
         query = (query.astype(jnp.float32) * scale).astype(jnp.bfloat16)
     low = lax.broadcasted_iota(jnp.int32, (tile_rows, width), 1) < half
@@ -48,61 +30,61 @@
     stack_ref[tile_rows:, :] = jnp.where(low, nothing, query)
     top_ref[...] = jnp.full_like(top_ref, -1e30)
     acc_ref[...] = jnp.zeros_like(acc_ref)
-    ones = jnp.ones((span, LANES), jnp.bfloat16)
-
-    def place_of(index, base):
-        offset = pl.multiple_of((index % tiles_per_source) * span, span)
-        return index // tiles_per_source, pl.ds(base + offset, span)
-
-    def score(index):
-        owner, place = place_of(index, query_rows)
+
+    def absorb(source, first, count, keys, masked_from=None):
+        place = pl.ds(first, count)
         scores = lax.dot_general(
-            stack_ref[...],
-            rows_ref[owner, place, :],
+            stack_ref[place, :],
+            rows_ref[source, pl.ds(tile_rows, keys), :],
             (((1,), (1,)), ((), ())),
             preferred_element_type=jnp.float32,
         )
-        return scores if exact else scores * scale
-
-    def absorb(index, scores):
-        owner, place = place_of(index, query_rows + key_rows)
-        before = top_ref[...]
+        if not exact:
+            scores = scores * scale
+        if masked_from is not None:
+            row = lax.broadcasted_iota(jnp.int32, (count, LANES), 0) + masked_from
+            where = row + part_ref[0] * sub
+            for step in range(1, tile_rows // sub):
+                if masked_from < (step + 1) * sub and masked_from + count > step * sub:
+                    where = where + jnp.where(row >= step * sub, (parts - 1) * sub, 0)
+                elif masked_from >= step * sub:
+                    where = where + (parts - 1) * sub
+            gap = where - lax.broadcasted_iota(jnp.int32, (count, LANES), 1)
+            scores = jnp.concatenate(
+                [
+                    jnp.where(gap >= start, scores[:, start : start + LANES], -jnp.inf)
+                    for start in range(0, keys, LANES)
+                ],
+                axis=1,
+            )
+        before = top_ref[place, :]
         after = jnp.maximum(before, jnp.max(scores, axis=1, keepdims=True))
         decay = jnp.exp(before - after)
-        weights = jnp.exp(scores - jnp.concatenate([after] * (span // LANES), axis=1))
-        top_ref[...] = after
-        acc_ref[...] = acc_ref[...] * jnp.concatenate(
+        weights = jnp.exp(scores - jnp.concatenate([after] * (keys // LANES), axis=1))
+        top_ref[place, :] = after
+        values = rows_ref[source, pl.ds(tile_rows + key_rows, keys), :]
+        acc_ref[place, :] = acc_ref[place, :] * jnp.concatenate(
             [decay] * (1 + width // LANES), axis=1
         ) + jnp.dot(
             weights.astype(jnp.bfloat16),
-            jnp.concatenate([rows_ref[owner, place, :], ones], axis=1),
+            jnp.concatenate([values, jnp.ones((keys, LANES), jnp.bfloat16)], axis=1),
             preferred_element_type=jnp.float32,
         )
 
-    score_ref[0] = score(0)
+    chunk = tile_rows // 2
 
     @pl.loop(0, tile)
-    def _(index):
-        score_ref[(index + 1) % 2] = score(index + 1)
-        absorb(index, score_ref[index % 2])
-
-    scores = score_ref[tile % 2]
-    row = lax.broadcasted_iota(jnp.int32, (tile_rows, LANES), 0)
-    place = row + part_ref[0] * sub
-    for step in range(1, OWNERS_PER_TILE):
-        place = place + jnp.where(row >= step * sub, (parts - 1) * sub, 0)
-    gap = place - lax.broadcasted_iota(jnp.int32, (tile_rows, LANES), 1)
-    gap = jnp.concatenate([gap, gap], axis=0)
-    absorb(
-        tile,
-        jnp.concatenate(
-            [
-                jnp.where(gap >= first, scores[:, first : first + LANES], -jnp.inf)
-                for first in range(0, span, LANES)
-            ],
-            axis=1,
-        ),
-    )
+    def _(source):
+        for first in range(0, 2 * tile_rows, chunk):
+            absorb(source, first, chunk, key_rows)
+
+    needed = [
+        -(-(owner + 1) * sub * parts // KEY_TILE) * KEY_TILE for owner in range(tile_rows // sub)
+    ]
+    for keys in sorted(set(needed)):
+        owners = [owner for owner in range(len(needed)) if needed[owner] == keys]
+        for base in (0, tile_rows):
+            absorb(tile, base + owners[0] * sub, len(owners) * sub, keys, owners[0] * sub)
 
     first = acc_ref[0:tile_rows, :]
     second = acc_ref[tile_rows:, :]
@@ -111,16 +93,13 @@
     out_ref[...] = (scaled * gain_ref[...]).astype(out_ref.dtype)
 
 
-def attention(part, lam, gain, arrived, sub, key_rows, parts, scale):
+def attention(part, lam, gain, arrived, sub, tile_rows, parts, scale):
     sources, _, width = arrived.shape
-    tile_rows = OWNERS_PER_TILE * sub
-    total_rows = sources * key_rows // parts
-    pairs = total_rows * sources * key_rows
+    total_rows = sources * tile_rows
+    pairs = total_rows * total_rows * parts
     return pl.pallas_call(
-        functools.partial(
-            attention_kernel, sub=sub, key_rows=key_rows, parts=parts, scale=scale
-        ),
-        grid=(total_rows // tile_rows,),
+        functools.partial(attention_kernel, sub=sub, parts=parts, scale=scale),
+        grid=(sources,),
         out_shape=jax.ShapeDtypeStruct((total_rows, width), jnp.bfloat16),
         in_specs=[
             pl.BlockSpec(memory_space=pltpu.SMEM),
@@ -131,11 +110,10 @@
         out_specs=pl.BlockSpec((tile_rows, width), lambda i: (i, 0)),
         scratch_shapes=[
             pltpu.VMEM((2 * tile_rows, width), jnp.bfloat16),
-            pltpu.VMEM((2, 2 * tile_rows, tile_rows * parts), jnp.float32),
             pltpu.VMEM((2 * tile_rows, width + LANES), jnp.float32),
             pltpu.VMEM((2 * tile_rows, LANES), jnp.float32),
         ],
-        compiler_params=pltpu.CompilerParams(vmem_limit_bytes=12 * 1024 * 1024),
+        compiler_params=pltpu.CompilerParams(vmem_limit_bytes=20 * 1024 * 1024),
         cost_estimate=pl.CostEstimate(
             flops=8 * pairs * width, bytes_accessed=2 * arrived.size, transcendentals=pairs
         ),
@@ -143,69 +121,70 @@
     )(part, lam, gain, arrived)
 
 
-def project_kernel(heads_ref, weight_ref, residual_ref, gain_ref, routes_ref, updated_ref, normed_ref, acc_ref, *, parts):
-    step = pl.program_id(0)
-    held = heads_ref.shape[0] // parts
-    left = jnp.concatenate(
-        [
-            jnp.concatenate([heads_ref[part * held + head, 0] for head in range(held)], axis=1)
-            for part in range(parts)
-        ],
-        axis=0,
-    )
-    product = jnp.dot(left, weight_ref[...], preferred_element_type=jnp.float32)
-
-    @pl.when(step == 0)
-    def _():
-        acc_ref[...] = residual_ref[...].astype(jnp.float32) + product
-
-    @pl.when(step > 0)
-    def _():
-        acc_ref[...] += product
-
-    @pl.when(step == pl.num_programs(0) - 1)
-    def _():
-        updated = acc_ref[...].astype(jnp.bfloat16)
-        updated_ref[...] = updated
-        wide = updated.astype(jnp.float32)
-        scaled = wide * lax.rsqrt(jnp.mean(wide * wide, axis=1, keepdims=True) + 1e-06)
-        model = wide.shape[1]
-        normed_ref[:, :model] = (scaled * gain_ref[...]).astype(jnp.bfloat16)
-        normed_ref[:, model:] = routes_ref[...]
+def project_kernel(
+    heads_ref, weight_ref, residual_ref, gain_ref, routes_ref, updated_ref, normed_ref, left_ref, kept_ref, acc_ref, sems, *, parts
+):
+    sources, columns, sub, width = heads_ref.shape
+    held = sources // parts
+    depth = held * width
+    copies = [
+        pltpu.make_async_copy(
+            weight_ref.at[pl.ds(column * depth, depth)], kept_ref.at[column], sems.at[column]
+        )
+        for column in range(columns)
+    ]
+    for copy in copies:
+        copy.start()
+    for part in range(parts):
+        for column in range(columns):
+            for head in range(held):
+                left_ref[
+                    column, part * sub : (part + 1) * sub, head * width : (head + 1) * width
+                ] = heads_ref[part * held + head, column]
+    for column, copy in enumerate(copies):
+        copy.wait()
+        product = jnp.dot(left_ref[column], kept_ref[column], preferred_element_type=jnp.float32)
+        if column == 0:
+            acc_ref[...] = residual_ref[...].astype(jnp.float32) + product
+        else:
+            acc_ref[...] += product
+    updated = acc_ref[...].astype(jnp.bfloat16)
+    updated_ref[...] = updated
+    wide = updated.astype(jnp.float32)
+    scaled = wide * lax.rsqrt(jnp.mean(wide * wide, axis=1, keepdims=True) + 1e-06)
+    model = wide.shape[1]
+    normed_ref[:, :model] = (scaled * gain_ref[...]).astype(jnp.bfloat16)
+    normed_ref[:, model:] = routes_ref[...]
 
 
 def project(heads, out_weight, residual, gain, routes, parts):
-    sources, columns, sub, width = heads.shape
+    sources, columns, _, width = heads.shape
     rows, model = residual.shape
     depth = sources // parts * width
+    whole = pl.BlockSpec(memory_space=pltpu.VMEM)
     return pl.pallas_call(
         functools.partial(project_kernel, parts=parts),
-        grid=(columns,),
         out_shape=(
             jax.ShapeDtypeStruct((rows, model), jnp.bfloat16),
             jax.ShapeDtypeStruct((rows, model + LANES), jnp.bfloat16),
         ),
-        in_specs=[
-            pl.BlockSpec((sources, 1, sub, width), lambda i: (0, i, 0, 0)),
-            pl.BlockSpec((depth, model), lambda i: (i, 0)),
-            pl.BlockSpec((rows, model), lambda i: (0, 0)),
-            pl.BlockSpec((1, model), lambda i: (0, 0)),
-            pl.BlockSpec((rows, LANES), lambda i: (0, 0)),
+        in_specs=[whole, pl.BlockSpec(memory_space=pl.ANY), whole, whole, whole],
+        out_specs=(whole, whole),
+        scratch_shapes=[
+            pltpu.VMEM((columns, rows, depth), jnp.bfloat16),
+            pltpu.VMEM((columns, depth, model), jnp.bfloat16),
+            pltpu.VMEM((rows, model), jnp.float32),
+            pltpu.SemaphoreType.DMA((columns,)),
         ],
-        out_specs=(
-            pl.BlockSpec((rows, model), lambda i: (0, 0)),
-            pl.BlockSpec((rows, model + LANES), lambda i: (0, 0)),
-        ),
-        scratch_shapes=[pltpu.VMEM((rows, model), jnp.float32)],
-        compiler_params=pltpu.CompilerParams(vmem_limit_bytes=48 * 1024 * 1024),
+        compiler_params=pltpu.CompilerParams(vmem_limit_bytes=56 * 1024 * 1024),
         cost_estimate=pl.CostEstimate(
-            flops=2 * rows * model * columns * depth, bytes_accessed=2 * out_weight.size, transcendentals=0
+            flops=2 * rows * out_weight.size, bytes_accessed=2 * out_weight.size, transcendentals=0
         ),
         name="project",
     )(heads, out_weight, residual, gain, routes)
 
 
-def choose_kernel(place_ref, block_ref, chosen_ref, *out_refs, held, experts, capacity):
+def choose_kernel(place_ref, block_ref, coarse_ref, fine_ref, *out_refs, held, experts, capacity):
     model = block_ref.shape[1] - LANES
     slots = len(out_refs) * held * capacity
     source = lax.broadcasted_iota(jnp.int32, (LANES, slots), 0)
@@ -216,15 +195,22 @@
             first = (column * held + expert) * capacity
             name = jnp.bitwise_xor(place_ref[0], column) * held + expert
             inside = (slot >= first) & (slot < first + capacity)
-            wanted = jnp.where(inside, 2 * experts + name, wanted)
-    table = jnp.where(source == wanted, 1.0, 0.0).astype(jnp.bfloat16)
-    ranks = jnp.dot(block_ref[:, model:], table, preferred_element_type=jnp.float32)
+            wanted = jnp.where(inside, name, wanted)
+
+    def looked_up(group):
+        table = jnp.where(source == wanted + group * experts, 1.0, 0.0).astype(jnp.bfloat16)
+        return jnp.dot(block_ref[:, model:], table, preferred_element_type=jnp.float32)
+
+    ranks = looked_up(2)
     lane = lax.broadcasted_iota(jnp.int32, ranks.shape, 1)
-    order = lax.rem(lane, capacity).astype(jnp.float32)
-    chosen = jnp.where(ranks == order, 1.0, 0.0).astype(jnp.bfloat16)
-    chosen_ref[...] = chosen
+    hit = ranks == lax.rem(lane, capacity).astype(jnp.float32)
+    coarse_ref[...] = jnp.where(hit, looked_up(0), 0.0).astype(jnp.bfloat16)
+    fine_ref[...] = jnp.where(hit, looked_up(1), 0.0).astype(jnp.bfloat16)
     rows = lax.dot_general(
-        chosen, block_ref[...], (((0,), (0,)), ((), ())), preferred_element_type=jnp.float32
+        jnp.where(hit, 1.0, 0.0).astype(jnp.bfloat16),
+        block_ref[:, :model],
+        (((0,), (0,)), ((), ())),
+        preferred_element_type=jnp.float32,
     ).astype(jnp.bfloat16)
     for column, out_ref in enumerate(out_refs):
         out_ref[...] = rows[column * held * capacity : (column + 1) * held * capacity]
@@ -234,14 +220,16 @@
     rows, width = block.shape
     slots = held * capacity
     whole = pl.BlockSpec(memory_space=pltpu.VMEM)
+    table = jax.ShapeDtypeStruct((rows, columns * slots), jnp.bfloat16)
     return pl.pallas_call(
         functools.partial(choose_kernel, held=held, experts=experts, capacity=capacity),
         out_shape=(
-            jax.ShapeDtypeStruct((rows, columns * slots), jnp.bfloat16),
-            *(jax.ShapeDtypeStruct((slots, width), jnp.bfloat16) for _ in range(columns)),
+            table,
+            table,
+            *(jax.ShapeDtypeStruct((slots, width - LANES), jnp.bfloat16) for _ in range(columns)),
         ),
         in_specs=[pl.BlockSpec(memory_space=pltpu.SMEM), whole],
-        out_specs=(whole,) * (columns + 1),
+        out_specs=(whole,) * (columns + 2),
         compiler_params=pltpu.CompilerParams(vmem_limit_bytes=16 * 1024 * 1024),
         cost_estimate=pl.CostEstimate(
             flops=2 * rows * width * columns * slots, bytes_accessed=4 * rows * width, transcendentals=0
@@ -250,41 +238,41 @@
     )(place, block)
 
 
-def merge_kernel(chosen_ref, *refs):
+def merge_kernel(coarse_ref, fine_ref, *refs):
     out_ref, kept_ref = refs[-2:]
     slots = refs[0].shape[0]
     for column, ref in enumerate(refs[:-2]):
         kept_ref[column * slots : (column + 1) * slots, :] = ref[...]
-    total = jnp.dot(chosen_ref[...], kept_ref[...], preferred_element_type=jnp.float32)
+    kept = kept_ref[...]
+    total = jnp.dot(coarse_ref[...], kept, preferred_element_type=jnp.float32)
+    total += jnp.dot(fine_ref[...], kept, preferred_element_type=jnp.float32)
     out_ref[...] = total.astype(out_ref.dtype)
 
 
-def merge(chosen, parts):
-    rows = chosen.shape[0]
+def merge(coarse, fine, parts):
+    rows = coarse.shape[0]
     model = parts[0].shape[1]
     whole = pl.BlockSpec(memory_space=pltpu.VMEM)
     return pl.pallas_call(
         merge_kernel,
         out_shape=jax.ShapeDtypeStruct((rows, model), jnp.bfloat16),
-        in_specs=[whole] * (1 + len(parts)),
+        in_specs=[whole] * (2 + len(parts)),
         out_specs=whole,
-        scratch_shapes=[pltpu.VMEM((chosen.shape[1], model), jnp.bfloat16)],
+        scratch_shapes=[pltpu.VMEM((coarse.shape[1], model), jnp.bfloat16)],
         compiler_params=pltpu.CompilerParams(vmem_limit_bytes=16 * 1024 * 1024),
         cost_estimate=pl.CostEstimate(
-            flops=2 * rows * chosen.shape[1] * model, bytes_accessed=4 * rows * model, transcendentals=0
+            flops=4 * rows * coarse.shape[1] * model, bytes_accessed=4 * rows * model, transcendentals=0
         ),
         name="merge",
-    )(chosen, *parts)
-
-
-def expert_kernel(*refs, blocks, experts):
-    first_ref = refs[0]
-    block_refs = refs[1 : 1 + blocks]
-    weight_refs = refs[1 + blocks : 7 + blocks]
-    out_refs = refs[7 + blocks : 7 + 2 * blocks]
-    kept_refs = refs[7 + 2 * blocks : 13 + 2 * blocks]
-    rows_ref, sems = refs[13 + 2 * blocks :]
-    model = rows_ref.shape[2] - LANES
+    )(coarse, fine, *parts)
+
+
+def expert_kernel(*refs, blocks):
+    block_refs = refs[:blocks]
+    weight_refs = refs[blocks : 6 + blocks]
+    out_refs = refs[6 + blocks : 6 + 2 * blocks]
+    kept_refs = refs[6 + 2 * blocks : 12 + 2 * blocks]
+    rows_ref, sems = refs[12 + 2 * blocks :]
     held = kept_refs[0].shape[0]
     capacity = block_refs[0].shape[0] // held
     sets = ((0, 1, 2), (3, 4, 5))
@@ -306,13 +294,7 @@
             ]
 
     for expert in range(held):
-        routes = rows_ref[expert, :, model:].astype(jnp.float32)
-        lane = lax.broadcasted_iota(jnp.int32, routes.shape, 1)
-        mine = first_ref[0] + expert
-        share = jnp.sum(
-            jnp.where((lane == mine) | (lane == mine + experts), routes, 0.0), axis=1, keepdims=True
-        )
-        rows = rows_ref[expert, :, :model]
+        rows = rows_ref[expert]
         total = None
         for indices in sets:
             parts = []
@@ -322,7 +304,7 @@
                     jnp.dot(rows, kept_refs[index][expert], preferred_element_type=jnp.float32)
                 )
             gate, up = parts
-            inner = (gate / (1.0 + jnp.exp(-gate)) * up * share).astype(jnp.bfloat16)
+            inner = (gate / (1.0 + jnp.exp(-gate)) * up).astype(jnp.bfloat16)
             copy(indices[2], expert).wait()
             term = jnp.dot(inner, kept_refs[indices[2]][expert], preferred_element_type=jnp.float32)
             total = term if total is None else total + term
@@ -333,21 +315,20 @@
             ]
 
 
-def expert_pass(first, blocks, weights, experts):
+def expert_pass(blocks, weights):
     held, model, hidden = weights[0].shape
     slots = blocks[0].shape[0]
     total = len(blocks) * slots
     whole = pl.BlockSpec(memory_space=pltpu.VMEM)
     return pl.pallas_call(
-        functools.partial(expert_kernel, blocks=len(blocks), experts=experts),
+        functools.partial(expert_kernel, blocks=len(blocks)),
         out_shape=tuple(jax.ShapeDtypeStruct((slots, model), jnp.bfloat16) for _ in blocks),
-        in_specs=[pl.BlockSpec(memory_space=pltpu.SMEM)]
-        + [whole] * len(blocks)
+        in_specs=[whole] * len(blocks)
         + [pl.BlockSpec(memory_space=pl.ANY)] * len(weights),
         out_specs=(whole,) * len(blocks),
         scratch_shapes=[pltpu.VMEM(w.shape, w.dtype) for w in weights]
         + [
-            pltpu.VMEM((held, total // held, model + LANES), jnp.bfloat16),
+            pltpu.VMEM((held, total // held, model), jnp.bfloat16),
             pltpu.SemaphoreType.DMA((len(weights), held)),
         ],
         compiler_params=pltpu.CompilerParams(vmem_limit_bytes=46 * 1024 * 1024),
@@ -357,7 +338,7 @@
             transcendentals=2 * total * hidden,
         ),
         name="experts",
-    )(first, *blocks, *weights)
+    )(*blocks, *weights)
 
 
 def balanced(
@@ -402,7 +383,7 @@
         head_gain.reshape(1, -1),
         arrived,
         sub,
-        tokens,
+        tokens // parts,
         parts,
         (width // 2) ** (-0.5),
     )
@@ -444,26 +425,25 @@
     layers = tp_count // 2
     capacity = row_capacity(rows, expert_ids.shape[1], experts)
     place = sp_index.reshape(1)
-    first = (sp_index * held).reshape(1)
     weights = (*mine, *other)
     blocks = [normed] + [lax.ppermute(normed, "tp", turn(-k)) for k in range(1, layers)]
     chosen, arrivals = [], []
     for block in blocks:
-        table, *sent = choose(place, block, sp_count, held, experts, capacity)
-        chosen.append(table)
+        coarse, fine, *sent = choose(place, block, sp_count, held, experts, capacity)
+        chosen.append((coarse, fine))
         arrivals.append([sent[0]] + [across(sent[c], c) for c in range(1, sp_count)])
     results = {}
     near = near_first(layers)
     for group in ((0, near[0]), near[1:]):
         rows_in = [block for k in group for block in arrivals[k]]
-        done = expert_pass(first, rows_in, weights, experts)
+        done = expert_pass(rows_in, weights)
         for i, k in enumerate(group):
             results[k] = done[i * sp_count : (i + 1) * sp_count]
     reduced = []
     for k in range(layers):
         result = results[k]
         back = [result[0]] + [across(result[c], c) for c in range(1, sp_count)]
-        reduced.append(merge(chosen[k], back))
+        reduced.append(merge(*chosen[k], back))
     returned = [lax.ppermute(reduced[k], "tp", turn(k)) for k in range(1, layers)]
     return summed_rows(updated, reduced[0], *returned)
 
@@ -621,12 +601,11 @@
     if sp_count != 4 or tp_count % 2 or tp_count < 6 or sp_count % heads or width != LANES:
         return False
     sub = rows // (sp_count // heads)
-    span = OWNERS_PER_TILE * rows
     capacity = row_capacity(rows, expert_ids.shape[1], held * sp_count)
     return (
         sub % 16 == 0
-        and tokens % span == 0
-        and span % LANES == 0
+        and tokens % KEY_TILE == 0
+        and tokens == rows * tp_count
         and capacity % 16 == 0
         and 3 * held * sp_count <= LANES
     )

time: 234 us -> 218 us (0.932)
  Pallas kernels: 56.4 us -> 41.1 us
  waiting for transfers between devices: 106 us -> 116 us
  local copies, waits for them, and re-layouts: 12.1 us -> 6.28 us
  starting transfers between devices: 55.3 us -> 50.8 us
    pallas_call x4, Pallas kernels: 50.9 us -> 36.8 us  [the longest x2 15.6 us: expert_pass(): pl.pallas_call(functools.partial(expert_kernel, blocks=len(blocks)), out_...]
    ppermute x3, waiting for transfers between devices: 22.8 us -> 30.5 us  [balanced(): lax.ppermute(normed, 'tp', turn(-k))]
    unnamed x38 -> x16, local copies, waits for them, and re-layouts: 7.67 us -> 1.77 us
    ppermute x24, starting transfers between devices: 29 us -> 25.5 us  [across(): return lax.ppermute(array, 'sp', [(i, i ^ column) for i in range(sp_count)])]
    ppermute x3, starting transfers between devices: 3.87 us -> 0.54 us  [balanced(): lax.ppermute(normed, 'tp', turn(-k))]
    ppermute x24, waiting for transfers between devices: 37 us -> 39.9 us  [across(): return lax.ppermute(array, 'sp', [(i, i ^ column) for i in range(sp_count)])]
  transfers between devices with their start and end apart: 35 -> 35, of which waited for: 12 -> 14; matrix products, arithmetic and copies ran while one was open for 1% -> 1% of each run, Pallas kernels for 24% -> 19%
where the time goes in v3:
time: 218 us; the launch traced here: 217 us
  waiting for transfers between devices  116 us (53%)
  starting transfers between devices  50.8 us (23%)
  Pallas kernels  41.1 us (19%)
  local copies, waits for them, and re-layouts  6.28 us (3%)
  other arithmetic  3.23 us (1%)
    ppermute x24, waiting for transfers between devices, across(): return lax.ppermute(array, 'sp', [(i, i ^ column) for i in range(sp_count)])  39.9 us
    ppermute x3, waiting for transfers between devices, balanced(): lax.ppermute(normed, 'tp', turn(-k))  30.5 us
    ppermute x24, starting transfers between devices, across(): return lax.ppermute(array, 'sp', [(i, i ^ column) for i in range(sp_count)])  25.5 us
    all_to_all x1, waiting for transfers between devices, balanced(): lax.all_to_all(jnp.concatenate([split, keys, values], axis=1), 'sp', spli...  22.5 us
    pallas_call x2, Pallas kernels, expert_pass(): pl.pallas_call(functools.partial(expert_kernel, blocks=len(blocks)), out_...  15.6 us
    pallas_call x1, Pallas kernels, attention(): pl.pallas_call(functools.partial(attention_kernel, sub=sub, parts=parts,...  15.3 us
    ppermute x3, starting transfers between devices, balanced(): lax.ppermute(reduced[k], 'tp', turn(k))  13.8 us
    all_to_all x1, waiting for transfers between devices, balanced(): lax.all_to_all(attended.reshape(sp_count * tp_count, sub, width), ('sp',...  12.5 us
  transfers between devices with their start and end apart: 35, of which 14 were waited for; matrix products, arithmetic and copies ran while one was open for 1% of the time, Pallas kernels for 19%

profile of v3, /device:TPU:0, one launch (start us, length us, event | category | flops | bytes accessed | tf_op | source)
XLA Modules:
  0.0 217.5 jit_solution(5788627617398375558)
XLA Ops:
  0.0 1.0 copy.30
  1.1 1.1 copy.29
  2.1 1.1 copy.28
  3.4 1.4 pad_maximum_fusion
  4.9 5.3 %all-to-all-start = ((bf16[4,1920,128]{2,1,0:T(8,128)(2,1)}), bf16[4,1920,128]{2,1,0:T(8,128)(2,1)}, u32[]{:S(2)}, u32[]{:S(2)}) async-start(bf16[4,1920,128]{2,1,0:T(8,128)(2,1)} %pad_maximum_fusion), calls=%async_computation | async-start | bytes 3932160 | tf_op jit(solution)/shard_map/all_to_all | solution.py:377
  10.2 0.5 collective-permute-start.8
  11.3 0.7 dynamic_slice.3.lam_ref
  12.0 22.5 %all-to-all-done.rows_ref = bf16[4,1920,128]{2,1,0:T(8,128)(2,1)} async-done(((bf16[4,1920,128]{2,1,0:T(8,128)(2,1)}), bf16[4,1920,128]{2,1,0:T(8,128)(2,1)}, u32[]{:S(2)}, u32[]{:S(2)}) %all-to-all-start) | async-done | bytes 1966112 | tf_op jit(solution)/shard_map/all_to_all | solution.py:377
  34.5 15.3 %attention.1 = bf16[1536,128]{1,0:T(8,128)(2,1)} custom-call(s32[1]{0:T(128)} %bitcast.part_ref, f32[1]{0:T(128)} %dynamic_slice.3.lam_ref, f32[1,128]{1,0:T(1,128)S(1)} %bitcast.15, bf16[4,1920,128]{2,1,0:T(8,128)(2,1)} %all-to-all-done.rows_ref), custom_call_target="tpu_custom_call" | custom-call | flops 4831838208 | bytes 1966080 | tf_op jit(solution)/shard_map/attention/pallas_call | solution.py:100
  49.8 5.1 %all-to-all-start.1 = ((bf16[32,48,128]{2,1,0:T(8,128)(2,1)}), bf16[32,48,128]{2,1,0:T(8,128)(2,1)S(1)}, u32[]{:S(2)}, u32[]{:S(2)}) async-start(bf16[32,48,128]{2,1,0:T(8,128)(2,1)} %bitcast.9), calls=%async_computation.1 | async-start | bytes 786432 | tf_op jit(solution)/shard_map/all_to_all | solution.py:390
  55.1 0.7 maximum_maximum_fusion.routes_ref
  55.8 12.5 %all-to-all-done.1 = bf16[32,48,128]{2,1,0:T(8,128)(2,1)S(1)} async-done(((bf16[32,48,128]{2,1,0:T(8,128)(2,1)}), bf16[32,48,128]{2,1,0:T(8,128)(2,1)S(1)}, u32[]{:S(2)}, u32[]{:S(2)}) %all-to-all-start.1) | async-done | bytes 393248 | tf_op jit(solution)/shard_map/all_to_all | solution.py:390
  68.3 0.7 copy-done.3
  69.1 5.8 %project.1 = (bf16[96,2048]{1,0:T(8,128)(2,1)}, bf16[96,2176]{1,0:T(8,128)(2,1)}) custom-call(bf16[4,8,48,128]{3,2,1,0:T(8,128)(2,1)} %bitcast.18, bf16[2048,2048]{1,0:T(8,128)(2,1)} %weight_ref.1, bf16[96,2048]{1,0:T(8,128)(2,1)} %residual_ref.1, f32[1,2048]{1,0:T(1,128)} %bitcast.23, bf16[96,128]{1,0:T(8,128)(2,1)} %maximum_maximum_fusion.routes_ref), custom_call_target="tpu_custom_call" | custom-call | flops 805306368 | bytes 8388608 | tf_op jit(solution)/shard_map/project/pallas_call | solution.py:165
  75.0 0.5 collective-permute-start.17
  75.5 14.1 %collective-permute-done.18.block_ref = bf16[96,2176]{1,0:T(8,128)(2,1)S(1)} collective-permute-done((bf16[96,2176]{1,0:T(8,128)(2,1)}, bf16[96,2176]{1,0:T(8,128)(2,1)S(1)}, u32[]{:S(2)}, u32[]{:S(2)}) %collective-permute-start.18) | collective-permute-done | bytes 417824 | tf_op jit(solution)/shard_map/ppermute | solution.py:429
  89.6 0.6 choose.7
  90.2 16.4 %collective-permute-done.17.block_ref = bf16[96,2176]{1,0:T(8,128)(2,1)S(1)} collective-permute-done((bf16[96,2176]{1,0:T(8,128)(2,1)}, bf16[96,2176]{1,0:T(8,128)(2,1)S(1)}, u32[]{:S(2)}, u32[]{:S(2)}) %collective-permute-start.17) | collective-permute-done | bytes 417824 | tf_op jit(solution)/shard_map/ppermute | solution.py:429
  106.6 0.6 collective-permute-start.19
  107.2 0.6 choose.6
  107.8 0.8 collective-permute-start.20
  108.6 2.2 collective-permute-start.21
  110.8 0.6 collective-permute-start.22
  111.4 0.8 collective-permute-start.23
  112.1 3.7 %collective-permute-done.19.refs_1_ = bf16[64,2048]{1,0:T(8,128)(2,1)S(1)} collective-permute-done((bf16[64,2048]{1,0:T(8,128)(2,1)S(1)}, bf16[64,2048]{1,0:T(8,128)(2,1)S(1)}, u32[]{:S(2)}, u32[]{:S(2)}) %collective-permute-start.19) | collective-permute-done | bytes 262176 | tf_op jit(solution)/shard_map/ppermute | solution.py:423
  115.8 0.8 collective-permute-start.24
  116.6 1.0 copy-done.1
  117.6 0.6 choose.4
  118.2 0.6 choose.5
  118.8 3.9 %collective-permute-done.20.refs_2_ = bf16[64,2048]{1,0:T(8,128)(2,1)S(1)} collective-permute-done((bf16[64,2048]{1,0:T(8,128)(2,1)S(1)}, bf16[64,2048]{1,0:T(8,128)(2,1)S(1)}, u32[]{:S(2)}, u32[]{:S(2)}) %collective-permute-start.20) | collective-permute-done | bytes 262176 | tf_op jit(solution)/shard_map/ppermute | solution.py:423
  122.7 1.5 collective-permute-start
  124.1 0.8 collective-permute-start.1
  124.9 2.1 collective-permute-done.22.refs_5_
  127.0 0.8 collective-permute-start.2
  127.8 6.1 %collective-permute-done.23.refs_6_ = bf16[64,2048]{1,0:T(8,128)(2,1)S(1)} collective-permute-done((bf16[64,2048]{1,0:T(8,128)(2,1)S(1)}, bf16[64,2048]{1,0:T(8,128)(2,1)S(1)}, u32[]{:S(2)}, u32[]{:S(2)}) %collective-permute-start.23) | collective-permute-done | bytes 262176 | tf_op jit(solution)/shard_map/ppermute | solution.py:423
  133.9 1.5 collective-permute-start.4
  135.4 0.8 collective-permute-start.5
  136.2 7.8 %experts.3 = (bf16[64,2048]{1,0:T(8,128)(2,1)S(1)}, bf16[64,2048]{1,0:T(8,128)(2,1)S(1)}, bf16[64,2048]{1,0:T(8,128)(2,1)S(1)}, bf16[64,2048]{1,0:T(8,128)(2,1)S...) custom-call(bf16[64,2048]{1,0:T(8,128)(2,1)S(1)} %get-tuple-element., ...), custom_call_target="tpu_custom_call" | custom-call | flops 3221225472 | bytes 12582912 | tf_op jit(solution)/shard_map/experts/pallas_call | solution.py:323
  144.0 1.3 collective-permute-start.6
  145.3 1.5 collective-permute-start.29
  146.8 0.8 collective-permute-start.30
  147.6 1.9 collective-permute-done.4.refs_5_
  149.5 0.8 collective-permute-start.31
  150.3 6.1 %collective-permute-done.5.refs_6_ = bf16[64,2048]{1,0:T(8,128)(2,1)S(1)} collective-permute-done((bf16[64,2048]{1,0:T(8,128)(2,1)S(1)}, bf16[64,2048]{1,0:T(8,128)(2,1)S(1)}, u32[]{:S(2)}, u32[]{:S(2)}) %collective-permute-start.5) | collective-permute-done | bytes 262176 | tf_op jit(solution)/shard_map/ppermute | solution.py:423
  156.4 1.5 collective-permute-start.25
  157.8 0.8 collective-permute-start.26
  158.6 2.1 collective-permute-done.29.refs_1_
  160.7 0.8 collective-permute-start.27
  161.5 7.8 %experts.2 = (bf16[64,2048]{1,0:T(8,128)(2,1)S(1)}, bf16[64,2048]{1,0:T(8,128)(2,1)S(1)}, bf16[64,2048]{1,0:T(8,128)(2,1)S(1)}, bf16[64,2048]{1,0:T(8,128)(2,1)S...) custom-call(bf16[64,2048]{1,0:T(8,128)(2,1)S(1)} %get-tuple-element., ...), custom_call_target="tpu_custom_call" | custom-call | flops 3221225472 | bytes 12582912 | tf_op jit(solution)/shard_map/experts/pallas_call | solution.py:323
  169.3 1.6 collective-permute-start.13
  170.9 1.2 collective-permute-start.14
  172.1 0.8 collective-permute-start.15
  172.9 6.0 %collective-permute-done.26.refs_2_ = bf16[64,2048]{1,0:T(8,128)(2,1)S(1)} collective-permute-done((bf16[64,2048]{1,0:T(8,128)(2,1)S(1)}, bf16[64,2048]{1,0:T(8,128)(2,1)S(1)}, u32[]{:S(2)}, u32[]{:S(2)}) %collective-permute-start.26) | collective-permute-done | bytes 262176 | tf_op jit(solution)/shard_map/ppermute | solution.py:423
  178.8 1.5 collective-permute-start.10
  180.8 8.0 %collective-permute-start.32 = (bf16[96,2048]{1,0:T(8,128)(2,1)S(1)}, bf16[96,2048]{1,0:T(8,128)(2,1)S(1)}, u32[]{:S(2)}, u32[]{:S(2)}) collective-permute-start(bf16[96,2048]{1,0:T(8,128)(2,1)S(1)} %merge.7), channel_id=1, source_target_pairs={{0,6},{1,7},{2,0},{3,1},{4,2},{5,3},{6,4},{7,5},{8,14},{9,15},{10,... | collective-permute-start | bytes 1179656 | tf_op jit(solution)/shard_map/ppermute | solution.py:447
  188.8 0.5 merge.6
  189.4 0.5 merge.5
  189.9 5.7 %collective-permute-start.16 = (bf16[96,2048]{1,0:T(8,128)(2,1)S(1)}, bf16[96,2048]{1,0:T(8,128)(2,1)S(1)}, u32[]{:S(2)}, u32[]{:S(2)}) collective-permute-start(bf16[96,2048]{1,0:T(8,128)(2,1)S(1)} %merge.5), channel_id=1, source_target_pairs={{0,2},{1,3},{2,4},{3,5},{4,6},{5,7},{6,0},{7,1},{8,10},{9,11},{10,... | collective-permute-start | bytes 1179656 | tf_op jit(solution)/shard_map/ppermute | solution.py:447
  195.6 0.8 collective-permute-start.11
  196.4 1.4 collective-permute-start.12
  197.8 8.0 %collective-permute-done.11.refs_2_ = bf16[64,2048]{1,0:T(8,128)(2,1)S(1)} collective-permute-done((bf16[64,2048]{1,0:T(8,128)(2,1)S(1)}, bf16[64,2048]{1,0:T(8,128)(2,1)S(1)}, u32[]{:S(2)}, u32[]{:S(2)}) %collective-permute-start.11) | collective-permute-done | bytes 262176 | tf_op jit(solution)/shard_map/ppermute | solution.py:423
  205.8 0.5 merge.4
  206.3 10.1 %collective-permute-done.28 = bf16[96,2048]{1,0:T(8,128)(2,1)S(1)} collective-permute-done((bf16[96,2048]{1,0:T(8,128)(2,1)S(1)}, bf16[96,2048]{1,0:T(8,128)(2,1)S(1)}, u32[]{:S(2)}, u32[]{:S(2)}) %collective-permute-start.28) | collective-permute-done | bytes 393248 | tf_op jit(solution)/shard_map/ppermute | solution.py:447
  216.4 1.1 add_convert_fusion
  (56 shorter events, 1.7 us)
Async XLA Ops:
  4.8 5.4 %copy-start = (bf16[2,2048,256]{2,1,0:T(8,128)(2,1)S(1)}, bf16[2,2048,256]{2,1,0:T(8,128)(2,1)}, u32[]{:S(2)}) copy-start(bf16[2,2048,256]{2,1,0:T(8,128)(2,1)} %refs_8_.3) | copy-start | bytes 6291460
  4.8 5.9 %copy-start.5 = (s32[96,2]{0,1:T(2,128)S(1)}, s32[96,2]{0,1:T(2,128)}, u32[]{:S(2)}) copy-start(s32[96,2]{0,1:T(2,128)} %param.21) | copy-start | bytes 2308
  4.8 6.1 %copy-start.6 = (f32[96,2]{0,1:T(2,128)S(1)}, f32[96,2]{0,1:T(2,128)}, u32[]{:S(2)}) copy-start(f32[96,2]{0,1:T(2,128)} %param.22) | copy-start | bytes 2308
  4.8 6.4 %copy-start.7 = (f32[2]{0:T(128)S(1)}, f32[2]{0:T(128)}, u32[]{:S(2)}) copy-start(f32[2]{0:T(128)} %param.16) | copy-start | bytes 28
  4.8 29.7 %copy-start.2 = (f32[128]{0:T(128)S(1)}, f32[128]{0:T(128)}, u32[]{:S(2)}) copy-start(f32[128]{0:T(128)} %param.17) | copy-start | bytes 1540
  4.9 29.7 %all-to-all-start = ((bf16[4,1920,128]{2,1,0:T(8,128)(2,1)}), bf16[4,1920,128]{2,1,0:T(8,128)(2,1)}, u32[]{:S(2)}, u32[]{:S(2)}) async-start(bf16[4,1920,128]{2,1,0:T(8,128)(2,1)} %pad_maximum_fusion), calls=%async_computation | async-start | bytes 3932160 | tf_op jit(solution)/shard_map/all_to_all | solution.py:377
  10.2 97.6 %collective-permute-start.7 = (bf16[2,2048,256]{2,1,0:T(8,128)(2,1)S(1)}, bf16[2,2048,256]{2,1,0:T(8,128)(2,1)}, u32[]{:S(2)}, u32[]{:S(2)}) collective-permute-start(bf16[2,2048,256]{2,1,0:T(8,128)(2,1)S(1)} %copy-done), channel_id=1, source_target_pairs={{0,1},{1,0},{2,3},{3,2},{4,5},{5,4},{6,7},{7,6},{8,9},{9,8},{10,11... | collective-permute-start | bytes 6291464 | tf_op jit(solution)/shard_map/ppermute | solution.py:370
  10.2 98.5 %collective-permute-start.8 = (bf16[2,2048,256]{2,1,0:T(8,128)(2,1)}, bf16[2,2048,256]{2,1,0:T(8,128)(2,1)}, u32[]{:S(2)}, u32[]{:S(2)}) collective-permute-start(bf16[2,2048,256]{2,1,0:T(8,128)(2,1)} %refs_9_.3), channel_id=1, source_target_pairs={{0,1},{1,0},{2,3},{3,2},{4,5},{5,4},{6,7},{7,6},{8,9},{9,8},{10,11... | collective-permute-start | bytes 6291464 | tf_op jit(solution)/shard_map/ppermute | solution.py:370
  10.7 100.1 %collective-permute-start.9 = (bf16[2,256,2048]{2,1,0:T(8,128)(2,1)}, bf16[2,256,2048]{2,1,0:T(8,128)(2,1)}, u32[]{:S(2)}, u32[]{:S(2)}) collective-permute-start(bf16[2,256,2048]{2,1,0:T(8,128)(2,1)} %refs_10_.3), channel_id=1, source_target_pairs={{0,1},{1,0},{2,3},{3,2},{4,5},{5,4},{6,7},{7,6},{8,9},{9,8},{10,11... | collective-permute-start | bytes 6291464 | tf_op jit(solution)/shard_map/ppermute | solution.py:370
  49.8 18.5 %all-to-all-start.1 = ((bf16[32,48,128]{2,1,0:T(8,128)(2,1)}), bf16[32,48,128]{2,1,0:T(8,128)(2,1)S(1)}, u32[]{:S(2)}, u32[]{:S(2)}) async-start(bf16[32,48,128]{2,1,0:T(8,128)(2,1)} %bitcast.9), calls=%async_computation.1 | async-start | bytes 786432 | tf_op jit(solution)/shard_map/all_to_all | solution.py:390
  68.3 0.7 copy-start.3
  74.9 14.7 %collective-permute-start.18 = (bf16[96,2176]{1,0:T(8,128)(2,1)}, bf16[96,2176]{1,0:T(8,128)(2,1)S(1)}, u32[]{:S(2)}, u32[]{:S(2)}) collective-permute-start(bf16[96,2176]{1,0:T(8,128)(2,1)} %get-tuple-element.48.block_ref), channel_id=1, source_target_pairs={{0,2},{1,3},{2,4},{3,5},{4,6},{5,7},{6,0},{7,1},{8,10},{9,11},{10,... | collective-permute-start | bytes 1253384 | tf_op jit(solution)/shard_map/ppermute | solution.py:429
  75.0 31.6 %collective-permute-start.17 = (bf16[96,2176]{1,0:T(8,128)(2,1)}, bf16[96,2176]{1,0:T(8,128)(2,1)S(1)}, u32[]{:S(2)}, u32[]{:S(2)}) collective-permute-start(bf16[96,2176]{1,0:T(8,128)(2,1)} %get-tuple-element.48.block_ref), channel_id=1, source_target_pairs={{0,4},{1,5},{2,6},{3,7},{4,0},{5,1},{6,2},{7,3},{8,12},{9,13},{10,... | collective-permute-start | bytes 1253384 | tf_op jit(solution)/shard_map/ppermute | solution.py:429
  89.6 21.8 %collective-permute-start.3 = (bf16[96,2176]{1,0:T(8,128)(2,1)}, bf16[96,2176]{1,0:T(8,128)(2,1)S(1)}, u32[]{:S(2)}, u32[]{:S(2)}) collective-permute-start(bf16[96,2176]{1,0:T(8,128)(2,1)} %get-tuple-element.48.block_ref), channel_id=1, source_target_pairs={{0,6},{1,7},{2,0},{3,1},{4,2},{5,3},{6,4},{7,5},{8,14},{9,15},{10,... | collective-permute-start | bytes 1253384 | tf_op jit(solution)/shard_map/ppermute | solution.py:429
  106.6 9.2 %collective-permute-start.19 = (bf16[64,2048]{1,0:T(8,128)(2,1)S(1)}, bf16[64,2048]{1,0:T(8,128)(2,1)S(1)}, u32[]{:S(2)}, u32[]{:S(2)}) collective-permute-start(bf16[64,2048]{1,0:T(8,128)(2,1)S(1)} %get-tuple-element.72), channel_id=1, source_target_pairs={{0,8},{8,0},{16,24},{24,16},{1,9},{9,1},{17,25},{25,17},{2,10},{10... | collective-permute-start | bytes 786440 | tf_op jit(solution)/shard_map/ppermute | solution.py:423
  107.8 14.9 %collective-permute-start.20 = (bf16[64,2048]{1,0:T(8,128)(2,1)S(1)}, bf16[64,2048]{1,0:T(8,128)(2,1)S(1)}, u32[]{:S(2)}, u32[]{:S(2)}) collective-permute-start(bf16[64,2048]{1,0:T(8,128)(2,1)S(1)} %get-tuple-element.73), channel_id=1, source_target_pairs={{0,16},{8,24},{16,0},{24,8},{1,17},{9,25},{17,1},{25,9},{2,18},{10... | collective-permute-start | bytes 786440 | tf_op jit(solution)/shard_map/ppermute | solution.py:423
  108.6 15.5 %collective-permute-start.21 = (bf16[64,2048]{1,0:T(8,128)(2,1)S(1)}, bf16[64,2048]{1,0:T(8,128)(2,1)S(1)}, u32[]{:S(2)}, u32[]{:S(2)}) collective-permute-start(bf16[64,2048]{1,0:T(8,128)(2,1)S(1)} %get-tuple-element.74), channel_id=1, source_target_pairs={{0,24},{8,16},{16,8},{24,0},{1,25},{9,17},{17,9},{25,1},{2,26},{10... | collective-permute-start | bytes 786440 | tf_op jit(solution)/shard_map/ppermute | solution.py:423
  110.8 16.2 %collective-permute-start.22 = (bf16[64,2048]{1,0:T(8,128)(2,1)S(1)}, bf16[64,2048]{1,0:T(8,128)(2,1)S(1)}, u32[]{:S(2)}, u32[]{:S(2)}) collective-permute-start(bf16[64,2048]{1,0:T(8,128)(2,1)S(1)} %get-tuple-element.76), channel_id=1, source_target_pairs={{0,8},{8,0},{16,24},{24,16},{1,9},{9,1},{17,25},{25,17},{2,10},{10... | collective-permute-start | bytes 786440 | tf_op jit(solution)/shard_map/ppermute | solution.py:423
  111.4 22.5 %collective-permute-start.23 = (bf16[64,2048]{1,0:T(8,128)(2,1)S(1)}, bf16[64,2048]{1,0:T(8,128)(2,1)S(1)}, u32[]{:S(2)}, u32[]{:S(2)}) collective-permute-start(bf16[64,2048]{1,0:T(8,128)(2,1)S(1)} %get-tuple-element.77), channel_id=1, source_target_pairs={{0,16},{8,24},{16,0},{24,8},{1,17},{9,25},{17,1},{25,9},{2,18},{10... | collective-permute-start | bytes 786440 | tf_op jit(solution)/shard_map/ppermute | solution.py:423
  115.8 19.6 %collective-permute-start.24 = (bf16[64,2048]{1,0:T(8,128)(2,1)S(1)}, bf16[64,2048]{1,0:T(8,128)(2,1)S(1)}, u32[]{:S(2)}, u32[]{:S(2)}) collective-permute-start(bf16[64,2048]{1,0:T(8,128)(2,1)S(1)} %get-tuple-element.78), channel_id=1, source_target_pairs={{0,24},{8,16},{16,8},{24,0},{1,25},{9,17},{17,9},{25,1},{2,26},{10... | collective-permute-start | bytes 786440 | tf_op jit(solution)/shard_map/ppermute | solution.py:423
  116.6 1.0 copy-start.1
  122.7 21.3 %collective-permute-start = (bf16[64,2048]{1,0:T(8,128)(2,1)S(1)}, bf16[64,2048]{1,0:T(8,128)(2,1)S(1)}, u32[]{:S(2)}, u32[]{:S(2)}) collective-permute-start(bf16[64,2048]{1,0:T(8,128)(2,1)S(1)} %get-tuple-element.52), channel_id=1, source_target_pairs={{0,8},{8,0},{16,24},{24,16},{1,9},{9,1},{17,25},{25,17},{2,10},{10... | collective-permute-start | bytes 786440 | tf_op jit(solution)/shard_map/ppermute | solution.py:423
  124.1 21.1 %collective-permute-start.1 = (bf16[64,2048]{1,0:T(8,128)(2,1)S(1)}, bf16[64,2048]{1,0:T(8,128)(2,1)S(1)}, u32[]{:S(2)}, u32[]{:S(2)}) collective-permute-start(bf16[64,2048]{1,0:T(8,128)(2,1)S(1)} %get-tuple-element.53), channel_id=1, source_target_pairs={{0,16},{8,24},{16,0},{24,8},{1,17},{9,25},{17,1},{25,9},{2,18},{10... | collective-permute-start | bytes 786440 | tf_op jit(solution)/shard_map/ppermute | solution.py:423
  127.0 19.7 %collective-permute-start.2 = (bf16[64,2048]{1,0:T(8,128)(2,1)S(1)}, bf16[64,2048]{1,0:T(8,128)(2,1)S(1)}, u32[]{:S(2)}, u32[]{:S(2)}) collective-permute-start(bf16[64,2048]{1,0:T(8,128)(2,1)S(1)} %get-tuple-element.54), channel_id=1, source_target_pairs={{0,24},{8,16},{16,8},{24,0},{1,25},{9,17},{17,9},{25,1},{2,26},{10... | collective-permute-start | bytes 786440 | tf_op jit(solution)/shard_map/ppermute | solution.py:423
  133.9 15.6 %collective-permute-start.4 = (bf16[64,2048]{1,0:T(8,128)(2,1)S(1)}, bf16[64,2048]{1,0:T(8,128)(2,1)S(1)}, u32[]{:S(2)}, u32[]{:S(2)}) collective-permute-start(bf16[64,2048]{1,0:T(8,128)(2,1)S(1)} %get-tuple-element.56), channel_id=1, source_target_pairs={{0,8},{8,0},{16,24},{24,16},{1,9},{9,1},{17,25},{25,17},{2,10},{10... | collective-permute-start | bytes 786440 | tf_op jit(solution)/shard_map/ppermute | solution.py:423
  135.4 21.0 %collective-permute-start.5 = (bf16[64,2048]{1,0:T(8,128)(2,1)S(1)}, bf16[64,2048]{1,0:T(8,128)(2,1)S(1)}, u32[]{:S(2)}, u32[]{:S(2)}) collective-permute-start(bf16[64,2048]{1,0:T(8,128)(2,1)S(1)} %get-tuple-element.57), channel_id=1, source_target_pairs={{0,16},{8,24},{16,0},{24,8},{1,17},{9,25},{17,1},{25,9},{2,18},{10... | collective-permute-start | bytes 786440 | tf_op jit(solution)/shard_map/ppermute | solution.py:423
  144.0 13.8 %collective-permute-start.6 = (bf16[64,2048]{1,0:T(8,128)(2,1)S(1)}, bf16[64,2048]{1,0:T(8,128)(2,1)S(1)}, u32[]{:S(2)}, u32[]{:S(2)}) collective-permute-start(bf16[64,2048]{1,0:T(8,128)(2,1)S(1)} %get-tuple-element.58), channel_id=1, source_target_pairs={{0,24},{8,16},{16,8},{24,0},{1,25},{9,17},{17,9},{25,1},{2,26},{10... | collective-permute-start | bytes 786440 | tf_op jit(solution)/shard_map/ppermute | solution.py:423
  145.3 15.5 %collective-permute-start.29 = (bf16[64,2048]{1,0:T(8,128)(2,1)S(1)}, bf16[64,2048]{1,0:T(8,128)(2,1)S(1)}, u32[]{:S(2)}, u32[]{:S(2)}) collective-permute-start(bf16[64,2048]{1,0:T(8,128)(2,1)S(1)} %get-tuple-element.86), channel_id=1, source_target_pairs={{0,8},{8,0},{16,24},{24,16},{1,9},{9,1},{17,25},{25,17},{2,10},{10... | collective-permute-start | bytes 786440 | tf_op jit(solution)/shard_map/ppermute | solution.py:423
  146.8 22.6 %collective-permute-start.30 = (bf16[64,2048]{1,0:T(8,128)(2,1)S(1)}, bf16[64,2048]{1,0:T(8,128)(2,1)S(1)}, u32[]{:S(2)}, u32[]{:S(2)}) collective-permute-start(bf16[64,2048]{1,0:T(8,128)(2,1)S(1)} %get-tuple-element.87), channel_id=1, source_target_pairs={{0,16},{8,24},{16,0},{24,8},{1,17},{9,25},{17,1},{25,9},{2,18},{10... | collective-permute-start | bytes 786440 | tf_op jit(solution)/shard_map/ppermute | solution.py:423
  149.5 21.4 %collective-permute-start.31 = (bf16[64,2048]{1,0:T(8,128)(2,1)S(1)}, bf16[64,2048]{1,0:T(8,128)(2,1)S(1)}, u32[]{:S(2)}, u32[]{:S(2)}) collective-permute-start(bf16[64,2048]{1,0:T(8,128)(2,1)S(1)} %get-tuple-element.88), channel_id=1, source_target_pairs={{0,24},{8,16},{16,8},{24,0},{1,25},{9,17},{17,9},{25,1},{2,26},{10... | collective-permute-start | bytes 786440 | tf_op jit(solution)/shard_map/ppermute | solution.py:423
  156.4 15.8 %collective-permute-start.25 = (bf16[64,2048]{1,0:T(8,128)(2,1)S(1)}, bf16[64,2048]{1,0:T(8,128)(2,1)S(1)}, u32[]{:S(2)}, u32[]{:S(2)}) collective-permute-start(bf16[64,2048]{1,0:T(8,128)(2,1)S(1)} %get-tuple-element.80), channel_id=1, source_target_pairs={{0,8},{8,0},{16,24},{24,16},{1,9},{9,1},{17,25},{25,17},{2,10},{10... | collective-permute-start | bytes 786440 | tf_op jit(solution)/shard_map/ppermute | solution.py:423
  157.8 21.0 %collective-permute-start.26 = (bf16[64,2048]{1,0:T(8,128)(2,1)S(1)}, bf16[64,2048]{1,0:T(8,128)(2,1)S(1)}, u32[]{:S(2)}, u32[]{:S(2)}) collective-permute-start(bf16[64,2048]{1,0:T(8,128)(2,1)S(1)} %get-tuple-element.81), channel_id=1, source_target_pairs={{0,16},{8,24},{16,0},{24,8},{1,17},{9,25},{17,1},{25,9},{2,18},{10... | collective-permute-start | bytes 786440 | tf_op jit(solution)/shard_map/ppermute | solution.py:423
  160.7 20.0 %collective-permute-start.27 = (bf16[64,2048]{1,0:T(8,128)(2,1)S(1)}, bf16[64,2048]{1,0:T(8,128)(2,1)S(1)}, u32[]{:S(2)}, u32[]{:S(2)}) collective-permute-start(bf16[64,2048]{1,0:T(8,128)(2,1)S(1)} %get-tuple-element.82), channel_id=1, source_target_pairs={{0,24},{8,16},{16,8},{24,0},{1,25},{9,17},{17,9},{25,1},{2,26},{10... | collective-permute-start | bytes 786440 | tf_op jit(solution)/shard_map/ppermute | solution.py:423
  169.3 19.9 %collective-permute-start.13 = (bf16[64,2048]{1,0:T(8,128)(2,1)S(1)}, bf16[64,2048]{1,0:T(8,128)(2,1)S(1)}, u32[]{:S(2)}, u32[]{:S(2)}) collective-permute-start(bf16[64,2048]{1,0:T(8,128)(2,1)S(1)} %get-tuple-element.66), channel_id=1, source_target_pairs={{0,8},{8,0},{16,24},{24,16},{1,9},{9,1},{17,25},{25,17},{2,10},{10... | collective-permute-start | bytes 786440 | tf_op jit(solution)/shard_map/ppermute | solution.py:423
  170.9 18.5 %collective-permute-start.14 = (bf16[64,2048]{1,0:T(8,128)(2,1)S(1)}, bf16[64,2048]{1,0:T(8,128)(2,1)S(1)}, u32[]{:S(2)}, u32[]{:S(2)}) collective-permute-start(bf16[64,2048]{1,0:T(8,128)(2,1)S(1)} %get-tuple-element.67), channel_id=1, source_target_pairs={{0,16},{8,24},{16,0},{24,8},{1,17},{9,25},{17,1},{25,9},{2,18},{10... | collective-permute-start | bytes 786440 | tf_op jit(solution)/shard_map/ppermute | solution.py:423
  172.1 17.2 %collective-permute-start.15 = (bf16[64,2048]{1,0:T(8,128)(2,1)S(1)}, bf16[64,2048]{1,0:T(8,128)(2,1)S(1)}, u32[]{:S(2)}, u32[]{:S(2)}) collective-permute-start(bf16[64,2048]{1,0:T(8,128)(2,1)S(1)} %get-tuple-element.68), channel_id=1, source_target_pairs={{0,24},{8,16},{16,8},{24,0},{1,25},{9,17},{17,9},{25,1},{2,26},{10... | collective-permute-start | bytes 786440 | tf_op jit(solution)/shard_map/ppermute | solution.py:423
  178.8 17.5 %collective-permute-start.10 = (bf16[64,2048]{1,0:T(8,128)(2,1)S(1)}, bf16[64,2048]{1,0:T(8,128)(2,1)S(1)}, u32[]{:S(2)}, u32[]{:S(2)}) collective-permute-start(bf16[64,2048]{1,0:T(8,128)(2,1)S(1)} %get-tuple-element.60), channel_id=1, source_target_pairs={{0,8},{8,0},{16,24},{24,16},{1,9},{9,1},{17,25},{25,17},{2,10},{10... | collective-permute-start | bytes 786440 | tf_op jit(solution)/shard_map/ppermute | solution.py:423
  180.8 25.5 %collective-permute-start.32 = (bf16[96,2048]{1,0:T(8,128)(2,1)S(1)}, bf16[96,2048]{1,0:T(8,128)(2,1)S(1)}, u32[]{:S(2)}, u32[]{:S(2)}) collective-permute-start(bf16[96,2048]{1,0:T(8,128)(2,1)S(1)} %merge.7), channel_id=1, source_target_pairs={{0,6},{1,7},{2,0},{3,1},{4,2},{5,3},{6,4},{7,5},{8,14},{9,15},{10,... | collective-permute-start | bytes 1179656 | tf_op jit(solution)/shard_map/ppermute | solution.py:447
  188.8 27.6 %copy-start.4 = (bf16[96,2048]{1,0:T(8,128)(2,1)S(1)}, bf16[96,2048]{1,0:T(8,128)(2,1)}, u32[]{:S(2)}) copy-start(bf16[96,2048]{1,0:T(8,128)(2,1)} %get-tuple-element.47) | copy-start | bytes 1179652
  189.3 27.1 %collective-permute-start.28 = (bf16[96,2048]{1,0:T(8,128)(2,1)S(1)}, bf16[96,2048]{1,0:T(8,128)(2,1)S(1)}, u32[]{:S(2)}, u32[]{:S(2)}) collective-permute-start(bf16[96,2048]{1,0:T(8,128)(2,1)S(1)} %merge.6), channel_id=1, source_target_pairs={{0,4},{1,5},{2,6},{3,7},{4,0},{5,1},{6,2},{7,3},{8,12},{9,13},{10,... | collective-permute-start | bytes 1179656 | tf_op jit(solution)/shard_map/ppermute | solution.py:447
  189.9 26.6 %collective-permute-start.16 = (bf16[96,2048]{1,0:T(8,128)(2,1)S(1)}, bf16[96,2048]{1,0:T(8,128)(2,1)S(1)}, u32[]{:S(2)}, u32[]{:S(2)}) collective-permute-start(bf16[96,2048]{1,0:T(8,128)(2,1)S(1)} %merge.5), channel_id=1, source_target_pairs={{0,2},{1,3},{2,4},{3,5},{4,6},{5,7},{6,0},{7,1},{8,10},{9,11},{10,... | collective-permute-start | bytes 1179656 | tf_op jit(solution)/shard_map/ppermute | solution.py:447
  195.6 10.2 %collective-permute-start.11 = (bf16[64,2048]{1,0:T(8,128)(2,1)S(1)}, bf16[64,2048]{1,0:T(8,128)(2,1)S(1)}, u32[]{:S(2)}, u32[]{:S(2)}) collective-permute-start(bf16[64,2048]{1,0:T(8,128)(2,1)S(1)} %get-tuple-element.61), channel_id=1, source_target_pairs={{0,16},{8,24},{16,0},{24,8},{1,17},{9,25},{17,1},{25,9},{2,18},{10... | collective-permute-start | bytes 786440 | tf_op jit(solution)/shard_map/ppermute | solution.py:423
  196.4 9.5 %collective-permute-start.12 = (bf16[64,2048]{1,0:T(8,128)(2,1)S(1)}, bf16[64,2048]{1,0:T(8,128)(2,1)S(1)}, u32[]{:S(2)}, u32[]{:S(2)}) collective-permute-start(bf16[64,2048]{1,0:T(8,128)(2,1)S(1)} %get-tuple-element.62), channel_id=1, source_target_pairs={{0,24},{8,16},{16,8},{24,0},{1,25},{9,17},{17,9},{25,1},{2,26},{10... | collective-permute-start | bytes 786440 | tf_op jit(solution)/shard_map/ppermute | solution.py:423

commit v4 on v3

--- a/solution.py
+++ b/solution.py
@@ -10,18 +10,38 @@
 
 LANES = 128
 KEY_TILE = 256
+PROJECT_LIMIT = 48 * 1024 * 1024
 
 
 def attention_kernel(
-    part_ref, lam_ref, gain_ref, rows_ref, out_ref, stack_ref, acc_ref, top_ref, *, sub, parts, scale
+    place_ref, part_ref, lam_ref, gain_ref, *refs, columns, sub, parts, scale
 ):
+    arrived_refs = refs[: 3 * columns]
+    out_ref, query_ref, key_ref, value_ref, stack_ref, acc_ref, top_ref, sems = refs[3 * columns :]
     exact = math.frexp(scale)[0] == 0.5
     tile = pl.program_id(0)
+
+    @pl.when(tile == 0)
+    def _():
+        copies = [
+            pltpu.make_async_copy(
+                arrived_refs[kind * columns + column],
+                ref.at[jnp.bitwise_xor(place_ref[0], column)],
+                sems.at[kind, column],
+            )
+            for column in range(columns)
+            for kind, ref in enumerate((query_ref, key_ref, value_ref))
+        ]
+        for copy in copies:
+            copy.start()
+        for copy in copies:
+            copy.wait()
+
     tile_rows, width = out_ref.shape
     key_rows = tile_rows * parts
     half = width // 2
 
-    query = rows_ref[tile, 0:tile_rows, :]
+    query = query_ref[tile]
     if exact:
         query = (query.astype(jnp.float32) * scale).astype(jnp.bfloat16)
     low = lax.broadcasted_iota(jnp.int32, (tile_rows, width), 1) < half
@@ -35,7 +55,7 @@
         place = pl.ds(first, count)
         scores = lax.dot_general(
             stack_ref[place, :],
-            rows_ref[source, pl.ds(tile_rows, keys), :],
+            key_ref[source, pl.ds(0, keys), :],
             (((1,), (1,)), ((), ())),
             preferred_element_type=jnp.float32,
         )
@@ -62,7 +82,7 @@
         decay = jnp.exp(before - after)
         weights = jnp.exp(scores - jnp.concatenate([after] * (keys // LANES), axis=1))
         top_ref[place, :] = after
-        values = rows_ref[source, pl.ds(tile_rows + key_rows, keys), :]
+        values = value_ref[source, pl.ds(0, keys), :]
         acc_ref[place, :] = acc_ref[place, :] * jnp.concatenate(
             [decay] * (1 + width // LANES), axis=1
         ) + jnp.dot(
@@ -93,40 +113,48 @@
     out_ref[...] = (scaled * gain_ref[...]).astype(out_ref.dtype)
 
 
-def attention(part, lam, gain, arrived, sub, tile_rows, parts, scale):
-    sources, _, width = arrived.shape
-    total_rows = sources * tile_rows
+def attention(place, part, lam, gain, queries, keys, values, sub, parts, scale):
+    columns = len(queries)
+    tile_rows, width = queries[0].shape
+    total_rows = columns * tile_rows
     pairs = total_rows * total_rows * parts
+    scalar = pl.BlockSpec(memory_space=pltpu.SMEM)
     return pl.pallas_call(
-        functools.partial(attention_kernel, sub=sub, parts=parts, scale=scale),
-        grid=(sources,),
+        functools.partial(attention_kernel, columns=columns, sub=sub, parts=parts, scale=scale),
+        grid=(columns,),
         out_shape=jax.ShapeDtypeStruct((total_rows, width), jnp.bfloat16),
         in_specs=[
-            pl.BlockSpec(memory_space=pltpu.SMEM),
-            pl.BlockSpec(memory_space=pltpu.SMEM),
+            scalar,
+            scalar,
+            scalar,
             pl.BlockSpec((1, width), lambda i: (0, 0)),
-            pl.BlockSpec(memory_space=pltpu.VMEM),
+            *(pl.BlockSpec(memory_space=pl.ANY) for _ in range(3 * columns)),
         ],
         out_specs=pl.BlockSpec((tile_rows, width), lambda i: (i, 0)),
         scratch_shapes=[
+            pltpu.VMEM((columns, tile_rows, width), jnp.bfloat16),
+            pltpu.VMEM((columns, tile_rows * parts, width), jnp.bfloat16),
+            pltpu.VMEM((columns, tile_rows * parts, width), jnp.bfloat16),
             pltpu.VMEM((2 * tile_rows, width), jnp.bfloat16),
             pltpu.VMEM((2 * tile_rows, width + LANES), jnp.float32),
             pltpu.VMEM((2 * tile_rows, LANES), jnp.float32),
+            pltpu.SemaphoreType.DMA((3, columns)),
         ],
-        compiler_params=pltpu.CompilerParams(vmem_limit_bytes=20 * 1024 * 1024),
+        compiler_params=pltpu.CompilerParams(vmem_limit_bytes=56 * 1024 * 1024),
         cost_estimate=pl.CostEstimate(
-            flops=8 * pairs * width, bytes_accessed=2 * arrived.size, transcendentals=pairs
+            flops=8 * pairs * width, bytes_accessed=6 * total_rows * width, transcendentals=pairs
         ),
         name="attention",
-    )(part, lam, gain, arrived)
+    )(place, part, lam, gain, *queries, *keys, *values)
 
 
 def project_kernel(
-    heads_ref, weight_ref, residual_ref, gain_ref, routes_ref, updated_ref, normed_ref, left_ref, kept_ref, acc_ref, sems, *, parts
+    place_ref, heads_ref, weight_ref, residual_ref, gain_ref, routes_ref, updated_ref, normed_ref, *refs, parts, held, experts, capacity
 ):
+    *chosen_refs, left_ref, kept_ref, acc_ref, sems = refs
     sources, columns, sub, width = heads_ref.shape
-    held = sources // parts
-    depth = held * width
+    together = sources // parts
+    depth = together * width
     copies = [
         pltpu.make_async_copy(
             weight_ref.at[pl.ds(column * depth, depth)], kept_ref.at[column], sems.at[column]
@@ -137,10 +165,10 @@
         copy.start()
     for part in range(parts):
         for column in range(columns):
-            for head in range(held):
+            for head in range(together):
                 left_ref[
                     column, part * sub : (part + 1) * sub, head * width : (head + 1) * width
-                ] = heads_ref[part * held + head, column]
+                ] = heads_ref[part * together + head, column]
     for column, copy in enumerate(copies):
         copy.wait()
         product = jnp.dot(left_ref[column], kept_ref[column], preferred_element_type=jnp.float32)
@@ -155,33 +183,48 @@
     model = wide.shape[1]
     normed_ref[:, :model] = (scaled * gain_ref[...]).astype(jnp.bfloat16)
     normed_ref[:, model:] = routes_ref[...]
-
-
-def project(heads, out_weight, residual, gain, routes, parts):
+    choose_kernel(place_ref, normed_ref, *chosen_refs, held=held, experts=experts, capacity=capacity)
+
+
+def project(place, heads, out_weight, residual, gain, routes, parts, held, experts, capacity):
     sources, columns, _, width = heads.shape
+    depth = sources // parts * width
     rows, model = residual.shape
-    depth = sources // parts * width
+    slots = held * capacity
     whole = pl.BlockSpec(memory_space=pltpu.VMEM)
+    table = jax.ShapeDtypeStruct((rows, sources * slots), jnp.bfloat16)
     return pl.pallas_call(
-        functools.partial(project_kernel, parts=parts),
+        functools.partial(
+            project_kernel, parts=parts, held=held, experts=experts, capacity=capacity
+        ),
         out_shape=(
             jax.ShapeDtypeStruct((rows, model), jnp.bfloat16),
             jax.ShapeDtypeStruct((rows, model + LANES), jnp.bfloat16),
-        ),
-        in_specs=[whole, pl.BlockSpec(memory_space=pl.ANY), whole, whole, whole],
-        out_specs=(whole, whole),
+            table,
+            table,
+            *(jax.ShapeDtypeStruct((slots, model), jnp.bfloat16) for _ in range(sources)),
+        ),
+        in_specs=[
+            pl.BlockSpec(memory_space=pltpu.SMEM),
+            whole,
+            pl.BlockSpec(memory_space=pl.ANY),
+            whole,
+            whole,
+            whole,
+        ],
+        out_specs=(whole,) * (4 + sources),
         scratch_shapes=[
             pltpu.VMEM((columns, rows, depth), jnp.bfloat16),
             pltpu.VMEM((columns, depth, model), jnp.bfloat16),
             pltpu.VMEM((rows, model), jnp.float32),
             pltpu.SemaphoreType.DMA((columns,)),
         ],
-        compiler_params=pltpu.CompilerParams(vmem_limit_bytes=56 * 1024 * 1024),
+        compiler_params=pltpu.CompilerParams(vmem_limit_bytes=PROJECT_LIMIT),
         cost_estimate=pl.CostEstimate(
             flops=2 * rows * out_weight.size, bytes_accessed=2 * out_weight.size, transcendentals=0
         ),
         name="project",
-    )(heads, out_weight, residual, gain, routes)
+    )(place, heads, out_weight, residual, gain, routes)
 
 
 def choose_kernel(place_ref, block_ref, coarse_ref, fine_ref, *out_refs, held, experts, capacity):
@@ -365,25 +408,44 @@
     held = gate_weight.shape[0]
     experts = held * sp_count
 
+    capacity = row_capacity(rows, expert_ids.shape[1], experts)
+    place = sp_index.reshape(1)
+
+    def across(array, column):
+        return lax.ppermute(array, "sp", [(i, i ^ column) for i in range(sp_count)])
+
+    def entries(array, count):
+        return [
+            lax.dynamic_index_in_dim(array, jnp.bitwise_xor(sp_index, c) % count, 0, keepdims=False)
+            for c in range(count)
+        ]
+
+    def spread(picked):
+        count = len(picked)
+        return [picked[0]] + [across(picked[c % count], c) for c in range(1, sp_count)]
+
+    values = entries(jnp.transpose(head_values, (1, 0, 2)), heads)
+    key_pairs, queries, *values = lax.optimization_barrier((key_pairs, queries, *values))
+    keys = entries(jnp.transpose(key_pairs, (1, 0, 2)), heads)
+    split = jnp.transpose(
+        queries.reshape(tp_count, parts, sub, heads, width), (1, 3, 0, 2, 4)
+    ).reshape(sp_count, tokens // parts, width)
+    values, keys = spread(values), spread(keys)
+    split = spread(entries(split, sp_count))
+
     swap = [(i, i ^ 1) for i in range(tp_count)]
     mine = (gate_weight, up_weight, down_weight)
     other = tuple(lax.ppermute(w, "tp", swap) for w in mine)
 
-    split = jnp.transpose(
-        queries.reshape(tp_count, parts, sub, heads, width), (1, 3, 0, 2, 4)
-    ).reshape(sp_count, tokens // parts, width)
-    keys = jnp.tile(jnp.transpose(key_pairs, (1, 0, 2)), (parts, 1, 1))
-    values = jnp.tile(jnp.transpose(head_values, (1, 0, 2)), (parts, 1, 1))
-    arrived = lax.all_to_all(
-        jnp.concatenate([split, keys, values], axis=1), "sp", split_axis=0, concat_axis=0, tiled=True
-    )
     attended = attention(
+        place,
         (sp_index // heads).reshape(1),
         lax.dynamic_slice_in_dim(lambdas, sp_index % heads, 1),
         head_gain.reshape(1, -1),
-        arrived,
+        split,
+        keys,
+        values,
         sub,
-        tokens // parts,
         parts,
         (width // 2) ** (-0.5),
     )
@@ -393,7 +455,8 @@
         split_axis=0,
         concat_axis=0,
         tiled=True,
-    ).reshape(sp_count, tp_count, sub, width)
+    )
+    regrouped = regrouped.reshape(sp_count, tp_count, sub, width)
 
     share = jnp.sum(
         jnp.where(
@@ -412,24 +475,30 @@
     routes = jnp.concatenate(
         [coarse, share - coarse, ranks, jnp.zeros((rows, LANES - 3 * experts), jnp.float32)], axis=1
     ).astype(jnp.bfloat16)
-    updated, normed = project(
-        regrouped, out_weight, residual, norm_gain.reshape(1, -1), routes, parts
+    updated, normed, *picked = project(
+        place,
+        regrouped,
+        out_weight,
+        residual,
+        norm_gain.reshape(1, -1),
+        routes,
+        parts,
+        held,
+        experts,
+        capacity,
     )
 
     def turn(k):
         return [(i, (i + 2 * k) % tp_count) for i in range(tp_count)]
 
-    def across(array, column):
-        return lax.ppermute(array, "sp", [(i, i ^ column) for i in range(sp_count)])
-
     layers = tp_count // 2
-    capacity = row_capacity(rows, expert_ids.shape[1], experts)
-    place = sp_index.reshape(1)
     weights = (*mine, *other)
     blocks = [normed] + [lax.ppermute(normed, "tp", turn(-k)) for k in range(1, layers)]
     chosen, arrivals = [], []
-    for block in blocks:
-        coarse, fine, *sent = choose(place, block, sp_count, held, experts, capacity)
+    for k, block in enumerate(blocks):
+        coarse, fine, *sent = (
+            choose(place, block, sp_count, held, experts, capacity) if k else picked
+        )
         chosen.append((coarse, fine))
         arrivals.append([sent[0]] + [across(sent[c], c) for c in range(1, sp_count)])
     results = {}

time: 218 us -> 224 us (1.028)
  waiting for transfers between devices: 116 us -> 130 us
  starting transfers between devices: 50.8 us -> 42.7 us
    ppermute x24 -> x33, waiting for transfers between devices: 39.9 us -> 84.8 us  [across(): return lax.ppermute(array, 'sp', [(i, i ^ column) for i in range(sp_count)])]
    all_to_all x1 -> x0, waiting for transfers between devices: 22.5 us -> none  [balanced(): lax.all_to_all(jnp.concatenate([split, keys, values], axis=1), 'sp', spli...]
    ppermute x3, starting transfers between devices: 13.8 us -> 0.84 us  [balanced(): lax.ppermute(reduced[k], 'tp', turn(k))]
    ppermute x24 -> x33, starting transfers between devices: 25.5 us -> 35.7 us  [across(): return lax.ppermute(array, 'sp', [(i, i ^ column) for i in range(sp_count)])]
    ppermute x3, waiting for transfers between devices: 10.1 us -> 4.23 us  [balanced(): lax.ppermute(reduced[k], 'tp', turn(k))]
    all_to_all x1 -> x0, starting transfers between devices: 5.34 us -> none  [balanced(): lax.all_to_all(jnp.concatenate([split, keys, values], axis=1), 'sp', spli...]
    ppermute x3, waiting for transfers between devices: 30.5 us -> 28.1 us  [balanced(): lax.ppermute(normed, 'tp', turn(-k))]
  transfers between devices with their start and end apart: 35 -> 43, of which waited for: 14 -> 24; matrix products, arithmetic and copies ran while one was open for 1% -> 2% of each run, Pallas kernels for 19% -> 18%
where the time goes in v4:
time: 224 us; the launch traced here: 221 us
  waiting for transfers between devices  130 us (58%)
  starting transfers between devices  42.7 us (19%)
  Pallas kernels  40 us (18%)
  local copies, waits for them, and re-layouts  6.66 us (3%)
    ppermute x33, waiting for transfers between devices, across(): return lax.ppermute(array, 'sp', [(i, i ^ column) for i in range(sp_count)])  84.8 us
    ppermute x33, starting transfers between devices, across(): return lax.ppermute(array, 'sp', [(i, i ^ column) for i in range(sp_count)])  35.7 us
    ppermute x3, waiting for transfers between devices, balanced(): lax.ppermute(normed, 'tp', turn(-k))  28.1 us
    pallas_call x1, Pallas kernels, attention(): pl.pallas_call(functools.partial(attention_kernel, columns=columns, sub=s...  16.3 us
    pallas_call x2, Pallas kernels, expert_pass(): pl.pallas_call(functools.partial(expert_kernel, blocks=len(blocks)), out_...  15.6 us
    all_to_all x1, waiting for transfers between devices, balanced(): lax.all_to_all(attended.reshape(sp_count * tp_count, sub, width), ('sp',...  13.1 us
    all_to_all x1, starting transfers between devices, balanced(): lax.all_to_all(attended.reshape(sp_count * tp_count, sub, width), ('sp',...  4.9 us
  transfers between devices with their start and end apart: 43, of which 24 were waited for; matrix products, arithmetic and copies ran while one was open for 2% of the time, Pallas kernels for 18%

profile of v4, /device:TPU:0, one launch (start us, length us, event | category | flops | bytes accessed | tf_op | source)
XLA Modules:
  0.0 221.3 jit_solution(1024900762827704685)
XLA Ops:
  0.0 2.0 constant_dynamic-slice_fusion
  2.2 0.7 dynamic-slice_bitcast_fusion
  2.9 3.0 %collective-permute-start.3 = (bf16[768,128]{1,0:T(8,128)(2,1)}, bf16[768,128]{1,0:T(8,128)(2,1)}, u32[]{:S(2)}, u32[]{:S(2)}) collective-permute-start(bf16[768,128]{1,0:T(8,128)(2,1)} %get-tuple-element.97), channel_id=1, source_target_pairs={{0,8},{8,0},{16,24},{24,16},{1,9},{9,1},{17,25},{25,17},{2,10},{10... | collective-permute-start | bytes 589832 | tf_op jit(solution)/shard_map/ppermute | solution.py:415
  5.9 1.5 collective-permute-start.5
  7.5 0.7 dynamic-slice_bitcast_fusion.2
  8.1 1.5 collective-permute-start
  9.6 0.5 collective-permute-start.1
  10.1 1.5 collective-permute-start.2
  11.8 0.7 dynamic_slice.21.lam_ref
  12.4 0.7 copy.42
  13.1 5.1 %collective-permute-done.refs_1_ = bf16[384,128]{1,0:T(8,128)(2,1)S(1)} collective-permute-done((bf16[384,128]{1,0:T(8,128)(2,1)S(1)}, bf16[384,128]{1,0:T(8,128)(2,1)S(1)}, u32[]{:S(2)}, u32[]{:S(2)}) %collective-permute-start) | collective-permute-done | bytes 98336 | tf_op jit(solution)/shard_map/ppermute | solution.py:415
  18.2 1.9 collective-permute-start.6
  20.2 1.5 collective-permute-start.8
  21.8 1.9 collective-permute-start.7
  23.7 0.7 copy.43
  24.6 7.7 %collective-permute-done.4.refs_6_ = bf16[768,128]{1,0:T(8,128)(2,1)} collective-permute-done((bf16[768,128]{1,0:T(8,128)(2,1)S(1)}, bf16[768,128]{1,0:T(8,128)(2,1)}, u32[]{:S(2)}, u32[]{:S(2)}) %collective-permute-start.4) | collective-permute-done | bytes 196640 | tf_op jit(solution)/shard_map/ppermute | solution.py:415
  32.3 0.5 collective-permute-start.17
  32.9 1.9 collective-permute-done.7.refs_10_
  34.8 0.7 copy-done.12
  35.5 16.3 %attention.1 = bf16[1536,128]{1,0:T(8,128)(2,1)} custom-call(s32[1]{0:T(128)} %bitcast.place_ref, s32[1]{0:T(128)} %bitcast.1.part_ref, f32[1]{0:T(128)} %dynamic_slice.21.lam_ref, f32[1,128]{1,0:T(1,128)} %bitcast.32, bf16[384,128]{1,0:T(8,128)(2,1)} %get-tuple-element.102.refs_0_, bf16[384,128]{1,0:T(8,128)(2,1)} %copy-done.13, ...), custom_call_target="tpu_custom_call" | custom-call | flops 4831838208 | bytes 1179648 | tf_op jit(solution)/shard_map/attention/pallas_call | solution.py:122
  51.8 4.9 %all-to-all-start = ((bf16[32,48,128]{2,1,0:T(8,128)(2,1)}), bf16[32,48,128]{2,1,0:T(8,128)(2,1)S(1)}, u32[]{:S(2)}, u32[]{:S(2)}) async-start(bf16[32,48,128]{2,1,0:T(8,128)(2,1)} %bitcast.31), calls=%async_computation | async-start | bytes 786432 | tf_op jit(solution)/shard_map/all_to_all | solution.py:452
  57.1 13.1 %all-to-all-done = bf16[32,48,128]{2,1,0:T(8,128)(2,1)S(1)} async-done(((bf16[32,48,128]{2,1,0:T(8,128)(2,1)}), bf16[32,48,128]{2,1,0:T(8,128)(2,1)S(1)}, u32[]{:S(2)}, u32[]{:S(2)}) %all-to-all-start) | async-done | bytes 393248 | tf_op jit(solution)/shard_map/all_to_all | solution.py:452
  70.2 4.4 %project.1 = (bf16[96,2048]{1,0:T(8,128)(2,1)S(1)}, bf16[96,2176]{1,0:T(8,128)(2,1)S(1)}, bf16[96,256]{1,0:T(8,128)(2,1)S(1)}, bf16[96,256]{1,0:T(8,128)(2,1)S(1...) custom-call(s32[1]{0:T(128)} %bitcast.place_ref, ...), custom_call_target="tpu_custom_call" | custom-call | flops 805306368 | bytes 8388608 | tf_op jit(solution)/shard_map/project/pallas_call | solution.py:196
  74.6 0.6 collective-permute-start.10
  75.1 0.6 collective-permute-start.11
  75.7 12.9 %collective-permute-done.10.refs_2_ = bf16[64,2048]{1,0:T(8,128)(2,1)S(1)} collective-permute-done((bf16[64,2048]{1,0:T(8,128)(2,1)S(1)}, bf16[64,2048]{1,0:T(8,128)(2,1)S(1)}, u32[]{:S(2)}, u32[]{:S(2)}) %collective-permute-start.10) | collective-permute-done | bytes 262176 | tf_op jit(solution)/shard_map/ppermute | solution.py:415
  88.6 0.6 collective-permute-start.12
  89.2 1.4 collective-permute-start.9
  90.6 6.6 %collective-permute-done.9.refs_1_ = bf16[64,2048]{1,0:T(8,128)(2,1)S(1)} collective-permute-done((bf16[64,2048]{1,0:T(8,128)(2,1)S(1)}, bf16[64,2048]{1,0:T(8,128)(2,1)S(1)}, u32[]{:S(2)}, u32[]{:S(2)}) %collective-permute-start.9) | collective-permute-done | bytes 262176 | tf_op jit(solution)/shard_map/ppermute | solution.py:415
  97.2 2.1 collective-permute-done.12.block_ref
  99.4 0.6 choose.3
  100.0 26.0 %collective-permute-done.26.block_ref = bf16[96,2176]{1,0:T(8,128)(2,1)S(1)} collective-permute-done((bf16[96,2176]{1,0:T(8,128)(2,1)S(1)}, bf16[96,2176]{1,0:T(8,128)(2,1)S(1)}, u32[]{:S(2)}, u32[]{:S(2)}) %collective-permute-start.26) | collective-permute-done | bytes 417824 | tf_op jit(solution)/shard_map/ppermute | solution.py:496
  125.9 1.2 collective-permute-start.13
  127.2 0.5 collective-permute-start.14
  127.7 0.6 choose.4
  128.3 5.9 %collective-permute-done.13.refs_5_ = bf16[64,2048]{1,0:T(8,128)(2,1)S(1)} collective-permute-done((bf16[64,2048]{1,0:T(8,128)(2,1)S(1)}, bf16[64,2048]{1,0:T(8,128)(2,1)S(1)}, u32[]{:S(2)}, u32[]{:S(2)}) %collective-permute-start.13) | collective-permute-done | bytes 262176 | tf_op jit(solution)/shard_map/ppermute | solution.py:415
  134.6 1.3 collective-permute-start.31
  135.9 0.6 choose.5
  136.5 7.7 %collective-permute-done.15.refs_7_ = bf16[64,2048]{1,0:T(8,128)(2,1)S(1)} collective-permute-done((bf16[64,2048]{1,0:T(8,128)(2,1)S(1)}, bf16[64,2048]{1,0:T(8,128)(2,1)S(1)}, u32[]{:S(2)}, u32[]{:S(2)}) %collective-permute-start.15) | collective-permute-done | bytes 262176 | tf_op jit(solution)/shard_map/ppermute | solution.py:415
  144.3 1.4 collective-permute-done.31.refs_5_
  145.7 3.0 %collective-permute-start.33 = (bf16[64,2048]{1,0:T(8,128)(2,1)S(1)}, bf16[64,2048]{1,0:T(8,128)(2,1)S(1)}, u32[]{:S(2)}, u32[]{:S(2)}) collective-permute-start(bf16[64,2048]{1,0:T(8,128)(2,1)S(1)} %get-tuple-element.86), channel_id=1, source_target_pairs={{0,24},{8,16},{16,8},{24,0},{1,25},{9,17},{17,9},{25,1},{2,26},{10... | collective-permute-start | bytes 786440 | tf_op jit(solution)/shard_map/ppermute | solution.py:415
  148.6 2.5 %collective-permute-start.28 = (bf16[64,2048]{1,0:T(8,128)(2,1)S(1)}, bf16[64,2048]{1,0:T(8,128)(2,1)S(1)}, u32[]{:S(2)}, u32[]{:S(2)}) collective-permute-start(bf16[64,2048]{1,0:T(8,128)(2,1)S(1)} %get-tuple-element.80), channel_id=1, source_target_pairs={{0,8},{8,0},{16,24},{24,16},{1,9},{9,1},{17,25},{25,17},{2,10},{10... | collective-permute-start | bytes 786440 | tf_op jit(solution)/shard_map/ppermute | solution.py:415
  151.1 1.5 collective-permute-start.30
  152.7 7.8 %experts.2 = (bf16[64,2048]{1,0:T(8,128)(2,1)S(1)}, bf16[64,2048]{1,0:T(8,128)(2,1)S(1)}, bf16[64,2048]{1,0:T(8,128)(2,1)S(1)}, bf16[64,2048]{1,0:T(8,128)(2,1)S...) custom-call(bf16[64,2048]{1,0:T(8,128)(2,1)S(1)} %get-tuple-element., ...), custom_call_target="tpu_custom_call" | custom-call | flops 3221225472 | bytes 12582912 | tf_op jit(solution)/shard_map/experts/pallas_call | solution.py:366
  160.5 2.0 collective-permute-start.22
  162.6 1.3 collective-permute-done.28.refs_1_
  164.1 5.7 %collective-permute-done.29.refs_2_ = bf16[64,2048]{1,0:T(8,128)(2,1)S(1)} collective-permute-done((bf16[64,2048]{1,0:T(8,128)(2,1)S(1)}, bf16[64,2048]{1,0:T(8,128)(2,1)S(1)}, u32[]{:S(2)}, u32[]{:S(2)}) %collective-permute-start.29) | collective-permute-done | bytes 262176 | tf_op jit(solution)/shard_map/ppermute | solution.py:415
  169.8 7.8 %experts.3 = (bf16[64,2048]{1,0:T(8,128)(2,1)S(1)}, bf16[64,2048]{1,0:T(8,128)(2,1)S(1)}, bf16[64,2048]{1,0:T(8,128)(2,1)S(1)}, bf16[64,2048]{1,0:T(8,128)(2,1)S...) custom-call(bf16[64,2048]{1,0:T(8,128)(2,1)S(1)} %get-tuple-element., ...), custom_call_target="tpu_custom_call" | custom-call | flops 3221225472 | bytes 12582912 | tf_op jit(solution)/shard_map/experts/pallas_call | solution.py:366
  177.6 1.2 collective-permute-start.34
  179.1 2.1 collective-permute-start.36
  181.2 2.0 collective-permute-done.23.refs_2_
  183.1 3.7 %collective-permute-done.34.refs_1_ = bf16[64,2048]{1,0:T(8,128)(2,1)S(1)} collective-permute-done((bf16[64,2048]{1,0:T(8,128)(2,1)S(1)}, bf16[64,2048]{1,0:T(8,128)(2,1)S(1)}, u32[]{:S(2)}, u32[]{:S(2)}) %collective-permute-start.34) | collective-permute-done | bytes 262176 | tf_op jit(solution)/shard_map/ppermute | solution.py:415
  186.8 0.8 collective-permute-start.40
  187.6 6.8 %collective-permute-done.35.refs_2_ = bf16[64,2048]{1,0:T(8,128)(2,1)S(1)} collective-permute-done((bf16[64,2048]{1,0:T(8,128)(2,1)S(1)}, bf16[64,2048]{1,0:T(8,128)(2,1)S(1)}, u32[]{:S(2)}, u32[]{:S(2)}) %collective-permute-start.35) | collective-permute-done | bytes 262176 | tf_op jit(solution)/shard_map/ppermute | solution.py:415
  195.5 2.7 %collective-permute-done.38.refs_1_ = bf16[64,2048]{1,0:T(8,128)(2,1)S(1)} collective-permute-done((bf16[64,2048]{1,0:T(8,128)(2,1)S(1)}, bf16[64,2048]{1,0:T(8,128)(2,1)S(1)}, u32[]{:S(2)}, u32[]{:S(2)}) %collective-permute-start.38) | collective-permute-done | bytes 262176 | tf_op jit(solution)/shard_map/ppermute | solution.py:415
  198.1 0.7 collective-permute-start.37
  198.9 2.9 %collective-permute-done.40.refs_3_ = bf16[64,2048]{1,0:T(8,128)(2,1)S(1)} collective-permute-done((bf16[64,2048]{1,0:T(8,128)(2,1)S(1)}, bf16[64,2048]{1,0:T(8,128)(2,1)S(1)}, u32[]{:S(2)}, u32[]{:S(2)}) %collective-permute-start.40) | collective-permute-done | bytes 262176 | tf_op jit(solution)/shard_map/ppermute | solution.py:415
  202.3 3.1 %collective-permute-start.20 = (bf16[64,2048]{1,0:T(8,128)(2,1)S(1)}, bf16[64,2048]{1,0:T(8,128)(2,1)S(1)}, u32[]{:S(2)}, u32[]{:S(2)}) collective-permute-start(bf16[64,2048]{1,0:T(8,128)(2,1)S(1)} %get-tuple-element.69), channel_id=1, source_target_pairs={{0,16},{8,24},{16,0},{24,8},{1,17},{9,25},{17,1},{25,9},{2,18},{10... | collective-permute-start | bytes 786440 | tf_op jit(solution)/shard_map/ppermute | solution.py:415
  205.4 2.8 %collective-permute-done.19.refs_1_ = bf16[64,2048]{1,0:T(8,128)(2,1)S(1)} collective-permute-done((bf16[64,2048]{1,0:T(8,128)(2,1)S(1)}, bf16[64,2048]{1,0:T(8,128)(2,1)S(1)}, u32[]{:S(2)}, u32[]{:S(2)}) %collective-permute-start.19) | collective-permute-done | bytes 262176 | tf_op jit(solution)/shard_map/ppermute | solution.py:415
  208.2 3.9 %collective-permute-done.20.refs_2_ = bf16[64,2048]{1,0:T(8,128)(2,1)S(1)} collective-permute-done((bf16[64,2048]{1,0:T(8,128)(2,1)S(1)}, bf16[64,2048]{1,0:T(8,128)(2,1)S(1)}, u32[]{:S(2)}, u32[]{:S(2)}) %collective-permute-start.20) | collective-permute-done | bytes 262176 | tf_op jit(solution)/shard_map/ppermute | solution.py:415
  212.1 3.4 %collective-permute-done.21.refs_3_ = bf16[64,2048]{1,0:T(8,128)(2,1)S(1)} collective-permute-done((bf16[64,2048]{1,0:T(8,128)(2,1)S(1)}, bf16[64,2048]{1,0:T(8,128)(2,1)S(1)}, u32[]{:S(2)}, u32[]{:S(2)}) %collective-permute-start.21) | collective-permute-done | bytes 262176 | tf_op jit(solution)/shard_map/ppermute | solution.py:415
  216.0 2.4 %collective-permute-done.37 = bf16[96,2048]{1,0:T(8,128)(2,1)S(1)} collective-permute-done((bf16[96,2048]{1,0:T(8,128)(2,1)S(1)}, bf16[96,2048]{1,0:T(8,128)(2,1)S(1)}, u32[]{:S(2)}, u32[]{:S(2)}) %collective-permute-start.37) | collective-permute-done | bytes 393248 | tf_op jit(solution)/shard_map/ppermute | solution.py:516
  218.4 1.8 collective-permute-done.41
  220.2 1.1 add_convert_fusion
  (85 shorter events, 4.1 us)
Async XLA Ops:
  0.0 2.1 copy-start.3
  0.0 7.4 %copy-start.4 = (bf16[768,2,128]{2,1,0:T(2,128)(2,1)S(1)}, bf16[768,2,128]{2,1,0:T(2,128)(2,1)}, u32[]{:S(2)}) copy-start(bf16[768,2,128]{2,1,0:T(2,128)(2,1)} %param.13) | copy-start | bytes 1179652
  2.0 9.6 %copy-start.9 = (s32[96,2]{0,1:T(2,128)S(1)}, s32[96,2]{0,1:T(2,128)}, u32[]{:S(2)}) copy-start(s32[96,2]{0,1:T(2,128)} %param.21) | copy-start | bytes 2308
  2.0 9.6 %copy-start.10 = (f32[96,2]{0,1:T(2,128)S(1)}, f32[96,2]{0,1:T(2,128)}, u32[]{:S(2)}) copy-start(f32[96,2]{0,1:T(2,128)} %param.22) | copy-start | bytes 2308
  2.0 9.7 %copy-start.14 = (f32[2]{0:T(128)S(1)}, f32[2]{0:T(128)}, u32[]{:S(2)}) copy-start(f32[2]{0:T(128)} %param.16) | copy-start | bytes 28
  2.0 30.3 %copy-start = (bf16[2,2048,256]{2,1,0:T(8,128)(2,1)S(1)}, bf16[2,2048,256]{2,1,0:T(8,128)(2,1)}, u32[]{:S(2)}) copy-start(bf16[2,2048,256]{2,1,0:T(8,128)(2,1)} %refs_8_.3) | copy-start | bytes 6291460
  2.1 33.4 %copy-start.5 = (bf16[768,128]{1,0:T(8,128)(2,1)}, bf16[768,128]{1,0:T(8,128)(2,1)S(1)}, u32[]{:S(2)}) copy-start(bf16[768,128]{1,0:T(8,128)(2,1)S(1)} %get-tuple-element.53.refs_8_) | copy-start | bytes 589828
  2.9 32.6 %copy-start.6 = (bf16[768,128]{1,0:T(8,128)(2,1)}, bf16[768,128]{1,0:T(8,128)(2,1)S(1)}, u32[]{:S(2)}) copy-start(bf16[768,128]{1,0:T(8,128)(2,1)S(1)} %get-tuple-element.98.refs_4_) | copy-start | bytes 589828
  2.9 18.8 %collective-permute-start.3 = (bf16[768,128]{1,0:T(8,128)(2,1)}, bf16[768,128]{1,0:T(8,128)(2,1)}, u32[]{:S(2)}, u32[]{:S(2)}) collective-permute-start(bf16[768,128]{1,0:T(8,128)(2,1)} %get-tuple-element.97), channel_id=1, source_target_pairs={{0,8},{8,0},{16,24},{24,16},{1,9},{9,1},{17,25},{25,17},{2,10},{10... | collective-permute-start | bytes 589832 | tf_op jit(solution)/shard_map/ppermute | solution.py:415
  5.9 26.4 %collective-permute-start.5 = (bf16[768,128]{1,0:T(8,128)(2,1)}, bf16[768,128]{1,0:T(8,128)(2,1)}, u32[]{:S(2)}, u32[]{:S(2)}) collective-permute-start(bf16[768,128]{1,0:T(8,128)(2,1)} %get-tuple-element.97), channel_id=1, source_target_pairs={{0,24},{8,16},{16,8},{24,0},{1,25},{9,17},{17,9},{25,1},{2,26},{10... | collective-permute-start | bytes 589832 | tf_op jit(solution)/shard_map/ppermute | solution.py:415
  8.1 10.1 %collective-permute-start = (bf16[384,128]{1,0:T(8,128)(2,1)S(1)}, bf16[384,128]{1,0:T(8,128)(2,1)S(1)}, u32[]{:S(2)}, u32[]{:S(2)}) collective-permute-start(bf16[384,128]{1,0:T(8,128)(2,1)S(1)} %get-tuple-element.101), channel_id=1, source_target_pairs={{0,8},{8,0},{16,24},{24,16},{1,9},{9,1},{17,25},{25,17},{2,10},{10... | collective-permute-start | bytes 294920 | tf_op jit(solution)/shard_map/ppermute | solution.py:415
  9.6 10.5 %collective-permute-start.1 = (bf16[384,128]{1,0:T(8,128)(2,1)S(1)}, bf16[384,128]{1,0:T(8,128)(2,1)}, u32[]{:S(2)}, u32[]{:S(2)}) collective-permute-start(bf16[384,128]{1,0:T(8,128)(2,1)S(1)} %get-tuple-element.100), channel_id=1, source_target_pairs={{0,16},{8,24},{16,0},{24,8},{1,17},{9,25},{17,1},{25,9},{2,18},{10... | collective-permute-start | bytes 294920 | tf_op jit(solution)/shard_map/ppermute | solution.py:415
  10.1 11.5 %collective-permute-start.2 = (bf16[384,128]{1,0:T(8,128)(2,1)S(1)}, bf16[384,128]{1,0:T(8,128)(2,1)}, u32[]{:S(2)}, u32[]{:S(2)}) collective-permute-start(bf16[384,128]{1,0:T(8,128)(2,1)S(1)} %get-tuple-element.99), channel_id=1, source_target_pairs={{0,24},{8,16},{16,8},{24,0},{1,25},{9,17},{17,9},{25,1},{2,26},{10... | collective-permute-start | bytes 294920 | tf_op jit(solution)/shard_map/ppermute | solution.py:415
  18.2 17.3 %copy-start.13 = (bf16[384,128]{1,0:T(8,128)(2,1)}, bf16[384,128]{1,0:T(8,128)(2,1)S(1)}, u32[]{:S(2)}) copy-start(bf16[384,128]{1,0:T(8,128)(2,1)S(1)} %collective-permute-done.refs_1_) | copy-start | bytes 294916
  18.2 14.6 %collective-permute-start.6 = (bf16[768,128]{1,0:T(8,128)(2,1)S(1)}, bf16[768,128]{1,0:T(8,128)(2,1)S(1)}, u32[]{:S(2)}, u32[]{:S(2)}) collective-permute-start(bf16[768,128]{1,0:T(8,128)(2,1)S(1)} %get-tuple-element.54), channel_id=1, source_target_pairs={{0,8},{8,0},{16,24},{24,16},{1,9},{9,1},{17,25},{25,17},{2,10},{10... | collective-permute-start | bytes 589832 | tf_op jit(solution)/shard_map/ppermute | solution.py:415
  20.2 14.6 %collective-permute-start.8 = (bf16[768,128]{1,0:T(8,128)(2,1)S(1)}, bf16[768,128]{1,0:T(8,128)(2,1)S(1)}, u32[]{:S(2)}, u32[]{:S(2)}) collective-permute-start(bf16[768,128]{1,0:T(8,128)(2,1)S(1)} %get-tuple-element.54), channel_id=1, source_target_pairs={{0,24},{8,16},{16,8},{24,0},{1,25},{9,17},{17,9},{25,1},{2,26},{10... | collective-permute-start | bytes 589832 | tf_op jit(solution)/shard_map/ppermute | solution.py:415
  21.7 10.7 %collective-permute-start.4 = (bf16[768,128]{1,0:T(8,128)(2,1)S(1)}, bf16[768,128]{1,0:T(8,128)(2,1)}, u32[]{:S(2)}, u32[]{:S(2)}) collective-permute-start(bf16[768,128]{1,0:T(8,128)(2,1)S(1)} %get-tuple-element.98.refs_4_), channel_id=1, source_target_pairs={{0,16},{8,24},{16,0},{24,8},{1,17},{9,25},{17,1},{25,9},{2,18},{10... | collective-permute-start | bytes 589832 | tf_op jit(solution)/shard_map/ppermute | solution.py:415
  21.8 13.0 %collective-permute-start.7 = (bf16[768,128]{1,0:T(8,128)(2,1)S(1)}, bf16[768,128]{1,0:T(8,128)(2,1)}, u32[]{:S(2)}, u32[]{:S(2)}) collective-permute-start(bf16[768,128]{1,0:T(8,128)(2,1)S(1)} %get-tuple-element.53.refs_8_), channel_id=1, source_target_pairs={{0,16},{8,24},{16,0},{24,8},{1,17},{9,25},{17,1},{25,9},{2,18},{10... | collective-permute-start | bytes 589832 | tf_op jit(solution)/shard_map/ppermute | solution.py:415
  32.3 116.3 %collective-permute-start.16 = (bf16[2,2048,256]{2,1,0:T(8,128)(2,1)S(1)}, bf16[2,2048,256]{2,1,0:T(8,128)(2,1)}, u32[]{:S(2)}, u32[]{:S(2)}) collective-permute-start(bf16[2,2048,256]{2,1,0:T(8,128)(2,1)S(1)} %copy-done), channel_id=1, source_target_pairs={{0,1},{1,0},{2,3},{3,2},{4,5},{5,4},{6,7},{7,6},{8,9},{9,8},{10,11... | collective-permute-start | bytes 6291464 | tf_op jit(solution)/shard_map/ppermute | solution.py:438
  32.3 118.8 %collective-permute-start.17 = (bf16[2,2048,256]{2,1,0:T(8,128)(2,1)}, bf16[2,2048,256]{2,1,0:T(8,128)(2,1)}, u32[]{:S(2)}, u32[]{:S(2)}) collective-permute-start(bf16[2,2048,256]{2,1,0:T(8,128)(2,1)} %refs_9_.3), channel_id=1, source_target_pairs={{0,1},{1,0},{2,3},{3,2},{4,5},{5,4},{6,7},{7,6},{8,9},{9,8},{10,11... | collective-permute-start | bytes 6291464 | tf_op jit(solution)/shard_map/ppermute | solution.py:438
  32.8 2.7 %copy-start.11 = (bf16[768,128]{1,0:T(8,128)(2,1)}, bf16[768,128]{1,0:T(8,128)(2,1)S(1)}, u32[]{:S(2)}) copy-start(bf16[768,128]{1,0:T(8,128)(2,1)S(1)} %collective-permute-done.6.refs_9_) | copy-start | bytes 589828
  32.8 118.3 %collective-permute-start.18 = (bf16[2,256,2048]{2,1,0:T(8,128)(2,1)}, bf16[2,256,2048]{2,1,0:T(8,128)(2,1)}, u32[]{:S(2)}, u32[]{:S(2)}) collective-permute-start(bf16[2,256,2048]{2,1,0:T(8,128)(2,1)} %refs_10_.3), channel_id=1, source_target_pairs={{0,1},{1,0},{2,3},{3,2},{4,5},{5,4},{6,7},{7,6},{8,9},{9,8},{10,11... | collective-permute-start | bytes 6291464 | tf_op jit(solution)/shard_map/ppermute | solution.py:438
  34.8 0.7 copy-start.12
  35.5 21.3 %copy-start.7 = (f32[96,8]{1,0:T(8,128)S(1)}, f32[96,8]{1,0:T(8,128)}, u32[]{:S(2)}) copy-start(f32[96,8]{1,0:T(8,128)} %copy.42) | copy-start | bytes 9220
  35.5 21.3 %copy-start.8 = (pred[96,8]{1,0:T(8,128)(4,1)S(1)}, pred[96,8]{1,0:T(8,128)(4,1)}, u32[]{:S(2)}) copy-start(pred[96,8]{1,0:T(8,128)(4,1)} %copy.43) | copy-start | bytes 2308
  35.5 34.7 %copy-start.1 = (bf16[96,2048]{1,0:T(8,128)(2,1)S(1)}, bf16[96,2048]{1,0:T(8,128)(2,1)}, u32[]{:S(2)}) copy-start(bf16[96,2048]{1,0:T(8,128)(2,1)} %residual_ref.1) | copy-start | bytes 1179652
  35.5 34.7 %copy-start.2 = (f32[2048]{0:T(1024)S(1)}, f32[2048]{0:T(1024)}, u32[]{:S(2)}) copy-start(f32[2048]{0:T(1024)} %param.20) | copy-start | bytes 24580
  51.8 18.3 %all-to-all-start = ((bf16[32,48,128]{2,1,0:T(8,128)(2,1)}), bf16[32,48,128]{2,1,0:T(8,128)(2,1)S(1)}, u32[]{:S(2)}, u32[]{:S(2)}) async-start(bf16[32,48,128]{2,1,0:T(8,128)(2,1)} %bitcast.31), calls=%async_computation | async-start | bytes 786432 | tf_op jit(solution)/shard_map/all_to_all | solution.py:452
  74.6 14.0 %collective-permute-start.10 = (bf16[64,2048]{1,0:T(8,128)(2,1)S(1)}, bf16[64,2048]{1,0:T(8,128)(2,1)S(1)}, u32[]{:S(2)}, u32[]{:S(2)}) collective-permute-start(bf16[64,2048]{1,0:T(8,128)(2,1)S(1)} %get-tuple-element.60), channel_id=1, source_target_pairs={{0,16},{8,24},{16,0},{24,8},{1,17},{9,25},{17,1},{25,9},{2,18},{10... | collective-permute-start | bytes 786440 | tf_op jit(solution)/shard_map/ppermute | solution.py:415
  75.1 14.0 %collective-permute-start.11 = (bf16[64,2048]{1,0:T(8,128)(2,1)S(1)}, bf16[64,2048]{1,0:T(8,128)(2,1)S(1)}, u32[]{:S(2)}, u32[]{:S(2)}) collective-permute-start(bf16[64,2048]{1,0:T(8,128)(2,1)S(1)} %get-tuple-element.61), channel_id=1, source_target_pairs={{0,24},{8,16},{16,8},{24,0},{1,25},{9,17},{17,9},{25,1},{2,26},{10... | collective-permute-start | bytes 786440 | tf_op jit(solution)/shard_map/ppermute | solution.py:415
  88.6 10.8 %collective-permute-start.12 = (bf16[96,2176]{1,0:T(8,128)(2,1)S(1)}, bf16[96,2176]{1,0:T(8,128)(2,1)S(1)}, u32[]{:S(2)}, u32[]{:S(2)}) collective-permute-start(bf16[96,2176]{1,0:T(8,128)(2,1)S(1)} %get-tuple-element.62), channel_id=1, source_target_pairs={{0,6},{1,7},{2,0},{3,1},{4,2},{5,3},{6,4},{7,5},{8,14},{9,15},{10,... | collective-permute-start | bytes 1253384 | tf_op jit(solution)/shard_map/ppermute | solution.py:496
  89.2 8.0 %collective-permute-start.9 = (bf16[64,2048]{1,0:T(8,128)(2,1)S(1)}, bf16[64,2048]{1,0:T(8,128)(2,1)S(1)}, u32[]{:S(2)}, u32[]{:S(2)}) collective-permute-start(bf16[64,2048]{1,0:T(8,128)(2,1)S(1)} %get-tuple-element.59), channel_id=1, source_target_pairs={{0,8},{8,0},{16,24},{24,16},{1,9},{9,1},{17,25},{25,17},{2,10},{10... | collective-permute-start | bytes 786440 | tf_op jit(solution)/shard_map/ppermute | solution.py:415
  97.2 28.7 %collective-permute-start.26 = (bf16[96,2176]{1,0:T(8,128)(2,1)S(1)}, bf16[96,2176]{1,0:T(8,128)(2,1)S(1)}, u32[]{:S(2)}, u32[]{:S(2)}) collective-permute-start(bf16[96,2176]{1,0:T(8,128)(2,1)S(1)} %get-tuple-element.62), channel_id=1, source_target_pairs={{0,4},{1,5},{2,6},{3,7},{4,0},{5,1},{6,2},{7,3},{8,12},{9,13},{10,... | collective-permute-start | bytes 1253384 | tf_op jit(solution)/shard_map/ppermute | solution.py:496
  99.4 27.8 %collective-permute-start.27 = (bf16[96,2176]{1,0:T(8,128)(2,1)S(1)}, bf16[96,2176]{1,0:T(8,128)(2,1)S(1)}, u32[]{:S(2)}, u32[]{:S(2)}) collective-permute-start(bf16[96,2176]{1,0:T(8,128)(2,1)S(1)} %get-tuple-element.62), channel_id=1, source_target_pairs={{0,2},{1,3},{2,4},{3,5},{4,6},{5,7},{6,0},{7,1},{8,10},{9,11},{10,... | collective-permute-start | bytes 1253384 | tf_op jit(solution)/shard_map/ppermute | solution.py:496
  125.9 8.2 %collective-permute-start.13 = (bf16[64,2048]{1,0:T(8,128)(2,1)S(1)}, bf16[64,2048]{1,0:T(8,128)(2,1)S(1)}, u32[]{:S(2)}, u32[]{:S(2)}) collective-permute-start(bf16[64,2048]{1,0:T(8,128)(2,1)S(1)} %get-tuple-element.64), channel_id=1, source_target_pairs={{0,8},{8,0},{16,24},{24,16},{1,9},{9,1},{17,25},{25,17},{2,10},{10... | collective-permute-start | bytes 786440 | tf_op jit(solution)/shard_map/ppermute | solution.py:415
  127.2 7.5 %collective-permute-start.14 = (bf16[64,2048]{1,0:T(8,128)(2,1)S(1)}, bf16[64,2048]{1,0:T(8,128)(2,1)S(1)}, u32[]{:S(2)}, u32[]{:S(2)}) collective-permute-start(bf16[64,2048]{1,0:T(8,128)(2,1)S(1)} %get-tuple-element.65), channel_id=1, source_target_pairs={{0,16},{8,24},{16,0},{24,8},{1,17},{9,25},{17,1},{25,9},{2,18},{10... | collective-permute-start | bytes 786440 | tf_op jit(solution)/shard_map/ppermute | solution.py:415
  134.2 10.1 %collective-permute-start.15 = (bf16[64,2048]{1,0:T(8,128)(2,1)S(1)}, bf16[64,2048]{1,0:T(8,128)(2,1)S(1)}, u32[]{:S(2)}, u32[]{:S(2)}) collective-permute-start(bf16[64,2048]{1,0:T(8,128)(2,1)S(1)} %get-tuple-element.66), channel_id=1, source_target_pairs={{0,24},{8,16},{16,8},{24,0},{1,25},{9,17},{17,9},{25,1},{2,26},{10... | collective-permute-start | bytes 786440 | tf_op jit(solution)/shard_map/ppermute | solution.py:415
  134.6 11.0 %collective-permute-start.31 = (bf16[64,2048]{1,0:T(8,128)(2,1)S(1)}, bf16[64,2048]{1,0:T(8,128)(2,1)S(1)}, u32[]{:S(2)}, u32[]{:S(2)}) collective-permute-start(bf16[64,2048]{1,0:T(8,128)(2,1)S(1)} %get-tuple-element.84), channel_id=1, source_target_pairs={{0,8},{8,0},{16,24},{24,16},{1,9},{9,1},{17,25},{25,17},{2,10},{10... | collective-permute-start | bytes 786440 | tf_op jit(solution)/shard_map/ppermute | solution.py:415
  144.3 16.2 %collective-permute-start.32 = (bf16[64,2048]{1,0:T(8,128)(2,1)S(1)}, bf16[64,2048]{1,0:T(8,128)(2,1)S(1)}, u32[]{:S(2)}, u32[]{:S(2)}) collective-permute-start(bf16[64,2048]{1,0:T(8,128)(2,1)S(1)} %get-tuple-element.85), channel_id=1, source_target_pairs={{0,16},{8,24},{16,0},{24,8},{1,17},{9,25},{17,1},{25,9},{2,18},{10... | collective-permute-start | bytes 786440 | tf_op jit(solution)/shard_map/ppermute | solution.py:415
  145.7 16.8 %collective-permute-start.33 = (bf16[64,2048]{1,0:T(8,128)(2,1)S(1)}, bf16[64,2048]{1,0:T(8,128)(2,1)S(1)}, u32[]{:S(2)}, u32[]{:S(2)}) collective-permute-start(bf16[64,2048]{1,0:T(8,128)(2,1)S(1)} %get-tuple-element.86), channel_id=1, source_target_pairs={{0,24},{8,16},{16,8},{24,0},{1,25},{9,17},{17,9},{25,1},{2,26},{10... | collective-permute-start | bytes 786440 | tf_op jit(solution)/shard_map/ppermute | solution.py:415
  148.6 15.3 %collective-permute-start.28 = (bf16[64,2048]{1,0:T(8,128)(2,1)S(1)}, bf16[64,2048]{1,0:T(8,128)(2,1)S(1)}, u32[]{:S(2)}, u32[]{:S(2)}) collective-permute-start(bf16[64,2048]{1,0:T(8,128)(2,1)S(1)} %get-tuple-element.80), channel_id=1, source_target_pairs={{0,8},{8,0},{16,24},{24,16},{1,9},{9,1},{17,25},{25,17},{2,10},{10... | collective-permute-start | bytes 786440 | tf_op jit(solution)/shard_map/ppermute | solution.py:415
  151.1 18.7 %collective-permute-start.29 = (bf16[64,2048]{1,0:T(8,128)(2,1)S(1)}, bf16[64,2048]{1,0:T(8,128)(2,1)S(1)}, u32[]{:S(2)}, u32[]{:S(2)}) collective-permute-start(bf16[64,2048]{1,0:T(8,128)(2,1)S(1)} %get-tuple-element.81), channel_id=1, source_target_pairs={{0,16},{8,24},{16,0},{24,8},{1,17},{9,25},{17,1},{25,9},{2,18},{10... | collective-permute-start | bytes 786440 | tf_op jit(solution)/shard_map/ppermute | solution.py:415
  151.1 18.7 %collective-permute-start.30 = (bf16[64,2048]{1,0:T(8,128)(2,1)S(1)}, bf16[64,2048]{1,0:T(8,128)(2,1)S(1)}, u32[]{:S(2)}, u32[]{:S(2)}) collective-permute-start(bf16[64,2048]{1,0:T(8,128)(2,1)S(1)} %get-tuple-element.82), channel_id=1, source_target_pairs={{0,24},{8,16},{16,8},{24,0},{1,25},{9,17},{17,9},{25,1},{2,26},{10... | collective-permute-start | bytes 786440 | tf_op jit(solution)/shard_map/ppermute | solution.py:415
  160.5 18.6 %collective-permute-start.22 = (bf16[64,2048]{1,0:T(8,128)(2,1)S(1)}, bf16[64,2048]{1,0:T(8,128)(2,1)S(1)}, u32[]{:S(2)}, u32[]{:S(2)}) collective-permute-start(bf16[64,2048]{1,0:T(8,128)(2,1)S(1)} %get-tuple-element.74), channel_id=1, source_target_pairs={{0,8},{8,0},{16,24},{24,16},{1,9},{9,1},{17,25},{25,17},{2,10},{10... | collective-permute-start | bytes 786440 | tf_op jit(solution)/shard_map/ppermute | solution.py:415
  162.5 20.6 %collective-permute-start.23 = (bf16[64,2048]{1,0:T(8,128)(2,1)S(1)}, bf16[64,2048]{1,0:T(8,128)(2,1)S(1)}, u32[]{:S(2)}, u32[]{:S(2)}) collective-permute-start(bf16[64,2048]{1,0:T(8,128)(2,1)S(1)} %get-tuple-element.75), channel_id=1, source_target_pairs={{0,16},{8,24},{16,0},{24,8},{1,17},{9,25},{17,1},{25,9},{2,18},{10... | collective-permute-start | bytes 786440 | tf_op jit(solution)/shard_map/ppermute | solution.py:415
  163.9 19.2 %collective-permute-start.24 = (bf16[64,2048]{1,0:T(8,128)(2,1)S(1)}, bf16[64,2048]{1,0:T(8,128)(2,1)S(1)}, u32[]{:S(2)}, u32[]{:S(2)}) collective-permute-start(bf16[64,2048]{1,0:T(8,128)(2,1)S(1)} %get-tuple-element.76), channel_id=1, source_target_pairs={{0,24},{8,16},{16,8},{24,0},{1,25},{9,17},{17,9},{25,1},{2,26},{10... | collective-permute-start | bytes 786440 | tf_op jit(solution)/shard_map/ppermute | solution.py:415
  177.6 9.2 %collective-permute-start.34 = (bf16[64,2048]{1,0:T(8,128)(2,1)S(1)}, bf16[64,2048]{1,0:T(8,128)(2,1)S(1)}, u32[]{:S(2)}, u32[]{:S(2)}) collective-permute-start(bf16[64,2048]{1,0:T(8,128)(2,1)S(1)} %get-tuple-element.88), channel_id=1, source_target_pairs={{0,8},{8,0},{16,24},{24,16},{1,9},{9,1},{17,25},{25,17},{2,10},{10... | collective-permute-start | bytes 786440 | tf_op jit(solution)/shard_map/ppermute | solution.py:415
  178.8 15.6 %collective-permute-start.35 = (bf16[64,2048]{1,0:T(8,128)(2,1)S(1)}, bf16[64,2048]{1,0:T(8,128)(2,1)S(1)}, u32[]{:S(2)}, u32[]{:S(2)}) collective-permute-start(bf16[64,2048]{1,0:T(8,128)(2,1)S(1)} %get-tuple-element.89), channel_id=1, source_target_pairs={{0,16},{8,24},{16,0},{24,8},{1,17},{9,25},{17,1},{25,9},{2,18},{10... | collective-permute-start | bytes 786440 | tf_op jit(solution)/shard_map/ppermute | solution.py:415
  179.1 15.9 %collective-permute-start.36 = (bf16[64,2048]{1,0:T(8,128)(2,1)S(1)}, bf16[64,2048]{1,0:T(8,128)(2,1)S(1)}, u32[]{:S(2)}, u32[]{:S(2)}) collective-permute-start(bf16[64,2048]{1,0:T(8,128)(2,1)S(1)} %get-tuple-element.90), channel_id=1, source_target_pairs={{0,24},{8,16},{16,8},{24,0},{1,25},{9,17},{17,9},{25,1},{2,26},{10... | collective-permute-start | bytes 786440 | tf_op jit(solution)/shard_map/ppermute | solution.py:415
  183.1 15.0 %collective-permute-start.38 = (bf16[64,2048]{1,0:T(8,128)(2,1)S(1)}, bf16[64,2048]{1,0:T(8,128)(2,1)S(1)}, u32[]{:S(2)}, u32[]{:S(2)}) collective-permute-start(bf16[64,2048]{1,0:T(8,128)(2,1)S(1)} %get-tuple-element.94), channel_id=1, source_target_pairs={{0,8},{8,0},{16,24},{24,16},{1,9},{9,1},{17,25},{25,17},{2,10},{10... | collective-permute-start | bytes 786440 | tf_op jit(solution)/shard_map/ppermute | solution.py:415
  183.1 15.7 %collective-permute-start.39 = (bf16[64,2048]{1,0:T(8,128)(2,1)S(1)}, bf16[64,2048]{1,0:T(8,128)(2,1)S(1)}, u32[]{:S(2)}, u32[]{:S(2)}) collective-permute-start(bf16[64,2048]{1,0:T(8,128)(2,1)S(1)} %get-tuple-element.95), channel_id=1, source_target_pairs={{0,16},{8,24},{16,0},{24,8},{1,17},{9,25},{17,1},{25,9},{2,18},{10... | collective-permute-start | bytes 786440 | tf_op jit(solution)/shard_map/ppermute | solution.py:415
  186.8 14.9 %collective-permute-start.40 = (bf16[64,2048]{1,0:T(8,128)(2,1)S(1)}, bf16[64,2048]{1,0:T(8,128)(2,1)S(1)}, u32[]{:S(2)}, u32[]{:S(2)}) collective-permute-start(bf16[64,2048]{1,0:T(8,128)(2,1)S(1)} %get-tuple-element.96), channel_id=1, source_target_pairs={{0,24},{8,16},{16,8},{24,0},{1,25},{9,17},{17,9},{25,1},{2,26},{10... | collective-permute-start | bytes 786440 | tf_op jit(solution)/shard_map/ppermute | solution.py:415
  194.4 13.8 %collective-permute-start.19 = (bf16[64,2048]{1,0:T(8,128)(2,1)S(1)}, bf16[64,2048]{1,0:T(8,128)(2,1)S(1)}, u32[]{:S(2)}, u32[]{:S(2)}) collective-permute-start(bf16[64,2048]{1,0:T(8,128)(2,1)S(1)} %get-tuple-element.68), channel_id=1, source_target_pairs={{0,8},{8,0},{16,24},{24,16},{1,9},{9,1},{17,25},{25,17},{2,10},{10... | collective-permute-start | bytes 786440 | tf_op jit(solution)/shard_map/ppermute | solution.py:415
  194.9 21.0 %collective-permute-start.25 = (bf16[96,2048]{1,0:T(8,128)(2,1)S(1)}, bf16[96,2048]{1,0:T(8,128)(2,1)S(1)}, u32[]{:S(2)}, u32[]{:S(2)}) collective-permute-start(bf16[96,2048]{1,0:T(8,128)(2,1)S(1)} %merge.5), channel_id=1, source_target_pairs={{0,2},{1,3},{2,4},{3,5},{4,6},{5,7},{6,0},{7,1},{8,10},{9,11},{10,... | collective-permute-start | bytes 1179656 | tf_op jit(solution)/shard_map/ppermute | solution.py:516
  198.1 20.2 %collective-permute-start.37 = (bf16[96,2048]{1,0:T(8,128)(2,1)S(1)}, bf16[96,2048]{1,0:T(8,128)(2,1)S(1)}, u32[]{:S(2)}, u32[]{:S(2)}) collective-permute-start(bf16[96,2048]{1,0:T(8,128)(2,1)S(1)} %merge.6), channel_id=1, source_target_pairs={{0,4},{1,5},{2,6},{3,7},{4,0},{5,1},{6,2},{7,3},{8,12},{9,13},{10,... | collective-permute-start | bytes 1179656 | tf_op jit(solution)/shard_map/ppermute | solution.py:516
  202.2 18.0 %collective-permute-start.41 = (bf16[96,2048]{1,0:T(8,128)(2,1)S(1)}, bf16[96,2048]{1,0:T(8,128)(2,1)S(1)}, u32[]{:S(2)}, u32[]{:S(2)}) collective-permute-start(bf16[96,2048]{1,0:T(8,128)(2,1)S(1)} %merge.7), channel_id=1, source_target_pairs={{0,6},{1,7},{2,0},{3,1},{4,2},{5,3},{6,4},{7,5},{8,14},{9,15},{10,... | collective-permute-start | bytes 1179656 | tf_op jit(solution)/shard_map/ppermute | solution.py:516
  202.3 9.8 %collective-permute-start.20 = (bf16[64,2048]{1,0:T(8,128)(2,1)S(1)}, bf16[64,2048]{1,0:T(8,128)(2,1)S(1)}, u32[]{:S(2)}, u32[]{:S(2)}) collective-permute-start(bf16[64,2048]{1,0:T(8,128)(2,1)S(1)} %get-tuple-element.69), channel_id=1, source_target_pairs={{0,16},{8,24},{16,0},{24,8},{1,17},{9,25},{17,1},{25,9},{2,18},{10... | collective-permute-start | bytes 786440 | tf_op jit(solution)/shard_map/ppermute | solution.py:415
  208.2 7.3 %collective-permute-start.21 = (bf16[64,2048]{1,0:T(8,128)(2,1)S(1)}, bf16[64,2048]{1,0:T(8,128)(2,1)S(1)}, u32[]{:S(2)}, u32[]{:S(2)}) collective-permute-start(bf16[64,2048]{1,0:T(8,128)(2,1)S(1)} %get-tuple-element.70), channel_id=1, source_target_pairs={{0,24},{8,16},{16,8},{24,0},{1,25},{9,17},{17,9},{25,1},{2,26},{10... | collective-permute-start | bytes 786440 | tf_op jit(solution)/shard_map/ppermute | solution.py:415

commit v5 on v4

--- a/solution.py
+++ b/solution.py
@@ -287,8 +287,9 @@
     for column, ref in enumerate(refs[:-2]):
         kept_ref[column * slots : (column + 1) * slots, :] = ref[...]
     kept = kept_ref[...]
-    total = jnp.dot(coarse_ref[...], kept, preferred_element_type=jnp.float32)
-    total += jnp.dot(fine_ref[...], kept, preferred_element_type=jnp.float32)
+    used = kept.shape[0]
+    total = jnp.dot(coarse_ref[...][:, :used], kept, preferred_element_type=jnp.float32)
+    total += jnp.dot(fine_ref[...][:, :used], kept, preferred_element_type=jnp.float32)
     out_ref[...] = total.astype(out_ref.dtype)
 
 
@@ -301,7 +302,7 @@
         out_shape=jax.ShapeDtypeStruct((rows, model), jnp.bfloat16),
         in_specs=[whole] * (2 + len(parts)),
         out_specs=whole,
-        scratch_shapes=[pltpu.VMEM((coarse.shape[1], model), jnp.bfloat16)],
+        scratch_shapes=[pltpu.VMEM((len(parts) * parts[0].shape[0], model), jnp.bfloat16)],
         compiler_params=pltpu.CompilerParams(vmem_limit_bytes=16 * 1024 * 1024),
         cost_estimate=pl.CostEstimate(
             flops=4 * rows * coarse.shape[1] * model, bytes_accessed=4 * rows * model, transcendentals=0
@@ -508,10 +509,13 @@
         done = expert_pass(rows_in, weights)
         for i, k in enumerate(group):
             results[k] = done[i * sp_count : (i + 1) * sp_count]
+    results = {k: list(result) for k, result in results.items()}
+    passed = lax.ppermute(results[near[0]].pop(), "tp", turn(near[0]))
+    results[0][-1] = summed_rows(results[0][-1], passed)
     reduced = []
     for k in range(layers):
         result = results[k]
-        back = [result[0]] + [across(result[c], c) for c in range(1, sp_count)]
+        back = [result[0]] + [across(result[c], c) for c in range(1, len(result))]
         reduced.append(merge(*chosen[k], back))
     returned = [lax.ppermute(reduced[k], "tp", turn(k)) for k in range(1, layers)]
     return summed_rows(updated, reduced[0], *returned)

time: 224 us -> 230 us (1.027)
  the two profiles are of different devices: /device:TPU:0 before, /device:TPU:28 now
where the time goes in v5:
time: 230 us; the launch traced here: 229 us
  waiting for transfers between devices  100 us (43%)
  starting transfers between devices  81 us (35%)
  Pallas kernels  39.9 us (17%)
  local copies, waits for them, and re-layouts  6.66 us (3%)
    ppermute x32, waiting for transfers between devices, across(): return lax.ppermute(array, 'sp', [(i, i ^ column) for i in range(sp_count)])  58.2 us
    ppermute x32, starting transfers between devices, across(): return lax.ppermute(array, 'sp', [(i, i ^ column) for i in range(sp_count)])  49.8 us
    ppermute x3, waiting for transfers between devices, balanced(): lax.ppermute(normed, 'tp', turn(-k))  18.5 us
    pallas_call x1, Pallas kernels, attention(): pl.pallas_call(functools.partial(attention_kernel, columns=columns, sub=s...  16.3 us
    pallas_call x2, Pallas kernels, expert_pass(): pl.pallas_call(functools.partial(expert_kernel, blocks=len(blocks)), out_...  15.6 us
    ppermute x3, waiting for transfers between devices, balanced(): lax.ppermute(reduced[k], 'tp', turn(k))  13.8 us
    ppermute x3, starting transfers between devices, balanced(): lax.ppermute(reduced[k], 'tp', turn(k))  13 us
    all_to_all x1, waiting for transfers between devices, balanced(): lax.all_to_all(attended.reshape(sp_count * tp_count, sub, width), ('sp',...  9.57 us
  transfers between devices with their start and end apart: 43, of which 16 were waited for; matrix products, arithmetic and copies ran while one was open for 2% of the time, Pallas kernels for 17%

profile of v5, /device:TPU:28, one launch (start us, length us, event | category | flops | bytes accessed | tf_op | source)
XLA Modules:
  0.0 229.5 jit_solution(13677979181954135684)
XLA Ops:
  0.0 2.0 constant_dynamic-slice_fusion
  2.2 0.7 dynamic-slice_bitcast_fusion
  2.9 1.5 collective-permute-start.3
  5.0 0.7 dynamic-slice_bitcast_fusion.2
  5.7 1.5 collective-permute-start
  7.1 1.5 collective-permute-start.1
  9.3 0.7 dynamic_slice.21.lam_ref
  9.9 0.7 copy.42
  10.6 6.5 %collective-permute-done.refs_1_ = bf16[384,128]{1,0:T(8,128)(2,1)S(1)} collective-permute-done((bf16[384,128]{1,0:T(8,128)(2,1)S(1)}, bf16[384,128]{1,0:T(8,128)(2,1)S(1)}, u32[]{:S(2)}, u32[]{:S(2)}) %collective-permute-start) | collective-permute-done | bytes 98336 | tf_op jit(solution)/shard_map/ppermute | solution.py:416
  17.2 1.5 collective-permute-start.6
  19.2 1.5 collective-permute-start.4
  20.7 0.5 collective-permute-start.7
  21.2 0.7 copy.43
  22.1 7.7 %collective-permute-done.4.refs_6_ = bf16[768,128]{1,0:T(8,128)(2,1)} collective-permute-done((bf16[768,128]{1,0:T(8,128)(2,1)S(1)}, bf16[768,128]{1,0:T(8,128)(2,1)}, u32[]{:S(2)}, u32[]{:S(2)}) %collective-permute-start.4) | collective-permute-done | bytes 196640 | tf_op jit(solution)/shard_map/ppermute | solution.py:416
  29.8 0.5 collective-permute-start.17
  30.4 1.9 collective-permute-done.7.refs_10_
  32.3 0.7 copy-done.12
  33.1 16.3 %attention.1 = bf16[1536,128]{1,0:T(8,128)(2,1)} custom-call(s32[1]{0:T(128)} %bitcast.place_ref, s32[1]{0:T(128)} %bitcast.1.part_ref, f32[1]{0:T(128)} %dynamic_slice.21.lam_ref, f32[1,128]{1,0:T(1,128)} %bitcast.32, bf16[384,128]{1,0:T(8,128)(2,1)} %get-tuple-element.102.refs_0_, bf16[384,128]{1,0:T(8,128)(2,1)} %copy-done.13, ...), custom_call_target="tpu_custom_call" | custom-call | flops 4831838208 | bytes 1179648 | tf_op jit(solution)/shard_map/attention/pallas_call | solution.py:122
  49.4 5.9 %all-to-all-start = ((bf16[32,48,128]{2,1,0:T(8,128)(2,1)}), bf16[32,48,128]{2,1,0:T(8,128)(2,1)S(1)}, u32[]{:S(2)}, u32[]{:S(2)}) async-start(bf16[32,48,128]{2,1,0:T(8,128)(2,1)} %bitcast.31), calls=%async_computation | async-start | bytes 786432 | tf_op jit(solution)/shard_map/all_to_all | solution.py:453
  55.6 9.6 %all-to-all-done = bf16[32,48,128]{2,1,0:T(8,128)(2,1)S(1)} async-done(((bf16[32,48,128]{2,1,0:T(8,128)(2,1)}), bf16[32,48,128]{2,1,0:T(8,128)(2,1)S(1)}, u32[]{:S(2)}, u32[]{:S(2)}) %all-to-all-start) | async-done | bytes 393248 | tf_op jit(solution)/shard_map/all_to_all | solution.py:453
  65.2 4.4 %project.1 = (bf16[96,2048]{1,0:T(8,128)(2,1)S(1)}, bf16[96,2176]{1,0:T(8,128)(2,1)S(1)}, bf16[96,256]{1,0:T(8,128)(2,1)S(1)}, bf16[96,256]{1,0:T(8,128)(2,1)S(1...) custom-call(s32[1]{0:T(128)} %bitcast.place_ref, ...), custom_call_target="tpu_custom_call" | custom-call | flops 805306368 | bytes 8388608 | tf_op jit(solution)/shard_map/project/pallas_call | solution.py:196
  70.0 2.6 %collective-permute-start.11 = (bf16[64,2048]{1,0:T(8,128)(2,1)S(1)}, bf16[64,2048]{1,0:T(8,128)(2,1)S(1)}, u32[]{:S(2)}, u32[]{:S(2)}) collective-permute-start(bf16[64,2048]{1,0:T(8,128)(2,1)S(1)} %get-tuple-element.61), channel_id=1, source_target_pairs={{0,24},{8,16},{16,8},{24,0},{1,25},{9,17},{17,9},{25,1},{2,26},{10... | collective-permute-start | bytes 786440 | tf_op jit(solution)/shard_map/ppermute | solution.py:416
  72.5 10.9 %collective-permute-done.10.refs_2_ = bf16[64,2048]{1,0:T(8,128)(2,1)S(1)} collective-permute-done((bf16[64,2048]{1,0:T(8,128)(2,1)S(1)}, bf16[64,2048]{1,0:T(8,128)(2,1)S(1)}, u32[]{:S(2)}, u32[]{:S(2)}) %collective-permute-start.10) | collective-permute-done | bytes 262176 | tf_op jit(solution)/shard_map/ppermute | solution.py:416
  83.5 1.1 collective-permute-start.12
  84.6 0.7 collective-permute-start.9
  85.4 6.4 %collective-permute-done.9.refs_1_ = bf16[64,2048]{1,0:T(8,128)(2,1)S(1)} collective-permute-done((bf16[64,2048]{1,0:T(8,128)(2,1)S(1)}, bf16[64,2048]{1,0:T(8,128)(2,1)S(1)}, u32[]{:S(2)}, u32[]{:S(2)}) %collective-permute-start.9) | collective-permute-done | bytes 262176 | tf_op jit(solution)/shard_map/ppermute | solution.py:416
  91.8 2.9 %collective-permute-start.26 = (bf16[96,2176]{1,0:T(8,128)(2,1)S(1)}, bf16[96,2176]{1,0:T(8,128)(2,1)S(1)}, u32[]{:S(2)}, u32[]{:S(2)}) collective-permute-start(bf16[96,2176]{1,0:T(8,128)(2,1)S(1)} %get-tuple-element.62), channel_id=1, source_target_pairs={{0,4},{1,5},{2,6},{3,7},{4,0},{5,1},{6,2},{7,3},{8,12},{9,13},{10,... | collective-permute-start | bytes 1253384 | tf_op jit(solution)/shard_map/ppermute | solution.py:497
  94.7 3.2 %collective-permute-done.12.block_ref = bf16[96,2176]{1,0:T(8,128)(2,1)S(1)} collective-permute-done((bf16[96,2176]{1,0:T(8,128)(2,1)S(1)}, bf16[96,2176]{1,0:T(8,128)(2,1)S(1)}, u32[]{:S(2)}, u32[]{:S(2)}) %collective-permute-start.12) | collective-permute-done | bytes 417824 | tf_op jit(solution)/shard_map/ppermute | solution.py:497
  97.9 0.7 collective-permute-start.27
  98.6 0.6 choose.3
  99.2 14.8 %collective-permute-done.26.block_ref = bf16[96,2176]{1,0:T(8,128)(2,1)S(1)} collective-permute-done((bf16[96,2176]{1,0:T(8,128)(2,1)S(1)}, bf16[96,2176]{1,0:T(8,128)(2,1)S(1)}, u32[]{:S(2)}, u32[]{:S(2)}) %collective-permute-start.26) | collective-permute-done | bytes 417824 | tf_op jit(solution)/shard_map/ppermute | solution.py:497
  114.1 0.7 collective-permute-start.13
  115.2 2.5 %collective-permute-start.14 = (bf16[64,2048]{1,0:T(8,128)(2,1)S(1)}, bf16[64,2048]{1,0:T(8,128)(2,1)S(1)}, u32[]{:S(2)}, u32[]{:S(2)}) collective-permute-start(bf16[64,2048]{1,0:T(8,128)(2,1)S(1)} %get-tuple-element.65), channel_id=1, source_target_pairs={{0,16},{8,24},{16,0},{24,8},{1,17},{9,25},{17,1},{25,9},{2,18},{10... | collective-permute-start | bytes 786440 | tf_op jit(solution)/shard_map/ppermute | solution.py:416
  117.8 0.6 choose.4
  118.4 3.8 %collective-permute-done.13.refs_5_ = bf16[64,2048]{1,0:T(8,128)(2,1)S(1)} collective-permute-done((bf16[64,2048]{1,0:T(8,128)(2,1)S(1)}, bf16[64,2048]{1,0:T(8,128)(2,1)S(1)}, u32[]{:S(2)}, u32[]{:S(2)}) %collective-permute-start.13) | collective-permute-done | bytes 262176 | tf_op jit(solution)/shard_map/ppermute | solution.py:416
  122.2 2.5 %collective-permute-start.15 = (bf16[64,2048]{1,0:T(8,128)(2,1)S(1)}, bf16[64,2048]{1,0:T(8,128)(2,1)S(1)}, u32[]{:S(2)}, u32[]{:S(2)}) collective-permute-start(bf16[64,2048]{1,0:T(8,128)(2,1)S(1)} %get-tuple-element.66), channel_id=1, source_target_pairs={{0,24},{8,16},{16,8},{24,0},{1,25},{9,17},{17,9},{25,1},{2,26},{10... | collective-permute-start | bytes 786440 | tf_op jit(solution)/shard_map/ppermute | solution.py:416
  124.7 7.4 %collective-permute-start.31 = (bf16[64,2048]{1,0:T(8,128)(2,1)S(1)}, bf16[64,2048]{1,0:T(8,128)(2,1)S(1)}, u32[]{:S(2)}, u32[]{:S(2)}) collective-permute-start(bf16[64,2048]{1,0:T(8,128)(2,1)S(1)} %get-tuple-element.84), channel_id=1, source_target_pairs={{0,8},{8,0},{16,24},{24,16},{1,9},{9,1},{17,25},{25,17},{2,10},{10... | collective-permute-start | bytes 786440 | tf_op jit(solution)/shard_map/ppermute | solution.py:416
  132.1 0.6 choose.5
  132.8 1.6 collective-permute-start.32
  134.3 3.4 %collective-permute-done.31.refs_5_ = bf16[64,2048]{1,0:T(8,128)(2,1)S(1)} collective-permute-done((bf16[64,2048]{1,0:T(8,128)(2,1)S(1)}, bf16[64,2048]{1,0:T(8,128)(2,1)S(1)}, u32[]{:S(2)}, u32[]{:S(2)}) %collective-permute-start.31) | collective-permute-done | bytes 262176 | tf_op jit(solution)/shard_map/ppermute | solution.py:416
  137.7 2.5 %collective-permute-start.28 = (bf16[64,2048]{1,0:T(8,128)(2,1)S(1)}, bf16[64,2048]{1,0:T(8,128)(2,1)S(1)}, u32[]{:S(2)}, u32[]{:S(2)}) collective-permute-start(bf16[64,2048]{1,0:T(8,128)(2,1)S(1)} %get-tuple-element.80), channel_id=1, source_target_pairs={{0,8},{8,0},{16,24},{24,16},{1,9},{9,1},{17,25},{25,17},{2,10},{10... | collective-permute-start | bytes 786440 | tf_op jit(solution)/shard_map/ppermute | solution.py:416
  140.2 1.5 collective-permute-start.29
  141.7 1.5 collective-permute-start.30
  143.2 7.8 %experts.2 = (bf16[64,2048]{1,0:T(8,128)(2,1)S(1)}, bf16[64,2048]{1,0:T(8,128)(2,1)S(1)}, bf16[64,2048]{1,0:T(8,128)(2,1)S(1)}, bf16[64,2048]{1,0:T(8,128)(2,1)S...) custom-call(bf16[64,2048]{1,0:T(8,128)(2,1)S(1)} %get-tuple-element., ...), custom_call_target="tpu_custom_call" | custom-call | flops 3221225472 | bytes 12582912 | tf_op jit(solution)/shard_map/experts/pallas_call | solution.py:367
  151.0 0.6 collective-permute-start.23
  151.6 1.5 collective-permute-start.24
  153.1 4.6 %collective-permute-done.29.refs_2_ = bf16[64,2048]{1,0:T(8,128)(2,1)S(1)} collective-permute-done((bf16[64,2048]{1,0:T(8,128)(2,1)S(1)}, bf16[64,2048]{1,0:T(8,128)(2,1)S(1)}, u32[]{:S(2)}, u32[]{:S(2)}) %collective-permute-start.29) | collective-permute-done | bytes 262176 | tf_op jit(solution)/shard_map/ppermute | solution.py:416
  157.7 7.8 %experts.3 = (bf16[64,2048]{1,0:T(8,128)(2,1)S(1)}, bf16[64,2048]{1,0:T(8,128)(2,1)S(1)}, bf16[64,2048]{1,0:T(8,128)(2,1)S(1)}, bf16[64,2048]{1,0:T(8,128)(2,1)S...) custom-call(bf16[64,2048]{1,0:T(8,128)(2,1)S(1)} %get-tuple-element., ...), custom_call_target="tpu_custom_call" | custom-call | flops 3221225472 | bytes 12582912 | tf_op jit(solution)/shard_map/experts/pallas_call | solution.py:367
  165.9 2.4 %collective-permute-start.35 = (bf16[64,2048]{1,0:T(8,128)(2,1)S(1)}, bf16[64,2048]{1,0:T(8,128)(2,1)S(1)}, u32[]{:S(2)}, u32[]{:S(2)}) collective-permute-start(bf16[64,2048]{1,0:T(8,128)(2,1)S(1)} %get-tuple-element.89), channel_id=1, source_target_pairs={{0,16},{8,24},{16,0},{24,8},{1,17},{9,25},{17,1},{25,9},{2,18},{10... | collective-permute-start | bytes 786440 | tf_op jit(solution)/shard_map/ppermute | solution.py:416
  168.3 1.1 collective-permute-start.36
  169.5 0.6 collective-permute-start.38
  170.0 1.8 collective-permute-start.39
  171.8 2.9 %collective-permute-done.34.refs_1_ = bf16[64,2048]{1,0:T(8,128)(2,1)S(1)} collective-permute-done((bf16[64,2048]{1,0:T(8,128)(2,1)S(1)}, bf16[64,2048]{1,0:T(8,128)(2,1)S(1)}, u32[]{:S(2)}, u32[]{:S(2)}) %collective-permute-start.34) | collective-permute-done | bytes 262176 | tf_op jit(solution)/shard_map/ppermute | solution.py:416
  174.8 2.2 collective-permute-start.40
  177.0 2.6 %collective-permute-done.35.refs_2_ = bf16[64,2048]{1,0:T(8,128)(2,1)S(1)} collective-permute-done((bf16[64,2048]{1,0:T(8,128)(2,1)S(1)}, bf16[64,2048]{1,0:T(8,128)(2,1)S(1)}, u32[]{:S(2)}, u32[]{:S(2)}) %collective-permute-start.35) | collective-permute-done | bytes 262176 | tf_op jit(solution)/shard_map/ppermute | solution.py:416
  179.6 7.0 %collective-permute-start.21 = (bf16[64,2048]{1,0:T(8,128)(2,1)S(1)}, bf16[64,2048]{1,0:T(8,128)(2,1)S(1)}, u32[]{:S(2)}, u32[]{:S(2)}) collective-permute-start(bf16[64,2048]{1,0:T(8,128)(2,1)S(1)} %get-tuple-element.71), channel_id=1, source_target_pairs={{0,2},{1,3},{2,4},{3,5},{4,6},{5,7},{6,0},{7,1},{8,10},{9,11},{10,... | collective-permute-start | bytes 786440 | tf_op jit(solution)/shard_map/ppermute | solution.py:513
  187.0 3.7 %collective-permute-start.19 = (bf16[64,2048]{1,0:T(8,128)(2,1)S(1)}, bf16[64,2048]{1,0:T(8,128)(2,1)S(1)}, u32[]{:S(2)}, u32[]{:S(2)}) collective-permute-start(bf16[64,2048]{1,0:T(8,128)(2,1)S(1)} %get-tuple-element.68), channel_id=1, source_target_pairs={{0,8},{8,0},{16,24},{24,16},{1,9},{9,1},{17,25},{25,17},{2,10},{10... | collective-permute-start | bytes 786440 | tf_op jit(solution)/shard_map/ppermute | solution.py:416
  191.1 2.2 collective-permute-start.20
  193.3 2.1 collective-permute-start.25
  195.4 4.6 %collective-permute-start.37 = (bf16[96,2048]{1,0:T(8,128)(2,1)S(1)}, bf16[96,2048]{1,0:T(8,128)(2,1)S(1)}, u32[]{:S(2)}, u32[]{:S(2)}) collective-permute-start(bf16[96,2048]{1,0:T(8,128)(2,1)S(1)} %merge.6), channel_id=1, source_target_pairs={{0,4},{1,5},{2,6},{3,7},{4,0},{5,1},{6,2},{7,3},{8,12},{9,13},{10,... | collective-permute-start | bytes 1179656 | tf_op jit(solution)/shard_map/ppermute | solution.py:520
  200.4 6.3 %collective-permute-start.41 = (bf16[96,2048]{1,0:T(8,128)(2,1)S(1)}, bf16[96,2048]{1,0:T(8,128)(2,1)S(1)}, u32[]{:S(2)}, u32[]{:S(2)}) collective-permute-start(bf16[96,2048]{1,0:T(8,128)(2,1)S(1)} %merge.7), channel_id=1, source_target_pairs={{0,6},{1,7},{2,0},{3,1},{4,2},{5,3},{6,4},{7,5},{8,14},{9,15},{10,... | collective-permute-start | bytes 1179656 | tf_op jit(solution)/shard_map/ppermute | solution.py:520
  206.9 7.2 %collective-permute-done.22.refs_3_ = bf16[64,2048]{1,0:T(8,128)(2,1)S(1)} collective-permute-done((bf16[64,2048]{1,0:T(8,128)(2,1)S(1)}, bf16[64,2048]{1,0:T(8,128)(2,1)S(1)}, u32[]{:S(2)}, u32[]{:S(2)}) %collective-permute-start.22) | collective-permute-done | bytes 262176 | tf_op jit(solution)/shard_map/ppermute | solution.py:416
  214.6 13.8 %collective-permute-done.37 = bf16[96,2048]{1,0:T(8,128)(2,1)S(1)} collective-permute-done((bf16[96,2048]{1,0:T(8,128)(2,1)S(1)}, bf16[96,2048]{1,0:T(8,128)(2,1)S(1)}, u32[]{:S(2)}, u32[]{:S(2)}) %collective-permute-start.37) | collective-permute-done | bytes 393248 | tf_op jit(solution)/shard_map/ppermute | solution.py:520
  228.4 1.1 add_convert_fusion
  (86 shorter events, 5.6 us)
Async XLA Ops:
  0.0 2.1 copy-start.3
  0.0 4.9 %copy-start.4 = (bf16[768,2,128]{2,1,0:T(2,128)(2,1)S(1)}, bf16[768,2,128]{2,1,0:T(2,128)(2,1)}, u32[]{:S(2)}) copy-start(bf16[768,2,128]{2,1,0:T(2,128)(2,1)} %param.13) | copy-start | bytes 1179652
  2.0 7.1 %copy-start.9 = (s32[96,2]{0,1:T(2,128)S(1)}, s32[96,2]{0,1:T(2,128)}, u32[]{:S(2)}) copy-start(s32[96,2]{0,1:T(2,128)} %param.21) | copy-start | bytes 2308
  2.0 7.1 %copy-start.10 = (f32[96,2]{0,1:T(2,128)S(1)}, f32[96,2]{0,1:T(2,128)}, u32[]{:S(2)}) copy-start(f32[96,2]{0,1:T(2,128)} %param.22) | copy-start | bytes 2308
  2.0 7.2 %copy-start.14 = (f32[2]{0:T(128)S(1)}, f32[2]{0:T(128)}, u32[]{:S(2)}) copy-start(f32[2]{0:T(128)} %param.16) | copy-start | bytes 28
  2.0 27.8 %copy-start = (bf16[2,2048,256]{2,1,0:T(8,128)(2,1)S(1)}, bf16[2,2048,256]{2,1,0:T(8,128)(2,1)}, u32[]{:S(2)}) copy-start(bf16[2,2048,256]{2,1,0:T(8,128)(2,1)} %refs_8_.3) | copy-start | bytes 6291460
  2.1 30.9 %copy-start.5 = (bf16[768,128]{1,0:T(8,128)(2,1)}, bf16[768,128]{1,0:T(8,128)(2,1)S(1)}, u32[]{:S(2)}) copy-start(bf16[768,128]{1,0:T(8,128)(2,1)S(1)} %get-tuple-element.53.refs_8_) | copy-start | bytes 589828
  2.9 30.1 %copy-start.6 = (bf16[768,128]{1,0:T(8,128)(2,1)}, bf16[768,128]{1,0:T(8,128)(2,1)S(1)}, u32[]{:S(2)}) copy-start(bf16[768,128]{1,0:T(8,128)(2,1)S(1)} %get-tuple-element.98.refs_4_) | copy-start | bytes 589828
  2.9 17.8 %collective-permute-start.3 = (bf16[768,128]{1,0:T(8,128)(2,1)}, bf16[768,128]{1,0:T(8,128)(2,1)}, u32[]{:S(2)}, u32[]{:S(2)}) collective-permute-start(bf16[768,128]{1,0:T(8,128)(2,1)} %get-tuple-element.97), channel_id=1, source_target_pairs={{0,8},{8,0},{16,24},{24,16},{1,9},{9,1},{17,25},{25,17},{2,10},{10... | collective-permute-start | bytes 589832 | tf_op jit(solution)/shard_map/ppermute | solution.py:416
  4.4 25.4 %collective-permute-start.5 = (bf16[768,128]{1,0:T(8,128)(2,1)}, bf16[768,128]{1,0:T(8,128)(2,1)}, u32[]{:S(2)}, u32[]{:S(2)}) collective-permute-start(bf16[768,128]{1,0:T(8,128)(2,1)} %get-tuple-element.97), channel_id=1, source_target_pairs={{0,24},{8,16},{16,8},{24,0},{1,25},{9,17},{17,9},{25,1},{2,26},{10... | collective-permute-start | bytes 589832 | tf_op jit(solution)/shard_map/ppermute | solution.py:416
  5.7 11.5 %collective-permute-start = (bf16[384,128]{1,0:T(8,128)(2,1)S(1)}, bf16[384,128]{1,0:T(8,128)(2,1)S(1)}, u32[]{:S(2)}, u32[]{:S(2)}) collective-permute-start(bf16[384,128]{1,0:T(8,128)(2,1)S(1)} %get-tuple-element.101), channel_id=1, source_target_pairs={{0,8},{8,0},{16,24},{24,16},{1,9},{9,1},{17,25},{25,17},{2,10},{10... | collective-permute-start | bytes 294920 | tf_op jit(solution)/shard_map/ppermute | solution.py:416
  7.1 11.5 %collective-permute-start.1 = (bf16[384,128]{1,0:T(8,128)(2,1)S(1)}, bf16[384,128]{1,0:T(8,128)(2,1)}, u32[]{:S(2)}, u32[]{:S(2)}) collective-permute-start(bf16[384,128]{1,0:T(8,128)(2,1)S(1)} %get-tuple-element.100), channel_id=1, source_target_pairs={{0,16},{8,24},{16,0},{24,8},{1,17},{9,25},{17,1},{25,9},{2,18},{10... | collective-permute-start | bytes 294920 | tf_op jit(solution)/shard_map/ppermute | solution.py:416
  8.7 10.5 %collective-permute-start.2 = (bf16[384,128]{1,0:T(8,128)(2,1)S(1)}, bf16[384,128]{1,0:T(8,128)(2,1)}, u32[]{:S(2)}, u32[]{:S(2)}) collective-permute-start(bf16[384,128]{1,0:T(8,128)(2,1)S(1)} %get-tuple-element.99), channel_id=1, source_target_pairs={{0,24},{8,16},{16,8},{24,0},{1,25},{9,17},{17,9},{25,1},{2,26},{10... | collective-permute-start | bytes 294920 | tf_op jit(solution)/shard_map/ppermute | solution.py:416
  17.2 15.8 %copy-start.13 = (bf16[384,128]{1,0:T(8,128)(2,1)}, bf16[384,128]{1,0:T(8,128)(2,1)S(1)}, u32[]{:S(2)}) copy-start(bf16[384,128]{1,0:T(8,128)(2,1)S(1)} %collective-permute-done.refs_1_) | copy-start | bytes 294916
  17.2 13.2 %collective-permute-start.6 = (bf16[768,128]{1,0:T(8,128)(2,1)S(1)}, bf16[768,128]{1,0:T(8,128)(2,1)S(1)}, u32[]{:S(2)}, u32[]{:S(2)}) collective-permute-start(bf16[768,128]{1,0:T(8,128)(2,1)S(1)} %get-tuple-element.54), channel_id=1, source_target_pairs={{0,8},{8,0},{16,24},{24,16},{1,9},{9,1},{17,25},{25,17},{2,10},{10... | collective-permute-start | bytes 589832 | tf_op jit(solution)/shard_map/ppermute | solution.py:416
  18.7 13.6 %collective-permute-start.8 = (bf16[768,128]{1,0:T(8,128)(2,1)S(1)}, bf16[768,128]{1,0:T(8,128)(2,1)S(1)}, u32[]{:S(2)}, u32[]{:S(2)}) collective-permute-start(bf16[768,128]{1,0:T(8,128)(2,1)S(1)} %get-tuple-element.54), channel_id=1, source_target_pairs={{0,24},{8,16},{16,8},{24,0},{1,25},{9,17},{17,9},{25,1},{2,26},{10... | collective-permute-start | bytes 589832 | tf_op jit(solution)/shard_map/ppermute | solution.py:416
  19.2 10.7 %collective-permute-start.4 = (bf16[768,128]{1,0:T(8,128)(2,1)S(1)}, bf16[768,128]{1,0:T(8,128)(2,1)}, u32[]{:S(2)}, u32[]{:S(2)}) collective-permute-start(bf16[768,128]{1,0:T(8,128)(2,1)S(1)} %get-tuple-element.98.refs_4_), channel_id=1, source_target_pairs={{0,16},{8,24},{16,0},{24,8},{1,17},{9,25},{17,1},{25,9},{2,18},{10... | collective-permute-start | bytes 589832 | tf_op jit(solution)/shard_map/ppermute | solution.py:416
  20.7 11.6 %collective-permute-start.7 = (bf16[768,128]{1,0:T(8,128)(2,1)S(1)}, bf16[768,128]{1,0:T(8,128)(2,1)}, u32[]{:S(2)}, u32[]{:S(2)}) collective-permute-start(bf16[768,128]{1,0:T(8,128)(2,1)S(1)} %get-tuple-element.53.refs_8_), channel_id=1, source_target_pairs={{0,16},{8,24},{16,0},{24,8},{1,17},{9,25},{17,1},{25,9},{2,18},{10... | collective-permute-start | bytes 589832 | tf_op jit(solution)/shard_map/ppermute | solution.py:416
  29.8 107.9 %collective-permute-start.16 = (bf16[2,2048,256]{2,1,0:T(8,128)(2,1)S(1)}, bf16[2,2048,256]{2,1,0:T(8,128)(2,1)}, u32[]{:S(2)}, u32[]{:S(2)}) collective-permute-start(bf16[2,2048,256]{2,1,0:T(8,128)(2,1)S(1)} %copy-done), channel_id=1, source_target_pairs={{0,1},{1,0},{2,3},{3,2},{4,5},{5,4},{6,7},{7,6},{8,9},{9,8},{10,11... | collective-permute-start | bytes 6291464 | tf_op jit(solution)/shard_map/ppermute | solution.py:439
  29.8 110.4 %collective-permute-start.17 = (bf16[2,2048,256]{2,1,0:T(8,128)(2,1)}, bf16[2,2048,256]{2,1,0:T(8,128)(2,1)}, u32[]{:S(2)}, u32[]{:S(2)}) collective-permute-start(bf16[2,2048,256]{2,1,0:T(8,128)(2,1)} %refs_9_.3), channel_id=1, source_target_pairs={{0,1},{1,0},{2,3},{3,2},{4,5},{5,4},{6,7},{7,6},{8,9},{9,8},{10,11... | collective-permute-start | bytes 6291464 | tf_op jit(solution)/shard_map/ppermute | solution.py:439
  30.3 2.7 %copy-start.11 = (bf16[768,128]{1,0:T(8,128)(2,1)}, bf16[768,128]{1,0:T(8,128)(2,1)S(1)}, u32[]{:S(2)}) copy-start(bf16[768,128]{1,0:T(8,128)(2,1)S(1)} %collective-permute-done.6.refs_9_) | copy-start | bytes 589828
  30.4 111.4 %collective-permute-start.18 = (bf16[2,256,2048]{2,1,0:T(8,128)(2,1)}, bf16[2,256,2048]{2,1,0:T(8,128)(2,1)}, u32[]{:S(2)}, u32[]{:S(2)}) collective-permute-start(bf16[2,256,2048]{2,1,0:T(8,128)(2,1)} %refs_10_.3), channel_id=1, source_target_pairs={{0,1},{1,0},{2,3},{3,2},{4,5},{5,4},{6,7},{7,6},{8,9},{9,8},{10,11... | collective-permute-start | bytes 6291464 | tf_op jit(solution)/shard_map/ppermute | solution.py:439
  32.3 0.7 copy-start.12
  33.0 22.3 %copy-start.7 = (f32[96,8]{1,0:T(8,128)S(1)}, f32[96,8]{1,0:T(8,128)}, u32[]{:S(2)}) copy-start(f32[96,8]{1,0:T(8,128)} %copy.42) | copy-start | bytes 9220
  33.0 22.3 %copy-start.8 = (pred[96,8]{1,0:T(8,128)(4,1)S(1)}, pred[96,8]{1,0:T(8,128)(4,1)}, u32[]{:S(2)}) copy-start(pred[96,8]{1,0:T(8,128)(4,1)} %copy.43) | copy-start | bytes 2308
  33.0 32.2 %copy-start.1 = (bf16[96,2048]{1,0:T(8,128)(2,1)S(1)}, bf16[96,2048]{1,0:T(8,128)(2,1)}, u32[]{:S(2)}) copy-start(bf16[96,2048]{1,0:T(8,128)(2,1)} %residual_ref.1) | copy-start | bytes 1179652
  33.0 32.1 %copy-start.2 = (f32[2048]{0:T(1024)S(1)}, f32[2048]{0:T(1024)}, u32[]{:S(2)}) copy-start(f32[2048]{0:T(1024)} %param.20) | copy-start | bytes 24580
  49.4 15.8 %all-to-all-start = ((bf16[32,48,128]{2,1,0:T(8,128)(2,1)}), bf16[32,48,128]{2,1,0:T(8,128)(2,1)S(1)}, u32[]{:S(2)}, u32[]{:S(2)}) async-start(bf16[32,48,128]{2,1,0:T(8,128)(2,1)} %bitcast.31), calls=%async_computation | async-start | bytes 786432 | tf_op jit(solution)/shard_map/all_to_all | solution.py:453
  69.6 13.9 %collective-permute-start.10 = (bf16[64,2048]{1,0:T(8,128)(2,1)S(1)}, bf16[64,2048]{1,0:T(8,128)(2,1)S(1)}, u32[]{:S(2)}, u32[]{:S(2)}) collective-permute-start(bf16[64,2048]{1,0:T(8,128)(2,1)S(1)} %get-tuple-element.60), channel_id=1, source_target_pairs={{0,16},{8,24},{16,0},{24,8},{1,17},{9,25},{17,1},{25,9},{2,18},{10... | collective-permute-start | bytes 786440 | tf_op jit(solution)/shard_map/ppermute | solution.py:416
  70.0 14.6 %collective-permute-start.11 = (bf16[64,2048]{1,0:T(8,128)(2,1)S(1)}, bf16[64,2048]{1,0:T(8,128)(2,1)S(1)}, u32[]{:S(2)}, u32[]{:S(2)}) collective-permute-start(bf16[64,2048]{1,0:T(8,128)(2,1)S(1)} %get-tuple-element.61), channel_id=1, source_target_pairs={{0,24},{8,16},{16,8},{24,0},{1,25},{9,17},{17,9},{25,1},{2,26},{10... | collective-permute-start | bytes 786440 | tf_op jit(solution)/shard_map/ppermute | solution.py:416
  83.5 14.4 %collective-permute-start.12 = (bf16[96,2176]{1,0:T(8,128)(2,1)S(1)}, bf16[96,2176]{1,0:T(8,128)(2,1)S(1)}, u32[]{:S(2)}, u32[]{:S(2)}) collective-permute-start(bf16[96,2176]{1,0:T(8,128)(2,1)S(1)} %get-tuple-element.62), channel_id=1, source_target_pairs={{0,6},{1,7},{2,0},{3,1},{4,2},{5,3},{6,4},{7,5},{8,14},{9,15},{10,... | collective-permute-start | bytes 1253384 | tf_op jit(solution)/shard_map/ppermute | solution.py:497
  84.6 7.2 %collective-permute-start.9 = (bf16[64,2048]{1,0:T(8,128)(2,1)S(1)}, bf16[64,2048]{1,0:T(8,128)(2,1)S(1)}, u32[]{:S(2)}, u32[]{:S(2)}) collective-permute-start(bf16[64,2048]{1,0:T(8,128)(2,1)S(1)} %get-tuple-element.59), channel_id=1, source_target_pairs={{0,8},{8,0},{16,24},{24,16},{1,9},{9,1},{17,25},{25,17},{2,10},{10... | collective-permute-start | bytes 786440 | tf_op jit(solution)/shard_map/ppermute | solution.py:416
  91.8 22.3 %collective-permute-start.26 = (bf16[96,2176]{1,0:T(8,128)(2,1)S(1)}, bf16[96,2176]{1,0:T(8,128)(2,1)S(1)}, u32[]{:S(2)}, u32[]{:S(2)}) collective-permute-start(bf16[96,2176]{1,0:T(8,128)(2,1)S(1)} %get-tuple-element.62), channel_id=1, source_target_pairs={{0,4},{1,5},{2,6},{3,7},{4,0},{5,1},{6,2},{7,3},{8,12},{9,13},{10,... | collective-permute-start | bytes 1253384 | tf_op jit(solution)/shard_map/ppermute | solution.py:497
  97.9 17.3 %collective-permute-start.27 = (bf16[96,2176]{1,0:T(8,128)(2,1)S(1)}, bf16[96,2176]{1,0:T(8,128)(2,1)S(1)}, u32[]{:S(2)}, u32[]{:S(2)}) collective-permute-start(bf16[96,2176]{1,0:T(8,128)(2,1)S(1)} %get-tuple-element.62), channel_id=1, source_target_pairs={{0,2},{1,3},{2,4},{3,5},{4,6},{5,7},{6,0},{7,1},{8,10},{9,11},{10,... | collective-permute-start | bytes 1253384 | tf_op jit(solution)/shard_map/ppermute | solution.py:497
  114.1 8.1 %collective-permute-start.13 = (bf16[64,2048]{1,0:T(8,128)(2,1)S(1)}, bf16[64,2048]{1,0:T(8,128)(2,1)S(1)}, u32[]{:S(2)}, u32[]{:S(2)}) collective-permute-start(bf16[64,2048]{1,0:T(8,128)(2,1)S(1)} %get-tuple-element.64), channel_id=1, source_target_pairs={{0,8},{8,0},{16,24},{24,16},{1,9},{9,1},{17,25},{25,17},{2,10},{10... | collective-permute-start | bytes 786440 | tf_op jit(solution)/shard_map/ppermute | solution.py:416
  115.2 9.5 %collective-permute-start.14 = (bf16[64,2048]{1,0:T(8,128)(2,1)S(1)}, bf16[64,2048]{1,0:T(8,128)(2,1)S(1)}, u32[]{:S(2)}, u32[]{:S(2)}) collective-permute-start(bf16[64,2048]{1,0:T(8,128)(2,1)S(1)} %get-tuple-element.65), channel_id=1, source_target_pairs={{0,16},{8,24},{16,0},{24,8},{1,17},{9,25},{17,1},{25,9},{2,18},{10... | collective-permute-start | bytes 786440 | tf_op jit(solution)/shard_map/ppermute | solution.py:416
  122.2 10.6 %collective-permute-start.15 = (bf16[64,2048]{1,0:T(8,128)(2,1)S(1)}, bf16[64,2048]{1,0:T(8,128)(2,1)S(1)}, u32[]{:S(2)}, u32[]{:S(2)}) collective-permute-start(bf16[64,2048]{1,0:T(8,128)(2,1)S(1)} %get-tuple-element.66), channel_id=1, source_target_pairs={{0,24},{8,16},{16,8},{24,0},{1,25},{9,17},{17,9},{25,1},{2,26},{10... | collective-permute-start | bytes 786440 | tf_op jit(solution)/shard_map/ppermute | solution.py:416
  124.7 13.0 %collective-permute-start.31 = (bf16[64,2048]{1,0:T(8,128)(2,1)S(1)}, bf16[64,2048]{1,0:T(8,128)(2,1)S(1)}, u32[]{:S(2)}, u32[]{:S(2)}) collective-permute-start(bf16[64,2048]{1,0:T(8,128)(2,1)S(1)} %get-tuple-element.84), channel_id=1, source_target_pairs={{0,8},{8,0},{16,24},{24,16},{1,9},{9,1},{17,25},{25,17},{2,10},{10... | collective-permute-start | bytes 786440 | tf_op jit(solution)/shard_map/ppermute | solution.py:416
  132.8 18.2 %collective-permute-start.32 = (bf16[64,2048]{1,0:T(8,128)(2,1)S(1)}, bf16[64,2048]{1,0:T(8,128)(2,1)S(1)}, u32[]{:S(2)}, u32[]{:S(2)}) collective-permute-start(bf16[64,2048]{1,0:T(8,128)(2,1)S(1)} %get-tuple-element.85), channel_id=1, source_target_pairs={{0,16},{8,24},{16,0},{24,8},{1,17},{9,25},{17,1},{25,9},{2,18},{10... | collective-permute-start | bytes 786440 | tf_op jit(solution)/shard_map/ppermute | solution.py:416
  137.7 13.9 %collective-permute-start.33 = (bf16[64,2048]{1,0:T(8,128)(2,1)S(1)}, bf16[64,2048]{1,0:T(8,128)(2,1)S(1)}, u32[]{:S(2)}, u32[]{:S(2)}) collective-permute-start(bf16[64,2048]{1,0:T(8,128)(2,1)S(1)} %get-tuple-element.86), channel_id=1, source_target_pairs={{0,24},{8,16},{16,8},{24,0},{1,25},{9,17},{17,9},{25,1},{2,26},{10... | collective-permute-start | bytes 786440 | tf_op jit(solution)/shard_map/ppermute | solution.py:416
  137.7 15.4 %collective-permute-start.28 = (bf16[64,2048]{1,0:T(8,128)(2,1)S(1)}, bf16[64,2048]{1,0:T(8,128)(2,1)S(1)}, u32[]{:S(2)}, u32[]{:S(2)}) collective-permute-start(bf16[64,2048]{1,0:T(8,128)(2,1)S(1)} %get-tuple-element.80), channel_id=1, source_target_pairs={{0,8},{8,0},{16,24},{24,16},{1,9},{9,1},{17,25},{25,17},{2,10},{10... | collective-permute-start | bytes 786440 | tf_op jit(solution)/shard_map/ppermute | solution.py:416
  140.2 17.5 %collective-permute-start.29 = (bf16[64,2048]{1,0:T(8,128)(2,1)S(1)}, bf16[64,2048]{1,0:T(8,128)(2,1)S(1)}, u32[]{:S(2)}, u32[]{:S(2)}) collective-permute-start(bf16[64,2048]{1,0:T(8,128)(2,1)S(1)} %get-tuple-element.81), channel_id=1, source_target_pairs={{0,16},{8,24},{16,0},{24,8},{1,17},{9,25},{17,1},{25,9},{2,18},{10... | collective-permute-start | bytes 786440 | tf_op jit(solution)/shard_map/ppermute | solution.py:416
  141.7 16.0 %collective-permute-start.30 = (bf16[64,2048]{1,0:T(8,128)(2,1)S(1)}, bf16[64,2048]{1,0:T(8,128)(2,1)S(1)}, u32[]{:S(2)}, u32[]{:S(2)}) collective-permute-start(bf16[64,2048]{1,0:T(8,128)(2,1)S(1)} %get-tuple-element.82), channel_id=1, source_target_pairs={{0,24},{8,16},{16,8},{24,0},{1,25},{9,17},{17,9},{25,1},{2,26},{10... | collective-permute-start | bytes 786440 | tf_op jit(solution)/shard_map/ppermute | solution.py:416
  151.0 18.4 %collective-permute-start.23 = (bf16[64,2048]{1,0:T(8,128)(2,1)S(1)}, bf16[64,2048]{1,0:T(8,128)(2,1)S(1)}, u32[]{:S(2)}, u32[]{:S(2)}) collective-permute-start(bf16[64,2048]{1,0:T(8,128)(2,1)S(1)} %get-tuple-element.75), channel_id=1, source_target_pairs={{0,8},{8,0},{16,24},{24,16},{1,9},{9,1},{17,25},{25,17},{2,10},{10... | collective-permute-start | bytes 786440 | tf_op jit(solution)/shard_map/ppermute | solution.py:416
  151.6 18.4 %collective-permute-start.24 = (bf16[64,2048]{1,0:T(8,128)(2,1)S(1)}, bf16[64,2048]{1,0:T(8,128)(2,1)S(1)}, u32[]{:S(2)}, u32[]{:S(2)}) collective-permute-start(bf16[64,2048]{1,0:T(8,128)(2,1)S(1)} %get-tuple-element.76), channel_id=1, source_target_pairs={{0,16},{8,24},{16,0},{24,8},{1,17},{9,25},{17,1},{25,9},{2,18},{10... | collective-permute-start | bytes 786440 | tf_op jit(solution)/shard_map/ppermute | solution.py:416
  165.5 9.2 %collective-permute-start.34 = (bf16[64,2048]{1,0:T(8,128)(2,1)S(1)}, bf16[64,2048]{1,0:T(8,128)(2,1)S(1)}, u32[]{:S(2)}, u32[]{:S(2)}) collective-permute-start(bf16[64,2048]{1,0:T(8,128)(2,1)S(1)} %get-tuple-element.88), channel_id=1, source_target_pairs={{0,8},{8,0},{16,24},{24,16},{1,9},{9,1},{17,25},{25,17},{2,10},{10... | collective-permute-start | bytes 786440 | tf_op jit(solution)/shard_map/ppermute | solution.py:416
  165.9 13.6 %collective-permute-start.35 = (bf16[64,2048]{1,0:T(8,128)(2,1)S(1)}, bf16[64,2048]{1,0:T(8,128)(2,1)S(1)}, u32[]{:S(2)}, u32[]{:S(2)}) collective-permute-start(bf16[64,2048]{1,0:T(8,128)(2,1)S(1)} %get-tuple-element.89), channel_id=1, source_target_pairs={{0,16},{8,24},{16,0},{24,8},{1,17},{9,25},{17,1},{25,9},{2,18},{10... | collective-permute-start | bytes 786440 | tf_op jit(solution)/shard_map/ppermute | solution.py:416
  168.3 18.6 %collective-permute-start.36 = (bf16[64,2048]{1,0:T(8,128)(2,1)S(1)}, bf16[64,2048]{1,0:T(8,128)(2,1)S(1)}, u32[]{:S(2)}, u32[]{:S(2)}) collective-permute-start(bf16[64,2048]{1,0:T(8,128)(2,1)S(1)} %get-tuple-element.90), channel_id=1, source_target_pairs={{0,24},{8,16},{16,8},{24,0},{1,25},{9,17},{17,9},{25,1},{2,26},{10... | collective-permute-start | bytes 786440 | tf_op jit(solution)/shard_map/ppermute | solution.py:416
  169.5 21.7 %collective-permute-start.38 = (bf16[64,2048]{1,0:T(8,128)(2,1)S(1)}, bf16[64,2048]{1,0:T(8,128)(2,1)S(1)}, u32[]{:S(2)}, u32[]{:S(2)}) collective-permute-start(bf16[64,2048]{1,0:T(8,128)(2,1)S(1)} %get-tuple-element.94), channel_id=1, source_target_pairs={{0,8},{8,0},{16,24},{24,16},{1,9},{9,1},{17,25},{25,17},{2,10},{10... | collective-permute-start | bytes 786440 | tf_op jit(solution)/shard_map/ppermute | solution.py:416
  170.0 23.2 %collective-permute-start.39 = (bf16[64,2048]{1,0:T(8,128)(2,1)S(1)}, bf16[64,2048]{1,0:T(8,128)(2,1)S(1)}, u32[]{:S(2)}, u32[]{:S(2)}) collective-permute-start(bf16[64,2048]{1,0:T(8,128)(2,1)S(1)} %get-tuple-element.95), channel_id=1, source_target_pairs={{0,16},{8,24},{16,0},{24,8},{1,17},{9,25},{17,1},{25,9},{2,18},{10... | collective-permute-start | bytes 786440 | tf_op jit(solution)/shard_map/ppermute | solution.py:416
  174.8 20.6 %collective-permute-start.40 = (bf16[64,2048]{1,0:T(8,128)(2,1)S(1)}, bf16[64,2048]{1,0:T(8,128)(2,1)S(1)}, u32[]{:S(2)}, u32[]{:S(2)}) collective-permute-start(bf16[64,2048]{1,0:T(8,128)(2,1)S(1)} %get-tuple-element.96), channel_id=1, source_target_pairs={{0,24},{8,16},{16,8},{24,0},{1,25},{9,17},{17,9},{25,1},{2,26},{10... | collective-permute-start | bytes 786440 | tf_op jit(solution)/shard_map/ppermute | solution.py:416
  179.6 20.9 %collective-permute-start.21 = (bf16[64,2048]{1,0:T(8,128)(2,1)S(1)}, bf16[64,2048]{1,0:T(8,128)(2,1)S(1)}, u32[]{:S(2)}, u32[]{:S(2)}) collective-permute-start(bf16[64,2048]{1,0:T(8,128)(2,1)S(1)} %get-tuple-element.71), channel_id=1, source_target_pairs={{0,2},{1,3},{2,4},{3,5},{4,6},{5,7},{6,0},{7,1},{8,10},{9,11},{10,... | collective-permute-start | bytes 786440 | tf_op jit(solution)/shard_map/ppermute | solution.py:513
  187.0 19.8 %collective-permute-start.19 = (bf16[64,2048]{1,0:T(8,128)(2,1)S(1)}, bf16[64,2048]{1,0:T(8,128)(2,1)S(1)}, u32[]{:S(2)}, u32[]{:S(2)}) collective-permute-start(bf16[64,2048]{1,0:T(8,128)(2,1)S(1)} %get-tuple-element.68), channel_id=1, source_target_pairs={{0,8},{8,0},{16,24},{24,16},{1,9},{9,1},{17,25},{25,17},{2,10},{10... | collective-permute-start | bytes 786440 | tf_op jit(solution)/shard_map/ppermute | solution.py:416
  191.1 15.8 %collective-permute-start.20 = (bf16[64,2048]{1,0:T(8,128)(2,1)S(1)}, bf16[64,2048]{1,0:T(8,128)(2,1)S(1)}, u32[]{:S(2)}, u32[]{:S(2)}) collective-permute-start(bf16[64,2048]{1,0:T(8,128)(2,1)S(1)} %get-tuple-element.69), channel_id=1, source_target_pairs={{0,16},{8,24},{16,0},{24,8},{1,17},{9,25},{17,1},{25,9},{2,18},{10... | collective-permute-start | bytes 786440 | tf_op jit(solution)/shard_map/ppermute | solution.py:416
  193.3 21.3 %collective-permute-start.25 = (bf16[96,2048]{1,0:T(8,128)(2,1)S(1)}, bf16[96,2048]{1,0:T(8,128)(2,1)S(1)}, u32[]{:S(2)}, u32[]{:S(2)}) collective-permute-start(bf16[96,2048]{1,0:T(8,128)(2,1)S(1)} %merge.5), channel_id=1, source_target_pairs={{0,2},{1,3},{2,4},{3,5},{4,6},{5,7},{6,0},{7,1},{8,10},{9,11},{10,... | collective-permute-start | bytes 1179656 | tf_op jit(solution)/shard_map/ppermute | solution.py:520
  195.4 33.1 %collective-permute-start.37 = (bf16[96,2048]{1,0:T(8,128)(2,1)S(1)}, bf16[96,2048]{1,0:T(8,128)(2,1)S(1)}, u32[]{:S(2)}, u32[]{:S(2)}) collective-permute-start(bf16[96,2048]{1,0:T(8,128)(2,1)S(1)} %merge.6), channel_id=1, source_target_pairs={{0,4},{1,5},{2,6},{3,7},{4,0},{5,1},{6,2},{7,3},{8,12},{9,13},{10,... | collective-permute-start | bytes 1179656 | tf_op jit(solution)/shard_map/ppermute | solution.py:520
  200.4 28.0 %collective-permute-start.41 = (bf16[96,2048]{1,0:T(8,128)(2,1)S(1)}, bf16[96,2048]{1,0:T(8,128)(2,1)S(1)}, u32[]{:S(2)}, u32[]{:S(2)}) collective-permute-start(bf16[96,2048]{1,0:T(8,128)(2,1)S(1)} %merge.7), channel_id=1, source_target_pairs={{0,6},{1,7},{2,0},{3,1},{4,2},{5,3},{6,4},{7,5},{8,14},{9,15},{10,... | collective-permute-start | bytes 1179656 | tf_op jit(solution)/shard_map/ppermute | solution.py:520
  206.8 7.3 %collective-permute-start.22 = (bf16[64,2048]{1,0:T(8,128)(2,1)S(1)}, bf16[64,2048]{1,0:T(8,128)(2,1)S(1)}, u32[]{:S(2)}, u32[]{:S(2)}) collective-permute-start(bf16[64,2048]{1,0:T(8,128)(2,1)S(1)} %add_convert_fusion.1), channel_id=1, source_target_pairs={{0,24},{8,16},{16,8},{24,0},{1,25},{9,17},{17,9},{25,1},{2,26},{10... | collective-permute-start | bytes 786440 | tf_op jit(solution)/shard_map/ppermute | solution.py:416
